TPU v7x, 32 devices: a whole 2x2x4 slice. The times are simulated.
32 devices in a mesh: kv: 8 (over z, y), tp: 4 (over x, core).
Axes of the slice: x: 2, y: 2, z: 4, core: 2. Of those that a mesh axis runs over, the one named last changes fastest.
Arguments:
- tokens: bfloat16 [3072, 2048], P('kv'), may hold values from -40 to 40
- w_query: bfloat16 [2048, 2048], P(None, 'tp'), may hold values from -0.125 to 0.125
- w_key: bfloat16 [2048, 256], replicated, may hold values from -0.125 to 0.125
- w_value: bfloat16 [2048, 256], replicated, may hold values from -0.125 to 0.125
- w_out: bfloat16 [2048, 2048], P(None, 'tp'), may hold values from -0.125 to 0.125
- chosen: int32 [48, 32], P('kv'), may hold values from -1 to 46, as said below
Outputs:
- mixed: bfloat16 [3072, 2048], P('kv', 'tp')
Inputs may be any that keep to these rules, and one draw needn't show every extreme that they name: `chosen`: row b lists min(b, 32) different blocks below b, block b - 1 among them when b > 0, and -1 in its other entries.
All inputs are finite; a program needn't handle non-finite values.
Results may differ from a plain program's by a relative error of at most 0.015.
The roundings to bfloat16 on the way count: a program that leaves them out, or rounds other values in their place, can miss the bound.
Values may be sent and summed in bfloat16 or wider, within the bound.
No kernel may reach another device: no remote copies, remote signals or barrier semaphores. Data moves between devices by JAX's collectives and lax.ppermute only.
A program may use at most 128 MiB of HBM per device.

v0:
```python
import jax
import jax.numpy as jnp
from jax import lax
from jax.sharding import PartitionSpec as P

H = 16
DH = 128
KVH = 2
BLK = 64
NSEL = 32


theta_base = 10000.0


def rotate(values, positions):
    half = values.shape[-1] // 2
    inverse = theta_base ** (-jnp.arange(half, dtype=jnp.float32) / half)
    angles = positions.astype(jnp.float32)[:, None] * inverse[None, :]
    cosine = jnp.cos(angles)[:, None, :]
    sine = jnp.sin(angles)[:, None, :]
    first = values[..., :half]
    second = values[..., half:]
    return jnp.concatenate(
        [first * cosine - second * sine, second * cosine + first * sine], axis=-1
    )


def body(tokens, w_query, w_key, w_value, w_out, chosen):
    rows = tokens.shape[0]
    width = tokens.shape[1]
    tp_count = lax.axis_size("tp")
    tp_index = lax.axis_index("tp")
    kv_index = lax.axis_index("kv")
    split = BLK // tp_count
    local_blocks = rows // BLK
    group = H // KVH
    own_heads = w_query.shape[1] // DH
    slots = NSEL + 1
    positions = kv_index * rows + jnp.arange(rows, dtype=jnp.int32)
    query = jnp.dot(tokens, w_query, preferred_element_type=jnp.float32).reshape(
        rows, own_heads, DH
    )
    query = rotate(query, positions).astype(jnp.bfloat16).reshape(rows, own_heads * DH)
    query_all = lax.all_gather(query, "tp", axis=1, tiled=True)
    offset = tp_index * split
    slab = lax.dynamic_slice_in_dim(tokens.reshape(local_blocks, BLK, width), offset, split, 1)
    slab = slab.reshape(local_blocks * split, width)
    slab_pos = kv_index * rows + jnp.arange(local_blocks, dtype=jnp.int32)[:, None] * BLK + offset
    slab_pos = (slab_pos + jnp.arange(split, dtype=jnp.int32)[None, :]).reshape(-1)
    keys = jnp.dot(slab, w_key, preferred_element_type=jnp.float32).reshape(-1, KVH, DH)
    keys = rotate(keys, slab_pos).astype(jnp.bfloat16).reshape(-1, KVH * DH)
    values = jnp.dot(slab, w_value, preferred_element_type=jnp.float32).astype(jnp.bfloat16)
    first_block = kv_index * local_blocks
    lists = jnp.concatenate(
        [chosen, (first_block + jnp.arange(local_blocks, dtype=jnp.int32))[:, None]], axis=1
    )
    safe = jnp.maximum(lists, 0)
    key_all, value_all = (
        lax.all_gather(keys, "kv", axis=0, tiled=True),
        lax.all_gather(values, "kv", axis=0, tiled=True),
    )
    picked_keys = key_all.reshape(-1, split, KVH * DH)[safe]
    picked_values = value_all.reshape(-1, split, KVH * DH)[safe]
    query_five = query_all.reshape(local_blocks, BLK, KVH, group, DH)
    key_five = picked_keys.reshape(local_blocks, slots, split, KVH, DH)
    scores = jnp.einsum(
        "nqkgd,nsrkd->nkgqsr", query_five, key_five, preferred_element_type=jnp.float32
    ) * DH ** (-0.5)
    query_pos = positions.reshape(local_blocks, BLK)
    key_pos = safe[:, :, None] * BLK + offset + jnp.arange(split, dtype=jnp.int32)[None, None, :]
    allowed = (lists[:, :, None] >= 0)[:, None, :, :] & (
        key_pos[:, None, :, :] <= query_pos[:, :, None, None]
    )
    allowed = allowed[:, None, None]
    scores = jnp.where(allowed, scores, -jnp.inf)
    local_top = jnp.max(scores, axis=(4, 5))
    top = lax.pmax(local_top, "tp")
    weights = jnp.where(allowed, jnp.exp(scores - top[..., None, None]), 0.0)
    total_local = jnp.sum(weights, axis=(4, 5))
    probs = weights.astype(jnp.bfloat16)
    value_five = picked_values.reshape(local_blocks, slots, split, KVH, DH)
    part = jnp.einsum("nkgqsr,nsrkd->nqkgd", probs, value_five, preferred_element_type=jnp.float32)
    part = part.astype(jnp.bfloat16).reshape(1, rows, H * DH)
    moved = lax.all_to_all(part, "tp", split_axis=2, concat_axis=0, tiled=True)
    summed = jnp.sum(moved.astype(jnp.float32), axis=0).reshape(rows, own_heads, DH)
    totals = jnp.transpose(total_local, (0, 3, 1, 2)).reshape(rows, H)
    whole_totals = lax.psum(totals, "tp")
    mine = lax.dynamic_slice_in_dim(whole_totals, tp_index * own_heads, own_heads, 1)
    attention = (summed / mine[:, :, None]).astype(jnp.bfloat16).reshape(rows, own_heads * DH)
    result = jnp.dot(
        lax.all_gather(attention, "tp", axis=1, tiled=True),
        w_out,
        preferred_element_type=jnp.float32,
    )
    return result.astype(jnp.bfloat16)


def solution(mesh):
    placed = (P("kv", None), P(None, "tp"), P(), P(), P(None, "tp"), P("kv", None))
    return jax.shard_map(body, mesh=mesh, in_specs=placed, out_specs=P("kv", "tp"), check_vma=False)
```

profile of v0, /device:TPU:0, one launch (start us, length us, event | category | flops | bytes accessed | tf_op | source)
XLA Modules:
  0.0 265.4 jit_solution(6446708634427179163)
XLA Ops:
  6.6 1.6 copy-done
  8.1 2.4 fusion.21
  14.9 1.0 constant_dynamic-slice_fusion.1
  16.6 32.9 %all_gather.13 = bf16[768,256]{1,0:T(8,128)(2,1)S(1)} all-gather(bf16[96,256]{1,0:T(8,128)(2,1)S(1)} %copy_bitcast_fusion.1), channel_id=1, replica_groups=mesh['kv'=8,'tp'=4] {'kv'}, dimensions={0}, use_global_device_ids=true | all-gather | bytes 442368 | tf_op jit(solution)/shard_map/all_gather | solution.py:60
  50.3 1.9 reshape.258
  52.5 31.0 %all_gather.12 = bf16[768,256]{1,0:T(8,128)(2,1)S(1)} all-gather(bf16[96,256]{1,0:T(8,128)(2,1)S(1)} %convolution_convert_fusion.1), channel_id=1, replica_groups=mesh['kv'=8,'tp'=4] {'kv'}, dimensions={0}, use_global_device_ids=true | all-gather | bytes 442368 | tf_op jit(solution)/shard_map/all_gather | solution.py:61
  84.3 1.9 reshape.256
  87.4 1.9 copy.54
  89.3 11.1 %fusion = (f32[6,2,8,64]{3,2,1,0:T(8,128)S(1)}, f32[6,2,33,16,64,8]{4,3,5,2,1,0:T(8,128)}) fusion(pred[6,64,33,16]{1,3,2,0:T(8,128)(4,1)S(1)} %compare_and_fusion, bf16[6,64,2,8,128,1]{4,3,2,1,0,5:T(8,128)(2,1)S(1)} %bitcast.72, bf16[6,33,16,2,128,1]{4,3,2,1,0,5:T(2,128)(2,1)S(1)} %bitcast.71), kind=kOutput, calls=%fused_computation.4 | convolution fusion | flops 840198144 | bytes 16398336 | tf_op jit(solution)/shard_map/nqkgd,nsrkd->nkgqsr/dot_general | solution.py:67
  100.4 10.5 %pmax.7 = f32[6,2,8,64]{3,2,1,0:T(8,128)S(1)} all-reduce(f32[6,2,8,64]{3,2,1,0:T(8,128)S(1)} %get-tuple-element.15), channel_id=1, replica_groups=mesh['kv'=8,'tp'=4] {'tp'}, use_global_device_ids=true, to_apply=%region_1.2 | all-reduce | flops 6144 | bytes 49152 | tf_op jit(solution)/shard_map/pmax | solution.py:78
  110.9 16.9 %fusion.1 = (f32[6,2,8,64]{3,2,1,0:T(8,128)S(1)}, bf16[6,2,8,64,33,16]{3,5,2,4,1,0:T(8,128)(2,1)}) fusion(f32[6,2,33,16,64,8]{4,3,5,2,1,0:T(8,128)} %get-tuple-element.16, f32[6,2,8,64]{3,2,1,0:T(8,128)S(1)} %pmax.7, pred[6,64,33,16]{1,3,2,0:T(8,128)(4,1)S(1)} %compare_and_fusion), kind=kLoop, calls=%fused_computation.5 | loop fusion | flops 19458048 | bytes 19716096 | tf_op jit(solution)/shard_map/reduce_sum | solution.py:80
  127.9 17.0 %fusion.13 = bf16[6,64,2,8,128]{4,1,3,2,0:T(8,128)(2,1)} fusion(bf16[6,2,8,64,33,16]{3,5,2,4,1,0:T(8,128)(2,1)} %get-tuple-element.6, bf16[6,33,16,2,128,1]{4,3,2,1,0,5:T(2,128)(2,1)S(1)} %bitcast.76), kind=kOutput, calls=%fused_computation.15 | convolution fusion | flops 831258624 | bytes 9682944 | tf_op jit(solution)/shard_map/nkgqsr,nsrkd->nqkgd/dot_general | solution.py:83
  144.9 2.6 copy.37
  147.6 2.1 reshape.261
  149.6 8.5 %copy.38 = bf16[1,384,2048]{1,0,2:T(2,128)(2,1)} copy(bf16[1,384,2048]{2,1,0:T(8,128)(2,1)} %reshape.261) | data formatting | bytes 3145728 | tf_op jit(solution)/shard_map/reshape | solution.py:84
  158.6 34.3 %reduce.3 = bf16[2048,384]{1,0:T(8,128)(2,1)S(1)} reduce(bf16[2048,1,384]{2,1,0:T(2,128)(2,1)} %bitcast.66, bf16[]{:T(256)} %broadcast.190), dimensions={1}, to_apply=%bitcast.54.reduce_sub_computation | reduce | bytes 3145730
  192.9 1.9 reshape.289
  194.8 3.6 %all-to-all-start = ((bf16[4,2,98304]{2,1,0:T(2,128)(2,1)}), bf16[4,2,98304]{2,1,0:T(2,128)(2,1)S(1)}, u32[]{:S(2)}, u32[]{:S(2)}) async-start(bf16[4,2,98304]{2,1,0:T(2,128)(2,1)} %reshape.289), calls=%async_computation | async-start | bytes 3145728 | tf_op jit(solution)/shard_map/all_to_all | solution.py:85
  198.5 25.8 %psum.7 = f32[384,16]{0,1:T(8,128)S(1)} all-reduce(f32[384,16]{0,1:T(8,128)S(1)} %reshape.262), channel_id=1, replica_groups=mesh['kv'=8,'tp'=4] {'tp'}, use_global_device_ids=true, to_apply=%region_4.5 | all-reduce | flops 6144 | bytes 49152 | tf_op jit(solution)/shard_map/psum | solution.py:88
  224.3 2.8 %reshape.290 = bf16[2048,1,384]{2,1,0:T(2,128)(2,1)} reshape(bf16[4,2,98304]{2,1,0:T(2,128)(2,1)S(1)} %all-to-all-done) | data formatting | bytes 3145728
  227.1 3.8 %copy.51 = f32[1,384,2048]{1,2,0:T(8,128)} copy(bf16[1,384,2048]{1,0,2:T(2,128)(2,1)} %bitcast.68) | data formatting | bytes 4718592
  230.9 2.1 reduce_sum.18
  233.9 20.9 %all-gather.5.cloned.1.call-done = bf16[384,2048]{0,1:T(8,128)(2,1)} async-done(((bf16[384,512]{0,1:T(8,128)(2,1)}), bf16[384,2048]{0,1:T(8,128)(2,1)}) %all-gather.5.cloned.1.call-update) | async-done | bytes 1572880 | tf_op jit(solution)/shard_map/all_gather | solution.py:92
  254.8 3.8 %convolution_convert_fusion = bf16[384,512]{1,0:T(8,128)(2,1)} fusion(bf16[384,2048]{0,1:T(8,128)(2,1)} %all-gather.5.cloned.1.call-done, bf16[2048,512]{1,0:T(8,128)(2,1)} %param.10), kind=kOutput, calls=%fused_computation.16 | convolution fusion | flops 805502976 | bytes 4063232 | tf_op jit(solution)/shard_map/dot_general | solution.py:91
  (52 shorter events, 9.5 us)
Async XLA Ops:
  6.5 1.6 copy-start
  6.5 80.9 %all-gather.3.cloned.1.call-start = ((), (), s32[]{:S(2)}) async-start(), calls=%async_computation.1 | async-start | bytes 1966080 | tf_op jit(solution)/shard_map/all_gather | solution.py:45
  12.2 1.4 copy-start.4
  12.7 1.9 copy-start.6
  50.3 1.9 copy-start.5
  87.4 2.0 copy-start.2
  110.9 17.0 %copy-start.3 = (bf16[6,33,16,2,128]{4,3,2,1,0:T(2,128)(2,1)S(1)}, bf16[6,33,16,2,128]{4,3,2,1,0:T(2,128)(2,1)}, u32[]{:S(2)}) copy-start(bf16[6,33,16,2,128]{4,3,2,1,0:T(2,128)(2,1)} %reshape.256) | copy-start | bytes 4866052
  194.8 29.5 %all-to-all-start = ((bf16[4,2,98304]{2,1,0:T(2,128)(2,1)}), bf16[4,2,98304]{2,1,0:T(2,128)(2,1)S(1)}, u32[]{:S(2)}, u32[]{:S(2)}) async-start(bf16[4,2,98304]{2,1,0:T(2,128)(2,1)} %reshape.289), calls=%async_computation | async-start | bytes 3145728 | tf_op jit(solution)/shard_map/all_to_all | solution.py:85
  198.4 56.4 %all-gather.5.cloned.1.call-start = ((), (), s32[]{:S(2)}) async-start(), calls=%async_computation.2 | async-start | bytes 1966080 | tf_op jit(solution)/shard_map/all_gather | solution.py:92
  233.9 24.7 %copy-start.1 = (bf16[2048,512]{1,0:T(8,128)(2,1)S(1)}, bf16[2048,512]{1,0:T(8,128)(2,1)}, u32[]{:S(2)}) copy-start(bf16[2048,512]{1,0:T(8,128)(2,1)} %param.7) | copy-start | bytes 6291460
Sparse Core Ops, SparseCore 0:
  13.7 22.3 all-gather.2
  234.0 20.7 all-gather.4
where the time goes:
time: 266 us; the launch traced here: 265 us
  blocking collectives  100 us (38%)
  other arithmetic  57.9 us (22%)
  matrix products  35.1 us (13%)
  local copies, waits for them, and re-layouts  34.1 us (13%)
  waiting for transfers between devices  21 us (8%)
  between operations  13.7 us (5%)
  starting transfers between devices  3.61 us (1%)
    unnamed x1, other arithmetic  34.3 us
    all_gather x1, blocking collectives, body(): lax.all_gather(keys, 'kv', axis=0, tiled=True)  32.9 us
    all_gather x1, blocking collectives, body(): lax.all_gather(values, 'kv', axis=0, tiled=True)  31 us
    psum x1, blocking collectives, body(): whole_totals = lax.psum(totals, 'tp')  25.8 us
    all_gather x1, waiting for transfers between devices, body(): lax.all_gather(attention, 'tp', axis=1, tiled=True)  20.9 us
    dot_general x1, matrix products, body(): jnp.einsum('nkgqsr,nsrkd->nqkgd', probs, value_five, preferred_element_ty...  17 us
    reduce_sum x1, other arithmetic, body(): total_local = jnp.sum(weights, axis=(4, 5))  16.9 us
    unnamed x20, local copies, waits for them, and re-layouts  13.3 us
  transfers between devices with their start and end apart: 3, of which 1 were waited for; matrix products, arithmetic and copies ran while one was open for 4% of the time, Pallas kernels for 0%

commit v1 on v0

v1 whole, which is shorter than its diff:
```python
import functools

import jax
import jax.numpy as jnp
import numpy as np
from jax import lax
from jax.experimental import pallas as pl
from jax.experimental.pallas import tpu as pltpu
from jax.sharding import PartitionSpec as P

H = 16
DH = 128
KVH = 2
BLK = 64
NSEL = 32
HALF = DH // 2
THETA = 10000.0
SCALE = DH ** (-0.5)
EXP2_SCALE = SCALE * 1.4426950408889634
MASKED = -1e30
TILE = 4

ANY = pl.BlockSpec(memory_space=pl.ANY)
VMEM = pl.BlockSpec(memory_space=pltpu.VMEM)
SMEM = pl.BlockSpec(memory_space=pltpu.SMEM)


def frequencies():
    inverse = (THETA ** (-np.arange(HALF, dtype=np.float64) / HALF)).astype(np.float32)
    return np.concatenate([inverse, inverse])[None, :]


def turn(values, first_position, inverse):
    rows = values.shape[0]
    position = first_position + lax.broadcasted_iota(jnp.int32, (rows, DH), 0)
    angles = position.astype(jnp.float32) * inverse
    cosine = jnp.cos(angles)
    sine = jnp.sin(angles)
    sine = jnp.where(lax.broadcasted_iota(jnp.int32, (rows, DH), 1) < HALF, -sine, sine)
    heads = []
    for head in range(values.shape[1] // DH):
        own = values[:, head * DH : (head + 1) * DH]
        swapped = pltpu.roll(own, HALF, 1)
        heads.append(own * cosine + swapped * sine)
    return heads


def key_value_kernel(where, tokens, w_key, w_value, inverse, out, slab, keys, values, sems):
    rows = slab.shape[0]
    width = tokens.shape[1]
    row = pl.multiple_of(where[0], 8)
    column = pl.multiple_of(where[1], DH)
    pieces = sems.shape[0]
    step = width // pieces
    copies = []
    for piece in range(pieces):
        part = pl.ds(piece * step, step)
        three = [
            pltpu.make_async_copy(tokens.at[pl.ds(row, rows), part], slab.at[:, part], sems.at[piece, 0]),
            pltpu.make_async_copy(w_key.at[part, pl.ds(column, DH)], keys.at[part], sems.at[piece, 1]),
            pltpu.make_async_copy(w_value.at[part, pl.ds(column, DH)], values.at[part], sems.at[piece, 2]),
        ]
        for copy in three:
            copy.start()
        copies.append(three)
    key = jnp.zeros((rows, DH), jnp.float32)
    value = jnp.zeros((rows, DH), jnp.float32)
    for piece in range(pieces):
        for copy in copies[piece]:
            copy.wait()
        part = pl.ds(piece * step, step)
        left = slab[:, part]
        key += jnp.dot(left, keys[part], preferred_element_type=jnp.float32)
        value += jnp.dot(left, values[part], preferred_element_type=jnp.float32)
    out[:, :DH] = turn(key, where[2], inverse[...])[0].astype(jnp.bfloat16)
    out[:, DH:] = value.astype(jnp.bfloat16)


def query_kernel(where, tokens, w_query, inverse, out):
    product = jnp.dot(tokens[...], w_query[...], preferred_element_type=jnp.float32)
    for head, turned in enumerate(turn(product, where[0], inverse[...])):
        out[:, head * DH : (head + 1) * DH] = turned.astype(jnp.bfloat16)


def attention_kernel(places, valid, own, query, key_value, out, scores):
    blocks = query.shape[0] // BLK
    heads = query.shape[1] // DH
    rows = heads * BLK
    tiles = NSEL // TILE
    lanes = TILE * BLK
    slot_of_lane = lax.broadcasted_iota(jnp.int32, (1, lanes), 1) // BLK
    causal = (lax.broadcasted_iota(jnp.int32, (rows, BLK), 0) % BLK) >= lax.broadcasted_iota(
        jnp.int32, (rows, BLK), 1
    )

    def rows_of(place):
        return pl.ds(pl.multiple_of(place * BLK, BLK), BLK)

    def picked(block, tile, part):
        return jnp.concatenate(
            [key_value[rows_of(places[block, tile * TILE + slot]), part] for slot in range(TILE)], axis=0
        )

    transposed = (((1,), (1,)), ((), ()))
    for block in range(blocks):
        span = pl.ds(block * BLK, BLK)
        mine = jnp.concatenate([query[span, head * DH : (head + 1) * DH] for head in range(heads)], axis=0)
        highest = jnp.full((rows, lanes), MASKED, jnp.float32)
        for tile in range(tiles):
            score = lax.dot_general(
                mine, picked(block, tile, slice(0, DH)), transposed, preferred_element_type=jnp.float32
            )
            bias = jnp.zeros((1, lanes), jnp.float32)
            for slot in range(TILE):
                missing = jnp.where(valid[block, tile * TILE + slot] < 0, MASKED, 0.0)
                bias = jnp.where(slot_of_lane == slot, missing, bias)
            score = score + bias
            scores[tile] = score
            highest = jnp.maximum(highest, score)
        diagonal = lax.dot_general(
            mine, key_value[rows_of(own[block]), :DH], transposed, preferred_element_type=jnp.float32
        )
        diagonal = jnp.where(causal, diagonal, MASKED)
        top = jnp.maximum(
            jnp.max(highest, axis=1, keepdims=True), jnp.max(diagonal, axis=1, keepdims=True)
        )
        ones = jnp.ones((lanes, DH), jnp.bfloat16)
        probs = jnp.exp2((diagonal - top) * EXP2_SCALE).astype(jnp.bfloat16)
        values = jnp.concatenate([key_value[rows_of(own[block]), DH:], ones[:BLK]], axis=1)
        summed = jnp.dot(probs, values, preferred_element_type=jnp.float32)
        for tile in range(tiles):
            probs = jnp.exp2((scores[tile] - top) * EXP2_SCALE).astype(jnp.bfloat16)
            values = jnp.concatenate([picked(block, tile, slice(DH, 2 * DH)), ones], axis=1)
            summed += jnp.dot(probs, values, preferred_element_type=jnp.float32)
        attention = (summed[:, :DH] / summed[:, DH:]).astype(jnp.bfloat16)
        for head in range(heads):
            out[span, head * DH : (head + 1) * DH] = attention[head * BLK : (head + 1) * BLK]


def project_kernel(order, *refs):
    pieces = refs[:-2]
    w_out, out = refs[-2:]
    depth = pieces[0].shape[1]
    total = None
    for index, piece in enumerate(pieces):
        rows = pl.ds(pl.multiple_of(order[index] * depth, depth), depth)
        product = jnp.dot(piece[...], w_out[rows], preferred_element_type=jnp.float32)
        total = product if total is None else total + product
    out[...] = total.astype(jnp.bfloat16)


def spread_small(own, kv_count, tp_count, depth):
    fast = 2
    slow = kv_count // fast
    by_slow = [own]
    for step in range(1, slow):
        pairs = [(i, i + step * fast) for i in range(kv_count - step * fast)]
        by_slow.append(lax.ppermute(own, "kv", pairs))
    both = []
    for piece in by_slow:
        both.append((piece, lax.ppermute(piece, "kv", [(i, i ^ 1) for i in range(kv_count)])))
    everything = []
    for pair in both:
        for piece in pair:
            everything.append(piece)
            everything.append(lax.ppermute(piece, "tp", [(i, i ^ 1) for i in range(tp_count)]))
    return jnp.concatenate(everything, axis=0)


def body(tokens, w_query, w_key, w_value, w_out, chosen):
    rows, width = tokens.shape
    tp_count = lax.axis_size("tp")
    kv_count = lax.axis_size("kv")
    tp_index = lax.axis_index("tp")
    kv_index = lax.axis_index("kv")
    local_blocks = rows // BLK
    own_heads = w_query.shape[1] // DH
    own_width = own_heads * DH
    sharing = tp_count // KVH
    member = tp_index % sharing
    key_head = tp_index // sharing
    part_rows = rows // sharing
    inverse = jnp.asarray(frequencies())
    first = kv_index * rows

    where = jnp.stack([member * part_rows, key_head * DH, first + member * part_rows]).astype(jnp.int32)
    own_part = pl.pallas_call(
        key_value_kernel,
        out_shape=jax.ShapeDtypeStruct((part_rows, 2 * DH), jnp.bfloat16),
        in_specs=[SMEM, ANY, ANY, ANY, VMEM],
        out_specs=VMEM,
        scratch_shapes=[
            pltpu.VMEM((part_rows, width), jnp.bfloat16),
            pltpu.VMEM((width, DH), jnp.bfloat16),
            pltpu.VMEM((width, DH), jnp.bfloat16),
            pltpu.SemaphoreType.DMA((4, 3)),
        ],
        cost_estimate=pl.CostEstimate(
            flops=4 * part_rows * width * DH, bytes_accessed=2 * width * (part_rows + 2 * DH), transcendentals=0
        ),
        name="key_value",
    )(where, tokens, w_key, w_value, inverse)

    query = pl.pallas_call(
        query_kernel,
        out_shape=jax.ShapeDtypeStruct((rows, own_width), jnp.bfloat16),
        in_specs=[SMEM, VMEM, VMEM, VMEM],
        out_specs=VMEM,
        cost_estimate=pl.CostEstimate(
            flops=2 * rows * width * own_width, bytes_accessed=2 * width * (rows + own_width), transcendentals=0
        ),
        name="query",
    )(jnp.stack([first]).astype(jnp.int32), tokens, w_query, inverse)

    safe = jnp.maximum(chosen, 0)
    mine = kv_index * local_blocks + jnp.arange(local_blocks, dtype=jnp.int32)
    small = kv_count == 8 and tp_count == 4
    if small:
        key_value = spread_small(own_part, kv_count, tp_count, 0)
        held = local_blocks // sharing

        def place_of(block):
            source = block // local_blocks
            inside = block % local_blocks
            steps = kv_index // 2 - source // 2
            across = (kv_index % 2) ^ (source % 2)
            sibling = member ^ (inside // held)
            return ((steps * 2 + across) * 2 + sibling) * held + inside % held

    else:
        groups = [[g * sharing + i for i in range(sharing)] for g in range(KVH)]
        whole = lax.all_gather(own_part, "tp", axis=0, tiled=True, axis_index_groups=groups)
        key_value = lax.all_gather(whole, "kv", axis=0, tiled=True)

        def place_of(block):
            return block

    places = place_of(safe)
    own_places = place_of(mine)

    splits = 3 if local_blocks % 3 == 0 else 1
    per = local_blocks // splits
    outs = []
    for split in range(splits):
        take = slice(split * per, (split + 1) * per)
        span = slice(split * per * BLK, (split + 1) * per * BLK)
        attention = pl.pallas_call(
            attention_kernel,
            out_shape=jax.ShapeDtypeStruct((per * BLK, own_width), jnp.bfloat16),
            in_specs=[SMEM, SMEM, SMEM, VMEM, VMEM],
            out_specs=VMEM,
            scratch_shapes=[pltpu.VMEM((NSEL // TILE, own_heads * BLK, TILE * BLK), jnp.float32)],
            cost_estimate=pl.CostEstimate(
                flops=4 * per * BLK * own_width * (NSEL + 1) * BLK,
                bytes_accessed=4 * DH * key_value.shape[0],
                transcendentals=per * BLK * own_heads * (NSEL + 1) * BLK,
            ),
            name="attention",
        )(places[take], chosen[take], own_places[take], query[span], key_value)
        if small:
            sibling = lax.ppermute(attention, "tp", [(i, i ^ 1) for i in range(tp_count)])
            across = lax.ppermute(attention, "tp", [(i, i ^ 2) for i in range(tp_count)])
            far = lax.ppermute(across, "tp", [(i, i ^ 1) for i in range(tp_count)])
            pieces = [attention, sibling, across, far]
            order = tp_index ^ jnp.arange(tp_count, dtype=jnp.int32)
        else:
            pieces = [lax.all_gather(attention, "tp", axis=1, tiled=True)]
            order = jnp.zeros((1,), jnp.int32)
        outs.append(
            pl.pallas_call(
                project_kernel,
                out_shape=jax.ShapeDtypeStruct((per * BLK, w_out.shape[1]), jnp.bfloat16),
                in_specs=[SMEM] + [VMEM] * len(pieces) + [VMEM],
                out_specs=VMEM,
                cost_estimate=pl.CostEstimate(
                    flops=2 * per * BLK * H * DH * w_out.shape[1],
                    bytes_accessed=2 * H * DH * w_out.shape[1],
                    transcendentals=0,
                ),
                name="project",
            )(order, *pieces, w_out)
        )
    return jnp.concatenate(outs, axis=0)


def solution(mesh):
    placed = (P("kv", None), P(None, "tp"), P(), P(), P(None, "tp"), P("kv", None))
    return jax.shard_map(body, mesh=mesh, in_specs=placed, out_specs=P("kv", "tp"), check_vma=False)
```

time: 266 us -> 72.9 us (0.27)
  blocking collectives: 100 us -> 0 us
  other arithmetic: 57.9 us -> 2.9 us
  matrix products: 35.1 us -> 0 us
  Pallas kernels: 0 us -> 30.8 us
  local copies, waits for them, and re-layouts: 34.1 us -> 7.64 us
  starting transfers between devices: 3.61 us -> 20.4 us
  between operations: 13.7 us -> 0.33 us
  waiting for transfers between devices: 21 us -> 10.3 us
    all_gather x2 -> x0, blocking collectives: 63.9 us -> none  [the longest x1 32.9 us: body(): lax.all_gather(keys, 'kv', axis=0, tiled=True)]
    dot_general x6 -> x0, matrix products: 35.1 us -> none  [the longest x1 17 us: body(): jnp.einsum('nkgqsr,nsrkd->nqkgd', probs, value_five, preferred_element_ty...]
    unnamed x1 -> x0, other arithmetic: 34.3 us -> none
    pallas_call x0 -> x8, Pallas kernels: none -> 30.8 us  [the longest x3 13.5 us: body(): pl.pallas_call(attention_kernel, out_shape=jax.ShapeDtypeStruct((per * BL...]
    psum x1 -> x0, blocking collectives: 25.8 us -> none  [body(): whole_totals = lax.psum(totals, 'tp')]
    all_gather x2 -> x0, waiting for transfers between devices: 20.9 us -> none  [the longest x1 20.9 us: body(): lax.all_gather(attention, 'tp', axis=1, tiled=True)]
    ppermute x0 -> x24, starting transfers between devices: none -> 20.4 us  [the longest x3 9.27 us: spread_small(): by_slow.append(lax.ppermute(own, 'kv', pairs))]
    reduce_sum x2 -> x0, other arithmetic: 19.1 us -> none  [the longest x1 16.9 us: body(): total_local = jnp.sum(weights, axis=(4, 5))]
  transfers between devices with their start and end apart: 3 -> 24, of which waited for: 1 -> 5; matrix products, arithmetic and copies ran while one was open for 4% -> 5% of each run, Pallas kernels for 0% -> 27%
where the time goes in v1:
time: 72.9 us; the launch traced here: 72.5 us
  Pallas kernels  30.8 us (42%)
  starting transfers between devices  20.4 us (28%)
  waiting for transfers between devices  10.3 us (14%)
  local copies, waits for them, and re-layouts  7.64 us (10%)
  other arithmetic  2.9 us (4%)
    pallas_call x3, Pallas kernels, body(): pl.pallas_call(attention_kernel, out_shape=jax.ShapeDtypeStruct((per * BL...  13.5 us
    ppermute x3, starting transfers between devices, spread_small(): by_slow.append(lax.ppermute(own, 'kv', pairs))  9.27 us
    pallas_call x3, Pallas kernels, body(): pl.pallas_call(project_kernel, out_shape=jax.ShapeDtypeStruct((per * BLK,...  8.94 us
    ppermute x4, waiting for transfers between devices, spread_small(): lax.ppermute(piece, 'kv', [(i, i ^ 1) for i in range(kv_count)])  5.89 us
    ppermute x4, starting transfers between devices, spread_small(): lax.ppermute(piece, 'kv', [(i, i ^ 1) for i in range(kv_count)])  5.42 us
    unnamed x45, local copies, waits for them, and re-layouts  4.56 us
    pallas_call x1, Pallas kernels, body(): pl.pallas_call(query_kernel, out_shape=jax.ShapeDtypeStruct((rows, own_wi...  4.47 us
    pallas_call x1, Pallas kernels, body(): pl.pallas_call(key_value_kernel, out_shape=jax.ShapeDtypeStruct((part_row...  3.91 us
  transfers between devices with their start and end apart: 24, of which 5 were waited for; matrix products, arithmetic and copies ran while one was open for 5% of the time, Pallas kernels for 27%

profile of v1, /device:TPU:0, one launch (start us, length us, event | category | flops | bytes accessed | tf_op | source)
XLA Modules:
  0.0 72.5 jit_solution(3410031917946854453)
XLA Ops:
  0.6 3.9 %key_value.1 = bf16[192,256]{1,0:T(8,128)(2,1)} custom-call(s32[3]{0:T(128)} %pad_add_fusion.where, bf16[384,2048]{1,0:T(8,128)(2,1)} %tokens.3, bf16[2048,256]{1,0:T(8,128)(2,1)} %w_key.1, bf16[2048,256]{1,0:T(8,128)(2,1)} %w_value.1, f32[1,128]{1,0:T(1,128)} %constant.131.clone.inverse), custom_call_target="tpu_custom_call" | custom-call | flops 201326592 | bytes 1835008 | tf_op jit(solution)/shard_map/key_value/pallas_call | solution.py:187
  5.1 2.6 %collective-permute-start.1 = (bf16[192,256]{1,0:T(8,128)(2,1)}, bf16[192,256]{1,0:T(8,128)(2,1)S(1)}, u32[]{:S(2)}, u32[]{:S(2)}) collective-permute-start(bf16[192,256]{1,0:T(8,128)(2,1)} %key_value.1), channel_id=1, source_target_pairs={{0,4},{4,0},{8,12},{12,8},{16,20},{20,16},{24,28},{28,24},{1,5},{5... | collective-permute-start | bytes 294920 | tf_op jit(solution)/shard_map/ppermute | solution.py:161
  7.7 3.5 %collective-permute-start.3 = (bf16[192,256]{1,0:T(8,128)(2,1)}, bf16[192,256]{1,0:T(8,128)(2,1)S(1)}, u32[]{:S(2)}, u32[]{:S(2)}) collective-permute-start(bf16[192,256]{1,0:T(8,128)(2,1)} %key_value.1), channel_id=1, source_target_pairs={{0,8},{4,12},{8,16},{12,20},{16,24},{20,28},{1,9},{5,13},{9,17},{1... | collective-permute-start | bytes 294920 | tf_op jit(solution)/shard_map/ppermute | solution.py:158
  11.2 4.5 %collective-permute-start.7 = (bf16[192,256]{1,0:T(8,128)(2,1)}, bf16[192,256]{1,0:T(8,128)(2,1)S(1)}, u32[]{:S(2)}, u32[]{:S(2)}) collective-permute-start(bf16[192,256]{1,0:T(8,128)(2,1)} %key_value.1), channel_id=1, source_target_pairs={{0,16},{4,20},{8,24},{12,28},{1,17},{5,21},{9,25},{13,29},{2,18},{... | collective-permute-start | bytes 294920 | tf_op jit(solution)/shard_map/ppermute | solution.py:158
  15.7 1.3 %collective-permute-start.11 = (bf16[192,256]{1,0:T(8,128)(2,1)}, bf16[192,256]{1,0:T(8,128)(2,1)S(1)}, u32[]{:S(2)}, u32[]{:S(2)}) collective-permute-start(bf16[192,256]{1,0:T(8,128)(2,1)} %key_value.1), channel_id=1, source_target_pairs={{0,24},{4,28},{1,25},{5,29},{2,26},{6,30},{3,27},{7,31}} | collective-permute-start | bytes 294920 | tf_op jit(solution)/shard_map/ppermute | solution.py:158
  18.3 4.5 %query.1 = bf16[384,512]{1,0:T(8,128)(2,1)} custom-call(s32[1]{0:T(128)} %bitcast.where, bf16[384,2048]{1,0:T(8,128)(2,1)} %tokens.3, bf16[2048,512]{1,0:T(8,128)(2,1)} %w_query.1, f32[1,128]{1,0:T(1,128)} %constant.131.clone.inverse), custom_call_target="tpu_custom_call" | custom-call | flops 805306368 | bytes 3670016 | tf_op jit(solution)/shard_map/query/pallas_call | solution.py:204
  22.8 1.8 %fusion.18 = (bf16[128,512]{1,0:T(8,128)(2,1)}, bf16[128,512]{1,0:T(8,128)(2,1)}, bf16[128,512]{1,0:T(8,128)(2,1)}) fusion(bf16[384,512]{1,0:T(8,128)(2,1)} %query.1), kind=kLoop, calls=%fused_computation.60 | loop fusion | bytes 786432 | tf_op jit(solution)/shard_map/slice | solution.py:259
  25.8 1.6 %collective-permute-start.9 = (bf16[192,256]{1,0:T(8,128)(2,1)S(1)}, bf16[192,256]{1,0:T(8,128)(2,1)S(1)}, u32[]{:S(2)}, u32[]{:S(2)}) collective-permute-start(bf16[192,256]{1,0:T(8,128)(2,1)S(1)} %collective-permute-done.7), channel_id=1, source_target_pairs={{0,4},{4,0},{8,12},{12,8},{16,20},{20,16},{24,28},{28,24},{1,5},{5... | collective-permute-start | bytes 294920 | tf_op jit(solution)/shard_map/ppermute | solution.py:161
  27.4 0.7 collective-permute-start.13
  28.2 2.2 %collective-permute-done.5 = bf16[192,256]{1,0:T(8,128)(2,1)S(1)} collective-permute-done((bf16[192,256]{1,0:T(8,128)(2,1)S(1)}, bf16[192,256]{1,0:T(8,128)(2,1)S(1)}, u32[]{:S(2)}, u32[]{:S(2)}) %collective-permute-start.5) | collective-permute-done | bytes 98336 | tf_op jit(solution)/shard_map/ppermute | solution.py:161
  30.4 2.1 %collective-permute-done.9 = bf16[192,256]{1,0:T(8,128)(2,1)S(1)} collective-permute-done((bf16[192,256]{1,0:T(8,128)(2,1)S(1)}, bf16[192,256]{1,0:T(8,128)(2,1)S(1)}, u32[]{:S(2)}, u32[]{:S(2)}) %collective-permute-start.9) | collective-permute-done | bytes 98336 | tf_op jit(solution)/shard_map/ppermute | solution.py:161
  32.6 1.6 %collective-permute-done.13 = bf16[192,256]{1,0:T(8,128)(2,1)S(1)} collective-permute-done((bf16[192,256]{1,0:T(8,128)(2,1)S(1)}, bf16[192,256]{1,0:T(8,128)(2,1)S(1)}, u32[]{:S(2)}, u32[]{:S(2)}) %collective-permute-start.13) | collective-permute-done | bytes 98336 | tf_op jit(solution)/shard_map/ppermute | solution.py:161
  34.3 1.1 %collective-permute-done.14 = bf16[192,256]{1,0:T(8,128)(2,1)S(1)} collective-permute-done((bf16[192,256]{1,0:T(8,128)(2,1)S(1)}, bf16[192,256]{1,0:T(8,128)(2,1)S(1)}, u32[]{:S(2)}, u32[]{:S(2)}) %collective-permute-start.14) | collective-permute-done | bytes 98336 | tf_op jit(solution)/shard_map/ppermute | solution.py:166
  35.4 1.2 %copy-done.14 = bf16[3072,256]{1,0:T(8,128)(2,1)} copy-done((bf16[3072,256]{1,0:T(8,128)(2,1)}, bf16[3072,256]{1,0:T(8,128)(2,1)S(1)}, u32[]{:S(2)}) %copy-start.14) | copy-done | bytes 1572888
  36.6 4.5 %attention.3.refs_0_ = bf16[128,512]{1,0:T(8,128)(2,1)} custom-call(s32[2,32]{1,0:T(2,128)} %get-tuple-element.19.places, s32[2,32]{1,0:T(2,128)} %get-tuple-element.8.valid, s32[2]{0:T(128)} %get-tuple-element.14.own, bf16[128,512]{1,0:T(8,128)(2,1)} %get-tuple-element.5.query, bf16[3072,256]{1,0:T(8,128)(2,1)} %copy-done.14), custom_call_target="tpu_custom_call" | custom-call | flops 553648128 | bytes 1572864 | tf_op jit(solution)/shard_map/attention/pallas_call | solution.py:247
  41.1 1.5 %collective-permute-start.16 = (bf16[128,512]{1,0:T(8,128)(2,1)}, bf16[128,512]{1,0:T(8,128)(2,1)S(1)}, u32[]{:S(2)}, u32[]{:S(2)}) collective-permute-start(bf16[128,512]{1,0:T(8,128)(2,1)} %attention.3.refs_0_), channel_id=1, source_target_pairs={{0,2},{1,3},{2,0},{3,1},{4,6},{5,7},{6,4},{7,5},{8,10},{9,11},{10,... | collective-permute-start | bytes 393224 | tf_op jit(solution)/shard_map/ppermute | solution.py:262
  42.6 4.5 %attention.4.refs_0_ = bf16[128,512]{1,0:T(8,128)(2,1)} custom-call(s32[2,32]{1,0:T(2,128)} %get-tuple-element.17.places, s32[2,32]{1,0:T(2,128)} %get-tuple-element.10.valid, s32[2]{0:T(128)} %get-tuple-element.16.own, bf16[128,512]{1,0:T(8,128)(2,1)} %get-tuple-element.7.query, bf16[3072,256]{1,0:T(8,128)(2,1)} %copy-done.14), custom_call_target="tpu_custom_call" | custom-call | flops 553648128 | bytes 1572864 | tf_op jit(solution)/shard_map/attention/pallas_call | solution.py:247
  47.6 4.5 %attention.5.refs_0_ = bf16[128,512]{1,0:T(8,128)(2,1)} custom-call(s32[2,32]{1,0:T(2,128)} %get-tuple-element.18.places, s32[2,32]{1,0:T(2,128)} %get-tuple-element.9.valid, s32[2]{0:T(128)} %get-tuple-element.15.own, bf16[128,512]{1,0:T(8,128)(2,1)} %get-tuple-element.6.query, bf16[3072,256]{1,0:T(8,128)(2,1)} %copy-done.14), custom_call_target="tpu_custom_call" | custom-call | flops 553648128 | bytes 1572864 | tf_op jit(solution)/shard_map/attention/pallas_call | solution.py:247
  52.1 1.5 %collective-permute-start.22 = (bf16[128,512]{1,0:T(8,128)(2,1)}, bf16[128,512]{1,0:T(8,128)(2,1)S(1)}, u32[]{:S(2)}, u32[]{:S(2)}) collective-permute-start(bf16[128,512]{1,0:T(8,128)(2,1)} %attention.5.refs_0_), channel_id=1, source_target_pairs={{0,2},{1,3},{2,0},{3,1},{4,6},{5,7},{6,4},{7,5},{8,10},{9,11},{10,... | collective-permute-start | bytes 393224 | tf_op jit(solution)/shard_map/ppermute | solution.py:262
  54.7 3.3 %collective-permute-done.22.refs_2_ = bf16[128,512]{1,0:T(8,128)(2,1)S(1)} collective-permute-done((bf16[128,512]{1,0:T(8,128)(2,1)}, bf16[128,512]{1,0:T(8,128)(2,1)S(1)}, u32[]{:S(2)}, u32[]{:S(2)}) %collective-permute-start.22) | collective-permute-done | bytes 131104 | tf_op jit(solution)/shard_map/ppermute | solution.py:262
  59.2 3.0 %project.3 = bf16[128,512]{1,0:T(8,128)(2,1)} custom-call(s32[4]{0:T(128)} %iota_xor_fusion.order, bf16[128,512]{1,0:T(8,128)(2,1)} %attention.3.refs_0_, bf16[128,512]{1,0:T(8,128)(2,1)} %copy-done.6, bf16[128,512]{1,0:T(8,128)(2,1)} %copy-done.4, bf16[128,512]{1,0:T(8,128)(2,1)} %copy-done.10, bf16[2048,512]{1,0:T(8,128)(2,1)} %refs_4_.5), custom_call_target="tpu_custom_call" | custom-call | flops 268435456 | bytes 2097152 | tf_op jit(solution)/shard_map/project/pallas_call | solution.py:270
  63.5 3.0 %project.4 = bf16[128,512]{1,0:T(8,128)(2,1)} custom-call(s32[4]{0:T(128)} %iota_xor_fusion.order, bf16[128,512]{1,0:T(8,128)(2,1)} %attention.4.refs_0_, bf16[128,512]{1,0:T(8,128)(2,1)} %copy-done.9, bf16[128,512]{1,0:T(8,128)(2,1)} %copy-done.5, bf16[128,512]{1,0:T(8,128)(2,1)} %copy-done.12, bf16[2048,512]{1,0:T(8,128)(2,1)} %refs_4_.5), custom_call_target="tpu_custom_call" | custom-call | flops 268435456 | bytes 2097152 | tf_op jit(solution)/shard_map/project/pallas_call | solution.py:270
  67.8 3.0 %project.5 = bf16[128,512]{1,0:T(8,128)(2,1)} custom-call(s32[4]{0:T(128)} %iota_xor_fusion.order, bf16[128,512]{1,0:T(8,128)(2,1)} %attention.5.refs_0_, bf16[128,512]{1,0:T(8,128)(2,1)} %copy-done.8, bf16[128,512]{1,0:T(8,128)(2,1)} %copy-done.7, bf16[128,512]{1,0:T(8,128)(2,1)} %copy-done.11, bf16[2048,512]{1,0:T(8,128)(2,1)} %refs_4_.5), custom_call_target="tpu_custom_call" | custom-call | flops 268435456 | bytes 2097152 | tf_op jit(solution)/shard_map/project/pallas_call | solution.py:270
  70.8 1.7 %pad_maximum_fusion = bf16[384,512]{1,0:T(8,128)(2,1)} fusion(bf16[128,512]{1,0:T(8,128)(2,1)} %project.5, bf16[128,512]{1,0:T(8,128)(2,1)S(1)} %copy-done.1, bf16[128,512]{1,0:T(8,128)(2,1)S(1)} %copy-done), kind=kLoop, calls=%fused_computation | loop fusion | flops 1179648 | bytes 786432 | tf_op jit(solution)/shard_map/concatenate | solution.py:283
  (86 shorter events, 9.3 us)
Async XLA Ops:
  4.5 20.2 %collective-permute-start = (bf16[192,256]{1,0:T(8,128)(2,1)}, bf16[192,256]{1,0:T(8,128)(2,1)S(1)}, u32[]{:S(2)}, u32[]{:S(2)}) collective-permute-start(bf16[192,256]{1,0:T(8,128)(2,1)} %key_value.1), channel_id=1, source_target_pairs={{0,1},{1,0},{2,3},{3,2},{4,5},{5,4},{6,7},{7,6},{8,9},{9,8},{10,11... | collective-permute-start | bytes 294920 | tf_op jit(solution)/shard_map/ppermute | solution.py:166
  5.1 20.2 %collective-permute-start.1 = (bf16[192,256]{1,0:T(8,128)(2,1)}, bf16[192,256]{1,0:T(8,128)(2,1)S(1)}, u32[]{:S(2)}, u32[]{:S(2)}) collective-permute-start(bf16[192,256]{1,0:T(8,128)(2,1)} %key_value.1), channel_id=1, source_target_pairs={{0,4},{4,0},{8,12},{12,8},{16,20},{20,16},{24,28},{28,24},{1,5},{5... | collective-permute-start | bytes 294920 | tf_op jit(solution)/shard_map/ppermute | solution.py:161
  7.7 16.9 %collective-permute-start.3 = (bf16[192,256]{1,0:T(8,128)(2,1)}, bf16[192,256]{1,0:T(8,128)(2,1)S(1)}, u32[]{:S(2)}, u32[]{:S(2)}) collective-permute-start(bf16[192,256]{1,0:T(8,128)(2,1)} %key_value.1), channel_id=1, source_target_pairs={{0,8},{4,12},{8,16},{12,20},{16,24},{20,28},{1,9},{5,13},{9,17},{1... | collective-permute-start | bytes 294920 | tf_op jit(solution)/shard_map/ppermute | solution.py:158
  11.2 14.3 %collective-permute-start.7 = (bf16[192,256]{1,0:T(8,128)(2,1)}, bf16[192,256]{1,0:T(8,128)(2,1)S(1)}, u32[]{:S(2)}, u32[]{:S(2)}) collective-permute-start(bf16[192,256]{1,0:T(8,128)(2,1)} %key_value.1), channel_id=1, source_target_pairs={{0,16},{4,20},{8,24},{12,28},{1,17},{5,21},{9,25},{13,29},{2,18},{... | collective-permute-start | bytes 294920 | tf_op jit(solution)/shard_map/ppermute | solution.py:158
  15.7 10.2 %collective-permute-start.11 = (bf16[192,256]{1,0:T(8,128)(2,1)}, bf16[192,256]{1,0:T(8,128)(2,1)S(1)}, u32[]{:S(2)}, u32[]{:S(2)}) collective-permute-start(bf16[192,256]{1,0:T(8,128)(2,1)} %key_value.1), channel_id=1, source_target_pairs={{0,24},{4,28},{1,25},{5,29},{2,26},{6,30},{3,27},{7,31}} | collective-permute-start | bytes 294920 | tf_op jit(solution)/shard_map/ppermute | solution.py:158
  24.6 3.5 %collective-permute-start.4 = (bf16[192,256]{1,0:T(8,128)(2,1)S(1)}, bf16[192,256]{1,0:T(8,128)(2,1)S(1)}, u32[]{:S(2)}, u32[]{:S(2)}) collective-permute-start(bf16[192,256]{1,0:T(8,128)(2,1)S(1)} %collective-permute-done.3), channel_id=1, source_target_pairs={{0,1},{1,0},{2,3},{3,2},{4,5},{5,4},{6,7},{7,6},{8,9},{9,8},{10,11... | collective-permute-start | bytes 294920 | tf_op jit(solution)/shard_map/ppermute | solution.py:166
  24.7 5.7 %collective-permute-start.5 = (bf16[192,256]{1,0:T(8,128)(2,1)S(1)}, bf16[192,256]{1,0:T(8,128)(2,1)S(1)}, u32[]{:S(2)}, u32[]{:S(2)}) collective-permute-start(bf16[192,256]{1,0:T(8,128)(2,1)S(1)} %collective-permute-done.3), channel_id=1, source_target_pairs={{0,4},{4,0},{8,12},{12,8},{16,20},{20,16},{24,28},{28,24},{1,5},{5... | collective-permute-start | bytes 294920 | tf_op jit(solution)/shard_map/ppermute | solution.py:161
  25.3 2.1 %collective-permute-start.2 = (bf16[192,256]{1,0:T(8,128)(2,1)S(1)}, bf16[192,256]{1,0:T(8,128)(2,1)S(1)}, u32[]{:S(2)}, u32[]{:S(2)}) collective-permute-start(bf16[192,256]{1,0:T(8,128)(2,1)S(1)} %collective-permute-done.1), channel_id=1, source_target_pairs={{0,1},{1,0},{2,3},{3,2},{4,5},{5,4},{6,7},{7,6},{8,9},{9,8},{10,11... | collective-permute-start | bytes 294920 | tf_op jit(solution)/shard_map/ppermute | solution.py:166
  25.4 8.8 %collective-permute-start.8 = (bf16[192,256]{1,0:T(8,128)(2,1)S(1)}, bf16[192,256]{1,0:T(8,128)(2,1)S(1)}, u32[]{:S(2)}, u32[]{:S(2)}) collective-permute-start(bf16[192,256]{1,0:T(8,128)(2,1)S(1)} %collective-permute-done.7), channel_id=1, source_target_pairs={{0,1},{1,0},{2,3},{3,2},{4,5},{5,4},{6,7},{7,6},{8,9},{9,8},{10,11... | collective-permute-start | bytes 294920 | tf_op jit(solution)/shard_map/ppermute | solution.py:166
  25.8 6.7 %collective-permute-start.9 = (bf16[192,256]{1,0:T(8,128)(2,1)S(1)}, bf16[192,256]{1,0:T(8,128)(2,1)S(1)}, u32[]{:S(2)}, u32[]{:S(2)}) collective-permute-start(bf16[192,256]{1,0:T(8,128)(2,1)S(1)} %collective-permute-done.7), channel_id=1, source_target_pairs={{0,4},{4,0},{8,12},{12,8},{16,20},{20,16},{24,28},{28,24},{1,5},{5... | collective-permute-start | bytes 294920 | tf_op jit(solution)/shard_map/ppermute | solution.py:161
  27.4 6.7 %collective-permute-start.13 = (bf16[192,256]{1,0:T(8,128)(2,1)S(1)}, bf16[192,256]{1,0:T(8,128)(2,1)S(1)}, u32[]{:S(2)}, u32[]{:S(2)}) collective-permute-start(bf16[192,256]{1,0:T(8,128)(2,1)S(1)} %collective-permute-done.11), channel_id=1, source_target_pairs={{0,4},{4,0},{8,12},{12,8},{16,20},{20,16},{24,28},{28,24},{1,5},{5... | collective-permute-start | bytes 294920 | tf_op jit(solution)/shard_map/ppermute | solution.py:161
  28.1 6.1 %collective-permute-start.12 = (bf16[192,256]{1,0:T(8,128)(2,1)S(1)}, bf16[192,256]{1,0:T(8,128)(2,1)S(1)}, u32[]{:S(2)}, u32[]{:S(2)}) collective-permute-start(bf16[192,256]{1,0:T(8,128)(2,1)S(1)} %collective-permute-done.11), channel_id=1, source_target_pairs={{0,1},{1,0},{2,3},{3,2},{4,5},{5,4},{6,7},{7,6},{8,9},{9,8},{10,11... | collective-permute-start | bytes 294920 | tf_op jit(solution)/shard_map/ppermute | solution.py:166
  30.4 3.7 %collective-permute-start.6 = (bf16[192,256]{1,0:T(8,128)(2,1)S(1)}, bf16[192,256]{1,0:T(8,128)(2,1)S(1)}, u32[]{:S(2)}, u32[]{:S(2)}) collective-permute-start(bf16[192,256]{1,0:T(8,128)(2,1)S(1)} %collective-permute-done.5), channel_id=1, source_target_pairs={{0,1},{1,0},{2,3},{3,2},{4,5},{5,4},{6,7},{7,6},{8,9},{9,8},{10,11... | collective-permute-start | bytes 294920 | tf_op jit(solution)/shard_map/ppermute | solution.py:166
  32.5 1.7 %collective-permute-start.10 = (bf16[192,256]{1,0:T(8,128)(2,1)S(1)}, bf16[192,256]{1,0:T(8,128)(2,1)S(1)}, u32[]{:S(2)}, u32[]{:S(2)}) collective-permute-start(bf16[192,256]{1,0:T(8,128)(2,1)S(1)} %collective-permute-done.9), channel_id=1, source_target_pairs={{0,1},{1,0},{2,3},{3,2},{4,5},{5,4},{6,7},{7,6},{8,9},{9,8},{10,11... | collective-permute-start | bytes 294920 | tf_op jit(solution)/shard_map/ppermute | solution.py:166
  34.1 1.3 %collective-permute-start.14 = (bf16[192,256]{1,0:T(8,128)(2,1)S(1)}, bf16[192,256]{1,0:T(8,128)(2,1)S(1)}, u32[]{:S(2)}, u32[]{:S(2)}) collective-permute-start(bf16[192,256]{1,0:T(8,128)(2,1)S(1)} %collective-permute-done.13), channel_id=1, source_target_pairs={{0,1},{1,0},{2,3},{3,2},{4,5},{5,4},{6,7},{7,6},{8,9},{9,8},{10,11... | collective-permute-start | bytes 294920 | tf_op jit(solution)/shard_map/ppermute | solution.py:166
  41.1 12.5 %collective-permute-start.16 = (bf16[128,512]{1,0:T(8,128)(2,1)}, bf16[128,512]{1,0:T(8,128)(2,1)S(1)}, u32[]{:S(2)}, u32[]{:S(2)}) collective-permute-start(bf16[128,512]{1,0:T(8,128)(2,1)} %attention.3.refs_0_), channel_id=1, source_target_pairs={{0,2},{1,3},{2,0},{3,1},{4,6},{5,7},{6,4},{7,5},{8,10},{9,11},{10,... | collective-permute-start | bytes 393224 | tf_op jit(solution)/shard_map/ppermute | solution.py:262
  42.6 11.6 %collective-permute-start.15 = (bf16[128,512]{1,0:T(8,128)(2,1)}, bf16[128,512]{1,0:T(8,128)(2,1)S(1)}, u32[]{:S(2)}, u32[]{:S(2)}) collective-permute-start(bf16[128,512]{1,0:T(8,128)(2,1)} %attention.3.refs_0_), channel_id=1, source_target_pairs={{0,1},{1,0},{2,3},{3,2},{4,5},{5,4},{6,7},{7,6},{8,9},{9,8},{10,11... | collective-permute-start | bytes 393224 | tf_op jit(solution)/shard_map/ppermute | solution.py:261
  47.1 7.1 %collective-permute-start.19 = (bf16[128,512]{1,0:T(8,128)(2,1)}, bf16[128,512]{1,0:T(8,128)(2,1)S(1)}, u32[]{:S(2)}, u32[]{:S(2)}) collective-permute-start(bf16[128,512]{1,0:T(8,128)(2,1)} %attention.4.refs_0_), channel_id=1, source_target_pairs={{0,2},{1,3},{2,0},{3,1},{4,6},{5,7},{6,4},{7,5},{8,10},{9,11},{10,... | collective-permute-start | bytes 393224 | tf_op jit(solution)/shard_map/ppermute | solution.py:262
  52.1 5.8 %collective-permute-start.22 = (bf16[128,512]{1,0:T(8,128)(2,1)}, bf16[128,512]{1,0:T(8,128)(2,1)S(1)}, u32[]{:S(2)}, u32[]{:S(2)}) collective-permute-start(bf16[128,512]{1,0:T(8,128)(2,1)} %attention.5.refs_0_), channel_id=1, source_target_pairs={{0,2},{1,3},{2,0},{3,1},{4,6},{5,7},{6,4},{7,5},{8,10},{9,11},{10,... | collective-permute-start | bytes 393224 | tf_op jit(solution)/shard_map/ppermute | solution.py:262
  53.6 4.9 %collective-permute-start.17 = (bf16[128,512]{1,0:T(8,128)(2,1)S(1)}, bf16[128,512]{1,0:T(8,128)(2,1)S(1)}, u32[]{:S(2)}, u32[]{:S(2)}) collective-permute-start(bf16[128,512]{1,0:T(8,128)(2,1)S(1)} %collective-permute-done.16.refs_2_), channel_id=1, source_target_pairs={{0,1},{1,0},{2,3},{3,2},{4,5},{5,4},{6,7},{7,6},{8,9},{9,8},{10,11... | collective-permute-start | bytes 393224 | tf_op jit(solution)/shard_map/ppermute | solution.py:263
  53.7 8.5 %collective-permute-start.18 = (bf16[128,512]{1,0:T(8,128)(2,1)S(1)}, bf16[128,512]{1,0:T(8,128)(2,1)S(1)}, u32[]{:S(2)}, u32[]{:S(2)}) collective-permute-start(bf16[128,512]{1,0:T(8,128)(2,1)S(1)} %copy-done.3), channel_id=1, source_target_pairs={{0,1},{1,0},{2,3},{3,2},{4,5},{5,4},{6,7},{7,6},{8,9},{9,8},{10,11... | collective-permute-start | bytes 393224 | tf_op jit(solution)/shard_map/ppermute | solution.py:261
  54.2 12.3 %collective-permute-start.21 = (bf16[128,512]{1,0:T(8,128)(2,1)}, bf16[128,512]{1,0:T(8,128)(2,1)S(1)}, u32[]{:S(2)}, u32[]{:S(2)}) collective-permute-start(bf16[128,512]{1,0:T(8,128)(2,1)} %attention.5.refs_0_), channel_id=1, source_target_pairs={{0,1},{1,0},{2,3},{3,2},{4,5},{5,4},{6,7},{7,6},{8,9},{9,8},{10,11... | collective-permute-start | bytes 393224 | tf_op jit(solution)/shard_map/ppermute | solution.py:261
  54.2 7.9 %collective-permute-start.20 = (bf16[128,512]{1,0:T(8,128)(2,1)S(1)}, bf16[128,512]{1,0:T(8,128)(2,1)S(1)}, u32[]{:S(2)}, u32[]{:S(2)}) collective-permute-start(bf16[128,512]{1,0:T(8,128)(2,1)S(1)} %collective-permute-done.19.refs_2_), channel_id=1, source_target_pairs={{0,1},{1,0},{2,3},{3,2},{4,5},{5,4},{6,7},{7,6},{8,9},{9,8},{10,11... | collective-permute-start | bytes 393224 | tf_op jit(solution)/shard_map/ppermute | solution.py:263
  58.0 8.5 %collective-permute-start.23 = (bf16[128,512]{1,0:T(8,128)(2,1)S(1)}, bf16[128,512]{1,0:T(8,128)(2,1)S(1)}, u32[]{:S(2)}, u32[]{:S(2)}) collective-permute-start(bf16[128,512]{1,0:T(8,128)(2,1)S(1)} %collective-permute-done.22.refs_2_), channel_id=1, source_target_pairs={{0,1},{1,0},{2,3},{3,2},{4,5},{5,4},{6,7},{7,6},{8,9},{9,8},{10,11... | collective-permute-start | bytes 393224 | tf_op jit(solution)/shard_map/ppermute | solution.py:263
  (15 other events, 68.7 us)

commit v2 on v1

v2 whole, which is shorter than its diff:
```python
import functools

import jax
import jax.numpy as jnp
import numpy as np
from jax import lax
from jax.experimental import pallas as pl
from jax.experimental.pallas import tpu as pltpu
from jax.sharding import PartitionSpec as P

H = 16
DH = 128
KVH = 2
BLK = 64
NSEL = 32
HALF = DH // 2
THETA = 10000.0
SCALE = DH ** (-0.5)
EXP2_SCALE = SCALE * 1.4426950408889634
MASKED = -1e30
TILE = 4

ANY = pl.BlockSpec(memory_space=pl.ANY)
VMEM = pl.BlockSpec(memory_space=pltpu.VMEM)
HBM = pl.BlockSpec(memory_space=pltpu.HBM)
SMEM = pl.BlockSpec(memory_space=pltpu.SMEM)


def tables(blocks):
    inverse = THETA ** (-np.arange(HALF, dtype=np.float64) / HALF)
    inverse = np.concatenate([inverse, inverse])[None, :]
    coarse = (np.arange(blocks) * BLK)[:, None] * inverse
    fine = np.arange(BLK)[:, None] * inverse
    pack = lambda angle: np.stack([np.cos(angle), np.sin(angle)]).astype(np.float32)
    return pack(coarse), pack(fine)


def turns(first_block, count, coarse, fine):
    minus = lax.broadcasted_iota(jnp.int32, (BLK, DH), 1) < HALF
    fine_cosine = fine[0]
    fine_sine = fine[1]
    result = []
    for block in range(count):
        row = pl.ds(first_block + block, 1)
        coarse_cosine = coarse[0, row, :]
        coarse_sine = coarse[1, row, :]
        cosine = coarse_cosine * fine_cosine - coarse_sine * fine_sine
        sine = coarse_sine * fine_cosine + coarse_cosine * fine_sine
        result.append((cosine, jnp.where(minus, -sine, sine)))
    return result


def turn(values, angle):
    cosine, sine = angle
    return values * cosine + pltpu.roll(values, HALF, 1) * sine


def key_value_kernel(tokens, w_key, w_value, coarse, fine, out, slab, keys, values, sems):
    rows = slab.shape[0]
    width = tokens.shape[1]
    member = lax.axis_index("tp") % (tokens.shape[0] // rows)
    head = lax.axis_index("tp") // (tokens.shape[0] // rows)
    row = pl.multiple_of(member * rows, 8)
    column = pl.multiple_of(head * DH, DH)
    pieces = sems.shape[0]
    step = width // pieces
    copies = []
    for piece in range(pieces):
        part = pl.ds(piece * step, step)
        three = [
            pltpu.make_async_copy(tokens.at[pl.ds(row, rows), part], slab.at[:, part], sems.at[piece, 0]),
            pltpu.make_async_copy(w_key.at[part, pl.ds(column, DH)], keys.at[part], sems.at[piece, 1]),
            pltpu.make_async_copy(w_value.at[part, pl.ds(column, DH)], values.at[part], sems.at[piece, 2]),
        ]
        for copy in three:
            copy.start()
        copies.append(three)
    product = jnp.zeros((rows, 2 * DH), jnp.float32)
    for piece in range(pieces):
        for copy in copies[piece]:
            copy.wait()
        part = pl.ds(piece * step, step)
        right = jnp.concatenate([keys[part], values[part]], axis=1)
        product += jnp.dot(slab[:, part], right, preferred_element_type=jnp.float32)
    out[:, DH:] = product[:, DH:].astype(jnp.bfloat16)
    whole = tokens.shape[0] // BLK
    offset = member * rows % BLK
    if rows % BLK == 0:
        first = lax.axis_index("kv") * whole + member * (rows // BLK)
        for block, angle in enumerate(turns(first, rows // BLK, coarse, fine)):
            span = slice(block * BLK, (block + 1) * BLK)
            out[span, :DH] = turn(product[span, :DH], angle).astype(jnp.bfloat16)
    else:
        half = BLK // 2
        for step in range(rows // half):
            at = member * (rows // half) + step
            low = pl.multiple_of(at % 2 * half, half)
            row = pl.ds(lax.axis_index("kv") * whole + at // 2, 1)
            span = slice(step * half, (step + 1) * half)
            minus = lax.broadcasted_iota(jnp.int32, (half, DH), 1) < HALF
            fine_cosine = fine[0, pl.ds(low, half), :]
            fine_sine = fine[1, pl.ds(low, half), :]
            cosine = coarse[0, row, :] * fine_cosine - coarse[1, row, :] * fine_sine
            sine = coarse[1, row, :] * fine_cosine + coarse[0, row, :] * fine_sine
            angle = (cosine, jnp.where(minus, -sine, sine))
            out[span, :DH] = turn(product[span, :DH], angle).astype(jnp.bfloat16)


def query_kernel(tokens, w_query, coarse, fine, out):
    blocks = tokens.shape[0] // BLK
    product = jnp.dot(tokens[...], w_query[...], preferred_element_type=jnp.float32)
    for block, angle in enumerate(turns(lax.axis_index("kv") * blocks, blocks, coarse, fine)):
        span = slice(block * BLK, (block + 1) * BLK)
        for head in range(w_query.shape[1] // DH):
            column = slice(head * DH, (head + 1) * DH)
            out[span, column] = turn(product[span, column], angle).astype(jnp.bfloat16)


def attend(block, first, chosen, query, key_value, out, scores):
    heads = query.shape[1] // DH
    rows = heads * BLK
    tiles = NSEL // TILE
    lanes = TILE * BLK
    slot_of_lane = lax.broadcasted_iota(jnp.int32, (1, lanes), 1) // BLK
    transposed = (((1,), (1,)), ((), ()))

    def rows_of(place):
        return pl.ds(pl.multiple_of(place * BLK, BLK), BLK)

    def picked(tile, part):
        return jnp.concatenate(
            [key_value[rows_of(jnp.maximum(chosen[block, tile * TILE + slot], 0)), part] for slot in range(TILE)],
            axis=0,
        )

    span = pl.ds(block * BLK, BLK)
    mine = jnp.concatenate([query[span, head * DH : (head + 1) * DH] for head in range(heads)], axis=0)
    own = rows_of(lax.axis_index("kv") * (query.shape[0] // BLK) + block)
    highest = jnp.full((rows, lanes), MASKED, jnp.float32)
    for tile in range(tiles):
        score = lax.dot_general(mine, picked(tile, slice(0, DH)), transposed, preferred_element_type=jnp.float32)
        bias = jnp.zeros((1, lanes), jnp.float32)
        for slot in range(TILE):
            missing = jnp.where(chosen[block, tile * TILE + slot] < 0, MASKED, 0.0)
            bias = jnp.where(slot_of_lane == slot, missing, bias)
        score = score + bias
        scores[tile] = score
        highest = jnp.maximum(highest, score)
    diagonal = lax.dot_general(mine, key_value[own, :DH], transposed, preferred_element_type=jnp.float32)
    causal = (lax.broadcasted_iota(jnp.int32, (rows, BLK), 0) % BLK) >= lax.broadcasted_iota(
        jnp.int32, (rows, BLK), 1
    )
    diagonal = jnp.where(causal, diagonal, MASKED)
    top = jnp.maximum(jnp.max(highest, axis=1, keepdims=True), jnp.max(diagonal, axis=1, keepdims=True))
    ones = jnp.ones((lanes, DH), jnp.bfloat16)
    probs = jnp.exp2((diagonal - top) * EXP2_SCALE).astype(jnp.bfloat16)
    values = jnp.concatenate([key_value[own, DH:], ones[:BLK]], axis=1)
    summed = jnp.dot(probs, values, preferred_element_type=jnp.float32)
    for tile in range(tiles):
        probs = jnp.exp2((scores[tile] - top) * EXP2_SCALE).astype(jnp.bfloat16)
        values = jnp.concatenate([picked(tile, slice(DH, 2 * DH)), ones], axis=1)
        summed += jnp.dot(probs, values, preferred_element_type=jnp.float32)
    attention = (summed[:, :DH] / summed[:, DH:]).astype(jnp.bfloat16)
    target = slice((block - first) * BLK, (block - first + 1) * BLK)
    for head in range(heads):
        out[target, head * DH : (head + 1) * DH] = attention[head * BLK : (head + 1) * BLK]


def first_attention_kernel(*refs, first, count, sharing):
    chosen, query = refs[:2]
    shards = refs[2:-4]
    out, key_value, scores, sems = refs[-4:]
    blocks = query.shape[0] // BLK
    kv_index = lax.axis_index("kv")
    member = lax.axis_index("tp") % sharing
    held = blocks // sharing
    span = held * BLK

    def moves(act):
        for number, shard in enumerate(shards):
            steps, across, sibling = number // 4, number // 2 % 2, number % 2
            source = (kv_index // 2 - steps) * 2 + (kv_index % 2 ^ across)
            place = pl.multiple_of((source * blocks + (member ^ sibling) * held) * BLK, BLK)
            copy = pltpu.make_async_copy(shard, key_value.at[pl.ds(place, span)], sems.at[number])

            @pl.when(source >= 0)
            def _():
                act(copy)

    moves(lambda copy: copy.start())
    moves(lambda copy: copy.wait())
    for block in range(first, first + count):
        attend(block, first, chosen, query, key_value, out, scores)


def attention_kernel(chosen, query, key_value, out, scores, *, first, count):
    for block in range(first, first + count):
        attend(block, first, chosen, query, key_value, out, scores)


def project_kernel(*refs, pieces, first, relative):
    parts = refs[:pieces]
    w_out = refs[pieces]
    out, staged, sem = refs[-3:]
    depth = parts[0].shape[1]
    total = None
    for index, part in enumerate(parts):
        place = (lax.axis_index("tp") ^ index) if relative else index
        rows = pl.ds(pl.multiple_of(place * depth, depth), depth)
        product = jnp.dot(part[...], w_out[rows], preferred_element_type=jnp.float32)
        total = product if total is None else total + product
    staged[...] = total.astype(jnp.bfloat16)
    copy = pltpu.make_async_copy(staged, out.at[pl.ds(first, staged.shape[0])], sem)
    copy.start()
    copy.wait()


def spread_small(own, kv_count, tp_count):
    fast = 2
    slow = kv_count // fast
    by_slow = [own]
    for step in range(1, slow):
        pairs = [(i, i + step * fast) for i in range(kv_count - step * fast)]
        by_slow.append(lax.ppermute(own, "kv", pairs))
    everything = []
    for piece in by_slow:
        for side in (piece, lax.ppermute(piece, "kv", [(i, i ^ 1) for i in range(kv_count)])):
            everything.append(side)
            everything.append(lax.ppermute(side, "tp", [(i, i ^ 1) for i in range(tp_count)]))
    return everything


def keep(array):
    return pltpu.with_memory_space_constraint(array, pltpu.VMEM)


def stay(array):
    return pltpu.with_memory_space_constraint(array, pltpu.HBM)


def room(mebibytes):
    return pltpu.CompilerParams(vmem_limit_bytes=mebibytes << 20)


def body(tokens, w_query, w_key, w_value, w_out, chosen):
    rows, width = tokens.shape
    tp_count = lax.axis_size("tp")
    kv_count = lax.axis_size("kv")
    local_blocks = rows // BLK
    own_heads = w_query.shape[1] // DH
    own_width = own_heads * DH
    sharing = tp_count // KVH
    part_rows = rows // sharing
    small = kv_count == 8 and tp_count == 4
    coarse, fine = (jnp.asarray(table) for table in tables(kv_count * local_blocks))

    own_part = pl.pallas_call(
        key_value_kernel,
        out_shape=pltpu.VMEM((part_rows, 2 * DH), jnp.bfloat16),
        in_specs=[HBM, HBM, HBM, VMEM, VMEM],
        out_specs=VMEM,
        scratch_shapes=[
            pltpu.VMEM((part_rows, width), jnp.bfloat16),
            pltpu.VMEM((width, DH), jnp.bfloat16),
            pltpu.VMEM((width, DH), jnp.bfloat16),
            pltpu.SemaphoreType.DMA((4, 3)),
        ],
        cost_estimate=pl.CostEstimate(
            flops=4 * part_rows * width * DH, bytes_accessed=2 * width * (part_rows + 2 * DH), transcendentals=0
        ),
        compiler_params=room(10),
        name="key_value",
    )(stay(tokens), stay(w_key), stay(w_value), coarse, fine)

    query = pl.pallas_call(
        query_kernel,
        out_shape=pltpu.VMEM((rows, own_width), jnp.bfloat16),
        in_specs=[VMEM, VMEM, VMEM, VMEM],
        out_specs=VMEM,
        cost_estimate=pl.CostEstimate(
            flops=2 * rows * width * own_width, bytes_accessed=2 * width * (rows + own_width), transcendentals=0
        ),
        compiler_params=room(12),
        name="query",
    )(keep(tokens), keep(w_query), coarse, fine)
    query = keep(query)

    if small:
        shards = [keep(shard) for shard in spread_small(own_part, kv_count, tp_count)]
        key_value = None
    else:
        groups = [[g * sharing + i for i in range(sharing)] for g in range(KVH)]
        whole = lax.all_gather(own_part, "tp", axis=0, tiled=True, axis_index_groups=groups)
        key_value = lax.all_gather(whole, "kv", axis=0, tiled=True)

    splits = 2
    per = local_blocks // splits
    scores = pltpu.VMEM((NSEL // TILE, own_heads * BLK, TILE * BLK), jnp.float32)
    result = None
    w_out = keep(w_out)
    for split in range(splits):
        first = split * per
        shape = pltpu.VMEM((per * BLK, own_width), jnp.bfloat16)
        cost = pl.CostEstimate(
            flops=4 * per * BLK * own_width * (NSEL + 1) * BLK,
            bytes_accessed=2 * per * BLK * own_width,
            transcendentals=per * BLK * own_heads * (NSEL + 1) * BLK,
        )
        if key_value is None:
            attention, key_value = pl.pallas_call(
                functools.partial(first_attention_kernel, first=first, count=per, sharing=sharing),
                out_shape=[shape, pltpu.VMEM((kv_count * rows, 2 * DH), jnp.bfloat16)],
                in_specs=[SMEM, VMEM] + [VMEM] * len(shards),
                out_specs=[VMEM, VMEM],
                scratch_shapes=[scores, pltpu.SemaphoreType.DMA((len(shards),))],
                cost_estimate=cost,
                compiler_params=room(12),
                name="first_attention",
            )(chosen, query, *shards)
            key_value = keep(key_value)
        else:
            attention = pl.pallas_call(
                functools.partial(attention_kernel, first=first, count=per),
                out_shape=shape,
                in_specs=[SMEM, VMEM, VMEM],
                out_specs=VMEM,
                scratch_shapes=[scores],
                cost_estimate=cost,
                compiler_params=room(12 if small else 40),
                name="attention",
            )(chosen, query, key_value)
        if small:
            sibling = lax.ppermute(attention, "tp", [(i, i ^ 1) for i in range(tp_count)])
            across = lax.ppermute(attention, "tp", [(i, i ^ 2) for i in range(tp_count)])
            far = lax.ppermute(across, "tp", [(i, i ^ 1) for i in range(tp_count)])
            parts = [attention, sibling, across, far]
        else:
            parts = [lax.all_gather(attention, "tp", axis=1, tiled=True)]
        parts = [keep(part) for part in parts]
        earlier = [] if result is None else [result]
        result = pl.pallas_call(
            functools.partial(project_kernel, pieces=len(parts), first=first * BLK, relative=small),
            out_shape=jax.ShapeDtypeStruct((rows, w_out.shape[1]), jnp.bfloat16),
            in_specs=[VMEM] * (len(parts) + 1) + [ANY] * len(earlier),
            out_specs=ANY,
            input_output_aliases={len(parts) + 1: 0} if earlier else {},
            scratch_shapes=[
                pltpu.VMEM((per * BLK, w_out.shape[1]), jnp.bfloat16),
                pltpu.SemaphoreType.DMA,
            ],
            cost_estimate=pl.CostEstimate(
                flops=2 * per * BLK * H * DH * w_out.shape[1], bytes_accessed=0, transcendentals=0
            ),
            compiler_params=room(8),
            name="project",
        )(*parts, w_out, *earlier)
    return result


def solution(mesh):
    placed = (P("kv", None), P(None, "tp"), P(), P(), P(None, "tp"), P("kv", None))
    return jax.shard_map(body, mesh=mesh, in_specs=placed, out_specs=P("kv", "tp"), check_vma=False)
```

time: 72.9 us -> 48.2 us (0.66)
  the two profiles are of different devices: /device:TPU:0 before, /device:TPU:17 now
where the time goes in v2:
time: 48.2 us; the launch traced here: 48 us
  starting transfers between devices  20 us (41%)
  Pallas kernels  15.1 us (31%)
  waiting for transfers between devices  10.8 us (22%)
  local copies, waits for them, and re-layouts  1.95 us (4%)
    ppermute x8, starting transfers between devices, spread_small(): lax.ppermute(side, 'tp', [(i, i ^ 1) for i in range(tp_count)])  6.87 us
    ppermute x3, starting transfers between devices, spread_small(): by_slow.append(lax.ppermute(own, 'kv', pairs))  5.79 us
    pallas_call x1, Pallas kernels, body(): pl.pallas_call(functools.partial(first_attention_kernel, first=first, cou...  5.49 us
    ppermute x2, waiting for transfers between devices, body(): lax.ppermute(attention, 'tp', [(i, i ^ 2) for i in range(tp_count)])  4.32 us
    ppermute x3, waiting for transfers between devices, spread_small(): by_slow.append(lax.ppermute(own, 'kv', pairs))  4.19 us
    pallas_call x1, Pallas kernels, body(): pl.pallas_call(functools.partial(attention_kernel, first=first, count=per...  3.66 us
    ppermute x4, starting transfers between devices, spread_small(): lax.ppermute(piece, 'kv', [(i, i ^ 1) for i in range(kv_count)])  3 us
    pallas_call x2, Pallas kernels, body(): pl.pallas_call(functools.partial(project_kernel, pieces=len(parts), first...  2.56 us
  transfers between devices with their start and end apart: 21, of which 6 were waited for; matrix products, arithmetic and copies ran while one was open for 0% of the time, Pallas kernels for 13%

profile of v2, /device:TPU:17, one launch (start us, length us, event | category | flops | bytes accessed | tf_op | source)
XLA Modules:
  0.0 48.0 jit_solution(2501549059764226254)
XLA Ops:
  0.0 1.0 %copy-done.3 = f32[2,64,128]{2,1,0:T(8,128)S(1)} copy-done((f32[2,64,128]{2,1,0:T(8,128)S(1)}, f32[2,64,128]{2,1,0:T(8,128)}, u32[]{:S(2)}) %copy-start.3) | copy-done | bytes 65560
  1.0 0.9 %copy-done.5 = f32[2,48,128]{2,1,0:T(8,128)S(1)} copy-done((f32[2,48,128]{2,1,0:T(8,128)S(1)}, f32[2,48,128]{2,1,0:T(8,128)}, u32[]{:S(2)}) %copy-start.5) | copy-done | bytes 49176
  1.9 2.2 %key_value.1.refs_2_ = bf16[192,256]{1,0:T(8,128)(2,1)S(1)} custom-call(bf16[384,2048]{1,0:T(8,128)(2,1)} %tokens.3, bf16[2048,256]{1,0:T(8,128)(2,1)} %w_key.1, bf16[2048,256]{1,0:T(8,128)(2,1)} %w_value.1, f32[2,48,128]{2,1,0:T(8,128)S(1)} %copy-done.5, f32[2,64,128]{2,1,0:T(8,128)S(1)} %copy-done.3), custom_call_target="tpu_custom_call" | custom-call | flops 201326592 | bytes 1835008 | tf_op jit(solution)/shard_map/key_value/pallas_call | solution.py:257
  4.8 1.3 %collective-permute-start.7 = (bf16[192,256]{1,0:T(8,128)(2,1)S(1)}, bf16[192,256]{1,0:T(8,128)(2,1)S(1)}, u32[]{:S(2)}, u32[]{:S(2)}) collective-permute-start(bf16[192,256]{1,0:T(8,128)(2,1)S(1)} %key_value.1.refs_2_), channel_id=1, source_target_pairs={{0,16},{4,20},{8,24},{12,28},{1,17},{5,21},{9,25},{13,29},{2,18},{... | collective-permute-start | bytes 294920 | tf_op jit(solution)/shard_map/ppermute | solution.py:224
  6.1 3.8 %collective-permute-start.3 = (bf16[192,256]{1,0:T(8,128)(2,1)S(1)}, bf16[192,256]{1,0:T(8,128)(2,1)S(1)}, u32[]{:S(2)}, u32[]{:S(2)}) collective-permute-start(bf16[192,256]{1,0:T(8,128)(2,1)S(1)} %key_value.1.refs_2_), channel_id=1, source_target_pairs={{0,8},{4,12},{8,16},{12,20},{16,24},{20,28},{1,9},{5,13},{9,17},{1... | collective-permute-start | bytes 294920 | tf_op jit(solution)/shard_map/ppermute | solution.py:224
  10.0 1.3 %collective-permute-start.1 = (bf16[192,256]{1,0:T(8,128)(2,1)S(1)}, bf16[192,256]{1,0:T(8,128)(2,1)S(1)}, u32[]{:S(2)}, u32[]{:S(2)}) collective-permute-start(bf16[192,256]{1,0:T(8,128)(2,1)S(1)} %key_value.1.refs_2_), channel_id=1, source_target_pairs={{0,4},{4,0},{8,12},{12,8},{16,20},{20,16},{24,28},{28,24},{1,5},{5... | collective-permute-start | bytes 294920 | tf_op jit(solution)/shard_map/ppermute | solution.py:227
  11.3 1.2 %collective-permute-start = (bf16[192,256]{1,0:T(8,128)(2,1)S(1)}, bf16[192,256]{1,0:T(8,128)(2,1)S(1)}, u32[]{:S(2)}, u32[]{:S(2)}) collective-permute-start(bf16[192,256]{1,0:T(8,128)(2,1)S(1)} %key_value.1.refs_2_), channel_id=1, source_target_pairs={{0,1},{1,0},{2,3},{3,2},{4,5},{5,4},{6,7},{7,6},{8,9},{9,8},{10,11... | collective-permute-start | bytes 294920 | tf_op jit(solution)/shard_map/ppermute | solution.py:229
  12.8 1.3 %collective-permute-done.7.refs_10_ = bf16[192,256]{1,0:T(8,128)(2,1)S(1)} collective-permute-done((bf16[192,256]{1,0:T(8,128)(2,1)S(1)}, bf16[192,256]{1,0:T(8,128)(2,1)S(1)}, u32[]{:S(2)}, u32[]{:S(2)}) %collective-permute-start.7) | collective-permute-done | bytes 98336 | tf_op jit(solution)/shard_map/ppermute | solution.py:224
  14.1 2.1 %collective-permute-start.12 = (bf16[192,256]{1,0:T(8,128)(2,1)S(1)}, bf16[192,256]{1,0:T(8,128)(2,1)S(1)}, u32[]{:S(2)}, u32[]{:S(2)}) collective-permute-start(bf16[192,256]{1,0:T(8,128)(2,1)S(1)} %collective-permute-done.11.refs_14_), channel_id=1, source_target_pairs={{0,1},{1,0},{2,3},{3,2},{4,5},{5,4},{6,7},{7,6},{8,9},{9,8},{10,11... | collective-permute-start | bytes 294920 | tf_op jit(solution)/shard_map/ppermute | solution.py:229
  16.2 2.8 %collective-permute-done.3.refs_6_ = bf16[192,256]{1,0:T(8,128)(2,1)S(1)} collective-permute-done((bf16[192,256]{1,0:T(8,128)(2,1)S(1)}, bf16[192,256]{1,0:T(8,128)(2,1)S(1)}, u32[]{:S(2)}, u32[]{:S(2)}) %collective-permute-start.3) | collective-permute-done | bytes 98336 | tf_op jit(solution)/shard_map/ppermute | solution.py:224
  19.0 1.2 %collective-permute-start.9 = (bf16[192,256]{1,0:T(8,128)(2,1)S(1)}, bf16[192,256]{1,0:T(8,128)(2,1)S(1)}, u32[]{:S(2)}, u32[]{:S(2)}) collective-permute-start(bf16[192,256]{1,0:T(8,128)(2,1)S(1)} %collective-permute-done.7.refs_10_), channel_id=1, source_target_pairs={{0,4},{4,0},{8,12},{12,8},{16,20},{20,16},{24,28},{28,24},{1,5},{5... | collective-permute-start | bytes 294920 | tf_op jit(solution)/shard_map/ppermute | solution.py:227
  21.8 1.1 %collective-permute-done.9.refs_12_ = bf16[192,256]{1,0:T(8,128)(2,1)S(1)} collective-permute-done((bf16[192,256]{1,0:T(8,128)(2,1)S(1)}, bf16[192,256]{1,0:T(8,128)(2,1)S(1)}, u32[]{:S(2)}, u32[]{:S(2)}) %collective-permute-start.9) | collective-permute-done | bytes 98336 | tf_op jit(solution)/shard_map/ppermute | solution.py:227
  22.9 1.4 %collective-permute-start.14 = (bf16[192,256]{1,0:T(8,128)(2,1)S(1)}, bf16[192,256]{1,0:T(8,128)(2,1)S(1)}, u32[]{:S(2)}, u32[]{:S(2)}) collective-permute-start(bf16[192,256]{1,0:T(8,128)(2,1)S(1)} %collective-permute-done.13.refs_16_), channel_id=1, source_target_pairs={{0,1},{1,0},{2,3},{3,2},{4,5},{5,4},{6,7},{7,6},{8,9},{9,8},{10,11... | collective-permute-start | bytes 294920 | tf_op jit(solution)/shard_map/ppermute | solution.py:229
  24.3 1.2 %collective-permute-done.5.refs_8_ = bf16[192,256]{1,0:T(8,128)(2,1)S(1)} collective-permute-done((bf16[192,256]{1,0:T(8,128)(2,1)S(1)}, bf16[192,256]{1,0:T(8,128)(2,1)S(1)}, u32[]{:S(2)}, u32[]{:S(2)}) %collective-permute-start.5) | collective-permute-done | bytes 98336 | tf_op jit(solution)/shard_map/ppermute | solution.py:227
  25.5 0.8 %collective-permute-start.6 = (bf16[192,256]{1,0:T(8,128)(2,1)S(1)}, bf16[192,256]{1,0:T(8,128)(2,1)S(1)}, u32[]{:S(2)}, u32[]{:S(2)}) collective-permute-start(bf16[192,256]{1,0:T(8,128)(2,1)S(1)} %collective-permute-done.5.refs_8_), channel_id=1, source_target_pairs={{0,1},{1,0},{2,3},{3,2},{4,5},{5,4},{6,7},{7,6},{8,9},{9,8},{10,11... | collective-permute-start | bytes 294920 | tf_op jit(solution)/shard_map/ppermute | solution.py:229
  26.3 1.1 %query.1.refs_1_ = bf16[384,512]{1,0:T(8,128)(2,1)S(1)} custom-call(bf16[384,2048]{1,0:T(8,128)(2,1)S(1)} %copy-done.1, bf16[2048,512]{1,0:T(8,128)(2,1)S(1)} %copy-done.2, f32[2,48,128]{2,1,0:T(8,128)S(1)} %copy-done.6, f32[2,64,128]{2,1,0:T(8,128)S(1)} %copy-done.4), custom_call_target="tpu_custom_call" | custom-call | flops 805306368 | bytes 3670016 | tf_op jit(solution)/shard_map/query/pallas_call | solution.py:275
  27.6 5.5 %first_attention.1 = (bf16[192,512]{1,0:T(8,128)(2,1)S(1)}, bf16[3072,256]{1,0:T(8,128)(2,1)S(1)}) custom-call(s32[6,32]{1,0:T(8,128)S(1)} %copy-done.7, bf16[384,512]{1,0:T(8,128)(2,1)S(1)} %query.1.refs_1_, bf16[192,256]{1,0:T(8,128)(2,1)S(1)} %key_value.1.refs_2_, bf16[192,256]{1,0:T(8,128)(2,1)S(1)} %collective-permute-done.refs_3_, ...), custom_call_target="tpu_custom_call" | custom-call | flops 830472192 | bytes 196608 | tf_op jit(solution)/shard_map/first_attention/pallas_call | solution.py:310
  33.1 1.3 %collective-permute-start.19 = (bf16[192,512]{1,0:T(8,128)(2,1)S(1)}, bf16[192,512]{1,0:T(8,128)(2,1)S(1)}, u32[]{:S(2)}, u32[]{:S(2)}) collective-permute-start(bf16[192,512]{1,0:T(8,128)(2,1)S(1)} %get-tuple-element.8.refs_0_), channel_id=1, source_target_pairs={{0,2},{1,3},{2,0},{3,1},{4,6},{5,7},{6,4},{7,5},{8,10},{9,11},{10,... | collective-permute-start | bytes 589832 | tf_op jit(solution)/shard_map/ppermute | solution.py:334
  34.3 3.7 %attention.1.refs_0_ = bf16[192,512]{1,0:T(8,128)(2,1)S(1)} custom-call(s32[6,32]{1,0:T(8,128)S(1)} %copy-done.7, bf16[384,512]{1,0:T(8,128)(2,1)S(1)} %query.1.refs_1_, bf16[3072,256]{1,0:T(8,128)(2,1)S(1)} %get-tuple-element.7.key_value), custom_call_target="tpu_custom_call" | custom-call | flops 830472192 | bytes 196608 | tf_op jit(solution)/shard_map/attention/pallas_call | solution.py:322
  39.5 0.9 %collective-permute-start.20 = (bf16[192,512]{1,0:T(8,128)(2,1)S(1)}, bf16[192,512]{1,0:T(8,128)(2,1)S(1)}, u32[]{:S(2)}, u32[]{:S(2)}) collective-permute-start(bf16[192,512]{1,0:T(8,128)(2,1)S(1)} %collective-permute-done.19.refs_2_), channel_id=1, source_target_pairs={{0,1},{1,0},{2,3},{3,2},{4,5},{5,4},{6,7},{7,6},{8,9},{9,8},{10,11... | collective-permute-start | bytes 589832 | tf_op jit(solution)/shard_map/ppermute | solution.py:335
  40.5 3.7 %collective-permute-done.16.refs_2_ = bf16[192,512]{1,0:T(8,128)(2,1)S(1)} collective-permute-done((bf16[192,512]{1,0:T(8,128)(2,1)S(1)}, bf16[192,512]{1,0:T(8,128)(2,1)S(1)}, u32[]{:S(2)}, u32[]{:S(2)}) %collective-permute-start.16) | collective-permute-done | bytes 196640 | tf_op jit(solution)/shard_map/ppermute | solution.py:334
  44.2 1.2 %collective-permute-start.17 = (bf16[192,512]{1,0:T(8,128)(2,1)S(1)}, bf16[192,512]{1,0:T(8,128)(2,1)S(1)}, u32[]{:S(2)}, u32[]{:S(2)}) collective-permute-start(bf16[192,512]{1,0:T(8,128)(2,1)S(1)} %collective-permute-done.16.refs_2_), channel_id=1, source_target_pairs={{0,1},{1,0},{2,3},{3,2},{4,5},{5,4},{6,7},{7,6},{8,9},{9,8},{10,11... | collective-permute-start | bytes 589832 | tf_op jit(solution)/shard_map/ppermute | solution.py:335
  45.4 1.3 %project.2.refs_5_ = bf16[384,512]{1,0:T(8,128)(2,1)} custom-call(bf16[192,512]{1,0:T(8,128)(2,1)S(1)} %get-tuple-element.8.refs_0_, bf16[192,512]{1,0:T(8,128)(2,1)S(1)} %collective-permute-done.18.refs_1_, bf16[192,512]{1,0:T(8,128)(2,1)S(1)} %collective-permute-done.19.refs_2_, bf16[192,512]{1,0:T(8,128)(2,1)S(1)} %collective-permute-done.20.refs_3_, ...), custom_call_target="tpu_custom_call" | custom-call | flops 402653184 | tf_op jit(solution)/shard_map/project/pallas_call | solution.py:341
  46.7 1.3 %project.3 = bf16[384,512]{1,0:T(8,128)(2,1)} custom-call(bf16[192,512]{1,0:T(8,128)(2,1)S(1)} %attention.1.refs_0_, bf16[192,512]{1,0:T(8,128)(2,1)S(1)} %collective-permute-done.15.refs_1_, bf16[192,512]{1,0:T(8,128)(2,1)S(1)} %collective-permute-done.16.refs_2_, ...), custom_call_target="tpu_custom_call", output_to_operand_aliasing={{}: (5, {})} | custom-call | flops 402653184 | tf_op jit(solution)/shard_map/project/pallas_call | solution.py:341
  (40 shorter events, 4.0 us)
Async XLA Ops:
  0.0 26.3 %copy-start.1 = (bf16[384,2048]{1,0:T(8,128)(2,1)S(1)}, bf16[384,2048]{1,0:T(8,128)(2,1)}, u32[]{:S(2)}) copy-start(bf16[384,2048]{1,0:T(8,128)(2,1)} %tokens.3) | copy-start | bytes 4718596
  0.0 26.3 %copy-start.2 = (bf16[2048,512]{1,0:T(8,128)(2,1)S(1)}, bf16[2048,512]{1,0:T(8,128)(2,1)}, u32[]{:S(2)}) copy-start(bf16[2048,512]{1,0:T(8,128)(2,1)} %w_query.1) | copy-start | bytes 6291460
  1.9 24.4 %copy-start.6 = (f32[2,48,128]{2,1,0:T(8,128)S(1)}, f32[2,48,128]{2,1,0:T(8,128)}, u32[]{:S(2)}) copy-start(f32[2,48,128]{2,1,0:T(8,128)} %constant.4.clone.coarse) | copy-start | bytes 147460
  4.2 8.4 %collective-permute-start.11 = (bf16[192,256]{1,0:T(8,128)(2,1)S(1)}, bf16[192,256]{1,0:T(8,128)(2,1)S(1)}, u32[]{:S(2)}, u32[]{:S(2)}) collective-permute-start(bf16[192,256]{1,0:T(8,128)(2,1)S(1)} %key_value.1.refs_2_), channel_id=1, source_target_pairs={{0,24},{4,28},{1,25},{5,29},{2,26},{6,30},{3,27},{7,31}} | collective-permute-start | bytes 294920 | tf_op jit(solution)/shard_map/ppermute | solution.py:224
  4.8 9.2 %collective-permute-start.7 = (bf16[192,256]{1,0:T(8,128)(2,1)S(1)}, bf16[192,256]{1,0:T(8,128)(2,1)S(1)}, u32[]{:S(2)}, u32[]{:S(2)}) collective-permute-start(bf16[192,256]{1,0:T(8,128)(2,1)S(1)} %key_value.1.refs_2_), channel_id=1, source_target_pairs={{0,16},{4,20},{8,24},{12,28},{1,17},{5,21},{9,25},{13,29},{2,18},{... | collective-permute-start | bytes 294920 | tf_op jit(solution)/shard_map/ppermute | solution.py:224
  6.1 12.9 %collective-permute-start.3 = (bf16[192,256]{1,0:T(8,128)(2,1)S(1)}, bf16[192,256]{1,0:T(8,128)(2,1)S(1)}, u32[]{:S(2)}, u32[]{:S(2)}) collective-permute-start(bf16[192,256]{1,0:T(8,128)(2,1)S(1)} %key_value.1.refs_2_), channel_id=1, source_target_pairs={{0,8},{4,12},{8,16},{12,20},{16,24},{20,28},{1,9},{5,13},{9,17},{1... | collective-permute-start | bytes 294920 | tf_op jit(solution)/shard_map/ppermute | solution.py:224
  10.0 10.3 %collective-permute-start.1 = (bf16[192,256]{1,0:T(8,128)(2,1)S(1)}, bf16[192,256]{1,0:T(8,128)(2,1)S(1)}, u32[]{:S(2)}, u32[]{:S(2)}) collective-permute-start(bf16[192,256]{1,0:T(8,128)(2,1)S(1)} %key_value.1.refs_2_), channel_id=1, source_target_pairs={{0,4},{4,0},{8,12},{12,8},{16,20},{20,16},{24,28},{28,24},{1,5},{5... | collective-permute-start | bytes 294920 | tf_op jit(solution)/shard_map/ppermute | solution.py:227
  11.3 9.7 %collective-permute-start = (bf16[192,256]{1,0:T(8,128)(2,1)S(1)}, bf16[192,256]{1,0:T(8,128)(2,1)S(1)}, u32[]{:S(2)}, u32[]{:S(2)}) collective-permute-start(bf16[192,256]{1,0:T(8,128)(2,1)S(1)} %key_value.1.refs_2_), channel_id=1, source_target_pairs={{0,1},{1,0},{2,3},{3,2},{4,5},{5,4},{6,7},{7,6},{8,9},{9,8},{10,11... | collective-permute-start | bytes 294920 | tf_op jit(solution)/shard_map/ppermute | solution.py:229
  12.5 8.7 %collective-permute-start.13 = (bf16[192,256]{1,0:T(8,128)(2,1)S(1)}, bf16[192,256]{1,0:T(8,128)(2,1)S(1)}, u32[]{:S(2)}, u32[]{:S(2)}) collective-permute-start(bf16[192,256]{1,0:T(8,128)(2,1)S(1)} %collective-permute-done.11.refs_14_), channel_id=1, source_target_pairs={{0,4},{4,0},{8,12},{12,8},{16,20},{20,16},{24,28},{28,24},{1,5},{5... | collective-permute-start | bytes 294920 | tf_op jit(solution)/shard_map/ppermute | solution.py:227
  14.1 7.5 %collective-permute-start.12 = (bf16[192,256]{1,0:T(8,128)(2,1)S(1)}, bf16[192,256]{1,0:T(8,128)(2,1)S(1)}, u32[]{:S(2)}, u32[]{:S(2)}) collective-permute-start(bf16[192,256]{1,0:T(8,128)(2,1)S(1)} %collective-permute-done.11.refs_14_), channel_id=1, source_target_pairs={{0,1},{1,0},{2,3},{3,2},{4,5},{5,4},{6,7},{7,6},{8,9},{9,8},{10,11... | collective-permute-start | bytes 294920 | tf_op jit(solution)/shard_map/ppermute | solution.py:229
  19.0 3.9 %collective-permute-start.9 = (bf16[192,256]{1,0:T(8,128)(2,1)S(1)}, bf16[192,256]{1,0:T(8,128)(2,1)S(1)}, u32[]{:S(2)}, u32[]{:S(2)}) collective-permute-start(bf16[192,256]{1,0:T(8,128)(2,1)S(1)} %collective-permute-done.7.refs_10_), channel_id=1, source_target_pairs={{0,4},{4,0},{8,12},{12,8},{16,20},{20,16},{24,28},{28,24},{1,5},{5... | collective-permute-start | bytes 294920 | tf_op jit(solution)/shard_map/ppermute | solution.py:227
  20.3 4.1 %collective-permute-start.8 = (bf16[192,256]{1,0:T(8,128)(2,1)S(1)}, bf16[192,256]{1,0:T(8,128)(2,1)S(1)}, u32[]{:S(2)}, u32[]{:S(2)}) collective-permute-start(bf16[192,256]{1,0:T(8,128)(2,1)S(1)} %collective-permute-done.7.refs_10_), channel_id=1, source_target_pairs={{0,1},{1,0},{2,3},{3,2},{4,5},{5,4},{6,7},{7,6},{8,9},{9,8},{10,11... | collective-permute-start | bytes 294920 | tf_op jit(solution)/shard_map/ppermute | solution.py:229
  21.0 4.5 %collective-permute-start.5 = (bf16[192,256]{1,0:T(8,128)(2,1)S(1)}, bf16[192,256]{1,0:T(8,128)(2,1)S(1)}, u32[]{:S(2)}, u32[]{:S(2)}) collective-permute-start(bf16[192,256]{1,0:T(8,128)(2,1)S(1)} %collective-permute-done.3.refs_6_), channel_id=1, source_target_pairs={{0,4},{4,0},{8,12},{12,8},{16,20},{20,16},{24,28},{28,24},{1,5},{5... | collective-permute-start | bytes 294920 | tf_op jit(solution)/shard_map/ppermute | solution.py:227
  21.3 6.2 %collective-permute-start.4 = (bf16[192,256]{1,0:T(8,128)(2,1)S(1)}, bf16[192,256]{1,0:T(8,128)(2,1)S(1)}, u32[]{:S(2)}, u32[]{:S(2)}) collective-permute-start(bf16[192,256]{1,0:T(8,128)(2,1)S(1)} %collective-permute-done.3.refs_6_), channel_id=1, source_target_pairs={{0,1},{1,0},{2,3},{3,2},{4,5},{5,4},{6,7},{7,6},{8,9},{9,8},{10,11... | collective-permute-start | bytes 294920 | tf_op jit(solution)/shard_map/ppermute | solution.py:229
  21.6 5.9 %collective-permute-start.2 = (bf16[192,256]{1,0:T(8,128)(2,1)S(1)}, bf16[192,256]{1,0:T(8,128)(2,1)S(1)}, u32[]{:S(2)}, u32[]{:S(2)}) collective-permute-start(bf16[192,256]{1,0:T(8,128)(2,1)S(1)} %collective-permute-done.1.refs_4_), channel_id=1, source_target_pairs={{0,1},{1,0},{2,3},{3,2},{4,5},{5,4},{6,7},{7,6},{8,9},{9,8},{10,11... | collective-permute-start | bytes 294920 | tf_op jit(solution)/shard_map/ppermute | solution.py:229
  22.9 4.6 %collective-permute-start.14 = (bf16[192,256]{1,0:T(8,128)(2,1)S(1)}, bf16[192,256]{1,0:T(8,128)(2,1)S(1)}, u32[]{:S(2)}, u32[]{:S(2)}) collective-permute-start(bf16[192,256]{1,0:T(8,128)(2,1)S(1)} %collective-permute-done.13.refs_16_), channel_id=1, source_target_pairs={{0,1},{1,0},{2,3},{3,2},{4,5},{5,4},{6,7},{7,6},{8,9},{9,8},{10,11... | collective-permute-start | bytes 294920 | tf_op jit(solution)/shard_map/ppermute | solution.py:229
  24.3 3.2 %collective-permute-start.10 = (bf16[192,256]{1,0:T(8,128)(2,1)S(1)}, bf16[192,256]{1,0:T(8,128)(2,1)S(1)}, u32[]{:S(2)}, u32[]{:S(2)}) collective-permute-start(bf16[192,256]{1,0:T(8,128)(2,1)S(1)} %collective-permute-done.9.refs_12_), channel_id=1, source_target_pairs={{0,1},{1,0},{2,3},{3,2},{4,5},{5,4},{6,7},{7,6},{8,9},{9,8},{10,11... | collective-permute-start | bytes 294920 | tf_op jit(solution)/shard_map/ppermute | solution.py:229
  25.5 2.1 %collective-permute-start.6 = (bf16[192,256]{1,0:T(8,128)(2,1)S(1)}, bf16[192,256]{1,0:T(8,128)(2,1)S(1)}, u32[]{:S(2)}, u32[]{:S(2)}) collective-permute-start(bf16[192,256]{1,0:T(8,128)(2,1)S(1)} %collective-permute-done.5.refs_8_), channel_id=1, source_target_pairs={{0,1},{1,0},{2,3},{3,2},{4,5},{5,4},{6,7},{7,6},{8,9},{9,8},{10,11... | collective-permute-start | bytes 294920 | tf_op jit(solution)/shard_map/ppermute | solution.py:229
  33.1 6.5 %collective-permute-start.19 = (bf16[192,512]{1,0:T(8,128)(2,1)S(1)}, bf16[192,512]{1,0:T(8,128)(2,1)S(1)}, u32[]{:S(2)}, u32[]{:S(2)}) collective-permute-start(bf16[192,512]{1,0:T(8,128)(2,1)S(1)} %get-tuple-element.8.refs_0_), channel_id=1, source_target_pairs={{0,2},{1,3},{2,0},{3,1},{4,6},{5,7},{6,4},{7,5},{8,10},{9,11},{10,... | collective-permute-start | bytes 589832 | tf_op jit(solution)/shard_map/ppermute | solution.py:334
  38.0 6.2 %collective-permute-start.16 = (bf16[192,512]{1,0:T(8,128)(2,1)S(1)}, bf16[192,512]{1,0:T(8,128)(2,1)S(1)}, u32[]{:S(2)}, u32[]{:S(2)}) collective-permute-start(bf16[192,512]{1,0:T(8,128)(2,1)S(1)} %attention.1.refs_0_), channel_id=1, source_target_pairs={{0,2},{1,3},{2,0},{3,1},{4,6},{5,7},{6,4},{7,5},{8,10},{9,11},{10,... | collective-permute-start | bytes 589832 | tf_op jit(solution)/shard_map/ppermute | solution.py:334
  38.3 7.1 %collective-permute-start.18 = (bf16[192,512]{1,0:T(8,128)(2,1)S(1)}, bf16[192,512]{1,0:T(8,128)(2,1)S(1)}, u32[]{:S(2)}, u32[]{:S(2)}) collective-permute-start(bf16[192,512]{1,0:T(8,128)(2,1)S(1)} %get-tuple-element.8.refs_0_), channel_id=1, source_target_pairs={{0,1},{1,0},{2,3},{3,2},{4,5},{5,4},{6,7},{7,6},{8,9},{9,8},{10,11... | collective-permute-start | bytes 589832 | tf_op jit(solution)/shard_map/ppermute | solution.py:333
  39.5 5.9 %collective-permute-start.20 = (bf16[192,512]{1,0:T(8,128)(2,1)S(1)}, bf16[192,512]{1,0:T(8,128)(2,1)S(1)}, u32[]{:S(2)}, u32[]{:S(2)}) collective-permute-start(bf16[192,512]{1,0:T(8,128)(2,1)S(1)} %collective-permute-done.19.refs_2_), channel_id=1, source_target_pairs={{0,1},{1,0},{2,3},{3,2},{4,5},{5,4},{6,7},{7,6},{8,9},{9,8},{10,11... | collective-permute-start | bytes 589832 | tf_op jit(solution)/shard_map/ppermute | solution.py:335
  40.5 6.2 %collective-permute-start.15 = (bf16[192,512]{1,0:T(8,128)(2,1)S(1)}, bf16[192,512]{1,0:T(8,128)(2,1)S(1)}, u32[]{:S(2)}, u32[]{:S(2)}) collective-permute-start(bf16[192,512]{1,0:T(8,128)(2,1)S(1)} %attention.1.refs_0_), channel_id=1, source_target_pairs={{0,1},{1,0},{2,3},{3,2},{4,5},{5,4},{6,7},{7,6},{8,9},{9,8},{10,11... | collective-permute-start | bytes 589832 | tf_op jit(solution)/shard_map/ppermute | solution.py:333
  44.2 2.5 %collective-permute-start.17 = (bf16[192,512]{1,0:T(8,128)(2,1)S(1)}, bf16[192,512]{1,0:T(8,128)(2,1)S(1)}, u32[]{:S(2)}, u32[]{:S(2)}) collective-permute-start(bf16[192,512]{1,0:T(8,128)(2,1)S(1)} %collective-permute-done.16.refs_2_), channel_id=1, source_target_pairs={{0,1},{1,0},{2,3},{3,2},{4,5},{5,4},{6,7},{7,6},{8,9},{9,8},{10,11... | collective-permute-start | bytes 589832 | tf_op jit(solution)/shard_map/ppermute | solution.py:335
  (5 other events, 62.1 us)

commit v3 on v2

--- a/solution.py
+++ b/solution.py
@@ -7,6 +7,7 @@
 from jax.experimental import pallas as pl
 from jax.experimental.pallas import tpu as pltpu
 from jax.sharding import PartitionSpec as P
+
 
 H = 16
 DH = 128
@@ -55,7 +56,7 @@
     return values * cosine + pltpu.roll(values, HALF, 1) * sine
 
 
-def key_value_kernel(tokens, w_key, w_value, coarse, fine, out, slab, keys, values, sems):
+def key_value_kernel(tokens, w_key, w_value, coarse_hbm, fine_hbm, out, slab, keys, values, coarse, fine, sems, table_sems):
     rows = slab.shape[0]
     width = tokens.shape[1]
     member = lax.axis_index("tp") % (tokens.shape[0] // rows)
@@ -75,6 +76,12 @@
         for copy in three:
             copy.start()
         copies.append(three)
+    both = [
+        pltpu.make_async_copy(coarse_hbm, coarse, table_sems.at[0]),
+        pltpu.make_async_copy(fine_hbm, fine, table_sems.at[1]),
+    ]
+    for copy in both:
+        copy.start()
     product = jnp.zeros((rows, 2 * DH), jnp.float32)
     for piece in range(pieces):
         for copy in copies[piece]:
@@ -83,8 +90,9 @@
         right = jnp.concatenate([keys[part], values[part]], axis=1)
         product += jnp.dot(slab[:, part], right, preferred_element_type=jnp.float32)
     out[:, DH:] = product[:, DH:].astype(jnp.bfloat16)
+    for copy in both:
+        copy.wait()
     whole = tokens.shape[0] // BLK
-    offset = member * rows % BLK
     if rows % BLK == 0:
         first = lax.axis_index("kv") * whole + member * (rows // BLK)
         for block, angle in enumerate(turns(first, rows // BLK, coarse, fine)):
@@ -166,29 +174,34 @@
         out[target, head * DH : (head + 1) * DH] = attention[head * BLK : (head + 1) * BLK]
 
 
-def first_attention_kernel(*refs, first, count, sharing):
-    chosen, query = refs[:2]
-    shards = refs[2:-4]
-    out, key_value, scores, sems = refs[-4:]
-    blocks = query.shape[0] // BLK
+def collect(shards, tags, key_value, sems, blocks, sharing):
     kv_index = lax.axis_index("kv")
     member = lax.axis_index("tp") % sharing
     held = blocks // sharing
     span = held * BLK
 
     def moves(act):
-        for number, shard in enumerate(shards):
-            steps, across, sibling = number // 4, number // 2 % 2, number % 2
-            source = (kv_index // 2 - steps) * 2 + (kv_index % 2 ^ across)
+        for number, (shard, (bits, sibling)) in enumerate(zip(shards, tags)):
+            source = kv_index ^ bits
             place = pl.multiple_of((source * blocks + (member ^ sibling) * held) * BLK, BLK)
             copy = pltpu.make_async_copy(shard, key_value.at[pl.ds(place, span)], sems.at[number])
 
-            @pl.when(source >= 0)
+            @pl.when(source <= kv_index)
             def _():
                 act(copy)
 
     moves(lambda copy: copy.start())
     moves(lambda copy: copy.wait())
+
+
+def collect_kernel(*refs, tags, blocks, sharing):
+    collect(refs[: len(tags)], tags, refs[-2], refs[-1], blocks, sharing)
+
+
+def first_attention_kernel(*refs, first, count, tags, sharing):
+    chosen, query = refs[:2]
+    out, key_value, scores, sems = refs[-4:]
+    collect(refs[2 : 2 + len(tags)], tags, key_value, sems, query.shape[0] // BLK, sharing)
     for block in range(first, first + count):
         attend(block, first, chosen, query, key_value, out, scores)
 
@@ -215,18 +228,18 @@
     copy.wait()
 
 
+EXCHANGES = ((4, 4), (2, 2), (1, 1), (3, 1), (6, 2), (7, 3), (5, 1))
+
+
 def spread_small(own, kv_count, tp_count):
-    fast = 2
-    slow = kv_count // fast
-    by_slow = [own]
-    for step in range(1, slow):
-        pairs = [(i, i + step * fast) for i in range(kv_count - step * fast)]
-        by_slow.append(lax.ppermute(own, "kv", pairs))
-    everything = []
-    for piece in by_slow:
-        for side in (piece, lax.ppermute(piece, "kv", [(i, i ^ 1) for i in range(kv_count)])):
-            everything.append(side)
-            everything.append(lax.ppermute(side, "tp", [(i, i ^ 1) for i in range(tp_count)]))
+    shards = {0: own}
+    for bits, hop in EXCHANGES:
+        pairs = [(i, i ^ hop) for i in range(kv_count)]
+        shards[bits] = lax.ppermute(shards[bits ^ hop], "kv", pairs)
+    everything = {}
+    for bits, shard in shards.items():
+        everything[bits, 0] = shard
+        everything[bits, 1] = lax.ppermute(shard, "tp", [(i, i ^ 1) for i in range(tp_count)])
     return everything
 
 
@@ -257,20 +270,23 @@
     own_part = pl.pallas_call(
         key_value_kernel,
         out_shape=pltpu.VMEM((part_rows, 2 * DH), jnp.bfloat16),
-        in_specs=[HBM, HBM, HBM, VMEM, VMEM],
+        in_specs=[HBM] * 5,
         out_specs=VMEM,
         scratch_shapes=[
             pltpu.VMEM((part_rows, width), jnp.bfloat16),
             pltpu.VMEM((width, DH), jnp.bfloat16),
             pltpu.VMEM((width, DH), jnp.bfloat16),
+            pltpu.VMEM(coarse.shape, jnp.float32),
+            pltpu.VMEM(fine.shape, jnp.float32),
             pltpu.SemaphoreType.DMA((4, 3)),
+            pltpu.SemaphoreType.DMA((2,)),
         ],
         cost_estimate=pl.CostEstimate(
             flops=4 * part_rows * width * DH, bytes_accessed=2 * width * (part_rows + 2 * DH), transcendentals=0
         ),
         compiler_params=room(10),
         name="key_value",
-    )(stay(tokens), stay(w_key), stay(w_value), coarse, fine)
+    )(stay(tokens), stay(w_key), stay(w_value), stay(coarse), stay(fine))
 
     query = pl.pallas_call(
         query_kernel,
@@ -286,14 +302,25 @@
     query = keep(query)
 
     if small:
-        shards = [keep(shard) for shard in spread_small(own_part, kv_count, tp_count)]
-        key_value = None
+        shards = spread_small(own_part, kv_count, tp_count)
+        late = [tag for tag in shards if tag[0] > 4]
+        early = [tag for tag in shards if tag not in late]
+        key_value = pl.pallas_call(
+            functools.partial(collect_kernel, tags=early, blocks=local_blocks, sharing=sharing),
+            out_shape=pltpu.VMEM((kv_count * rows, 2 * DH), jnp.bfloat16),
+            in_specs=[VMEM] * len(early),
+            out_specs=VMEM,
+            scratch_shapes=[pltpu.SemaphoreType.DMA((len(early),))],
+            compiler_params=room(2),
+            name="collect",
+        )(*[keep(shards[tag]) for tag in early])
+        key_value = keep(key_value)
     else:
         groups = [[g * sharing + i for i in range(sharing)] for g in range(KVH)]
         whole = lax.all_gather(own_part, "tp", axis=0, tiled=True, axis_index_groups=groups)
         key_value = lax.all_gather(whole, "kv", axis=0, tiled=True)
 
-    splits = 2
+    splits = 3
     per = local_blocks // splits
     scores = pltpu.VMEM((NSEL // TILE, own_heads * BLK, TILE * BLK), jnp.float32)
     result = None
@@ -306,20 +333,21 @@
             bytes_accessed=2 * per * BLK * own_width,
             transcendentals=per * BLK * own_heads * (NSEL + 1) * BLK,
         )
-        if key_value is None:
+        if small and split == 0:
             attention, key_value = pl.pallas_call(
-                functools.partial(first_attention_kernel, first=first, count=per, sharing=sharing),
+                functools.partial(first_attention_kernel, first=first, count=per, tags=late, sharing=sharing),
                 out_shape=[shape, pltpu.VMEM((kv_count * rows, 2 * DH), jnp.bfloat16)],
-                in_specs=[SMEM, VMEM] + [VMEM] * len(shards),
+                in_specs=[SMEM, VMEM] + [VMEM] * (len(late) + 1),
                 out_specs=[VMEM, VMEM],
-                scratch_shapes=[scores, pltpu.SemaphoreType.DMA((len(shards),))],
+                input_output_aliases={len(late) + 2: 1},
+                scratch_shapes=[scores, pltpu.SemaphoreType.DMA((len(late),))],
                 cost_estimate=cost,
                 compiler_params=room(12),
                 name="first_attention",
-            )(chosen, query, *shards)
+            )(chosen, query, *[keep(shards[tag]) for tag in late], key_value)
             key_value = keep(key_value)
         else:
-            attention = pl.pallas_call(
+            call = pl.pallas_call(
                 functools.partial(attention_kernel, first=first, count=per),
                 out_shape=shape,
                 in_specs=[SMEM, VMEM, VMEM],
@@ -328,7 +356,8 @@
                 cost_estimate=cost,
                 compiler_params=room(12 if small else 40),
                 name="attention",
-            )(chosen, query, key_value)
+            )
+            attention = call(chosen, query, key_value)
         if small:
             sibling = lax.ppermute(attention, "tp", [(i, i ^ 1) for i in range(tp_count)])
             across = lax.ppermute(attention, "tp", [(i, i ^ 2) for i in range(tp_count)])
@@ -338,7 +367,7 @@
             parts = [lax.all_gather(attention, "tp", axis=1, tiled=True)]
         parts = [keep(part) for part in parts]
         earlier = [] if result is None else [result]
-        result = pl.pallas_call(
+        call = pl.pallas_call(
             functools.partial(project_kernel, pieces=len(parts), first=first * BLK, relative=small),
             out_shape=jax.ShapeDtypeStruct((rows, w_out.shape[1]), jnp.bfloat16),
             in_specs=[VMEM] * (len(parts) + 1) + [ANY] * len(earlier),
@@ -353,10 +382,12 @@
             ),
             compiler_params=room(8),
             name="project",
-        )(*parts, w_out, *earlier)
+        )
+        result = call(*parts, w_out, *earlier)
     return result
 
 
 def solution(mesh):
     placed = (P("kv", None), P(None, "tp"), P(), P(), P(None, "tp"), P("kv", None))
+
     return jax.shard_map(body, mesh=mesh, in_specs=placed, out_specs=P("kv", "tp"), check_vma=False)

time: 48.2 us -> 44.9 us (0.932)
  the two profiles are of different devices: /device:TPU:17 before, /device:TPU:0 now
where the time goes in v3:
time: 44.9 us; the launch traced here: 44.7 us
  Pallas kernels  16.4 us (37%)
  starting transfers between devices  16.4 us (37%)
  waiting for transfers between devices  11.5 us (26%)
    ppermute x7, starting transfers between devices, spread_small(): shards[bits] = lax.ppermute(shards[bits ^ hop], 'kv', pairs)  10.7 us
    ppermute x7, waiting for transfers between devices, spread_small(): shards[bits] = lax.ppermute(shards[bits ^ hop], 'kv', pairs)  7.04 us
    pallas_call x2, Pallas kernels, body(): attention = call(chosen, query, key_value)  5.99 us
    ppermute x3, waiting for transfers between devices, body(): lax.ppermute(attention, 'tp', [(i, i ^ 2) for i in range(tp_count)])  4.41 us
    ppermute x3, starting transfers between devices, body(): lax.ppermute(attention, 'tp', [(i, i ^ 2) for i in range(tp_count)])  3.65 us
    pallas_call x3, Pallas kernels, body(): result = call(*parts, w_out, *earlier)  3.35 us
    pallas_call x1, Pallas kernels, body(): pl.pallas_call(functools.partial(first_attention_kernel, first=first, cou...  3.09 us
    pallas_call x1, Pallas kernels, body(): pl.pallas_call(key_value_kernel, out_shape=pltpu.VMEM((part_rows, 2 * DH)...  2.39 us
  transfers between devices with their start and end apart: 24, of which 7 were waited for; matrix products, arithmetic and copies ran while one was open for 0% of the time, Pallas kernels for 15%

profile of v3, /device:TPU:0, one launch (start us, length us, event | category | flops | bytes accessed | tf_op | source)
XLA Modules:
  0.0 44.7 jit_solution(2094984679873023232)
XLA Ops:
  0.0 2.4 %key_value.1.refs_0_ = bf16[192,256]{1,0:T(8,128)(2,1)S(1)} custom-call(bf16[384,2048]{1,0:T(8,128)(2,1)} %tokens.3, bf16[2048,256]{1,0:T(8,128)(2,1)} %w_key.1, bf16[2048,256]{1,0:T(8,128)(2,1)} %w_value.1, f32[2,48,128]{2,1,0:T(8,128)} %constant.4.clone.coarse.coarse_hbm, f32[2,64,128]{2,1,0:T(8,128)} %constant.5.clone.fine.fine_hbm), custom_call_target="tpu_custom_call" | custom-call | flops 201326592 | bytes 1835008 | tf_op jit(solution)/shard_map/key_value/pallas_call | solution.py:270
  2.4 3.1 %collective-permute-start.11 = (bf16[192,256]{1,0:T(8,128)(2,1)S(1)}, bf16[192,256]{1,0:T(8,128)(2,1)S(1)}, u32[]{:S(2)}, u32[]{:S(2)}) collective-permute-start(bf16[192,256]{1,0:T(8,128)(2,1)S(1)} %key_value.1.refs_0_), channel_id=1, source_target_pairs={{0,4},{4,0},{8,12},{12,8},{16,20},{20,16},{24,28},{28,24},{1,5},{5... | collective-permute-start | bytes 294920 | tf_op jit(solution)/shard_map/ppermute | solution.py:238
  5.5 1.6 %collective-permute-start.9 = (bf16[192,256]{1,0:T(8,128)(2,1)S(1)}, bf16[192,256]{1,0:T(8,128)(2,1)S(1)}, u32[]{:S(2)}, u32[]{:S(2)}) collective-permute-start(bf16[192,256]{1,0:T(8,128)(2,1)S(1)} %key_value.1.refs_0_), channel_id=1, source_target_pairs={{0,8},{4,12},{8,0},{12,4},{16,24},{20,28},{24,16},{28,20},{1,9},{5... | collective-permute-start | bytes 294920 | tf_op jit(solution)/shard_map/ppermute | solution.py:238
  7.1 2.6 %collective-permute-start = (bf16[192,256]{1,0:T(8,128)(2,1)S(1)}, bf16[192,256]{1,0:T(8,128)(2,1)S(1)}, u32[]{:S(2)}, u32[]{:S(2)}) collective-permute-start(bf16[192,256]{1,0:T(8,128)(2,1)S(1)} %key_value.1.refs_0_), channel_id=1, source_target_pairs={{0,16},{4,20},{8,24},{12,28},{16,0},{20,4},{24,8},{28,12},{1,17},{... | collective-permute-start | bytes 294920 | tf_op jit(solution)/shard_map/ppermute | solution.py:238
  9.7 0.5 %collective-permute-start.12 = (bf16[192,256]{1,0:T(8,128)(2,1)S(1)}, bf16[192,256]{1,0:T(8,128)(2,1)S(1)}, u32[]{:S(2)}, u32[]{:S(2)}) collective-permute-start(bf16[192,256]{1,0:T(8,128)(2,1)S(1)} %collective-permute-done.11.refs_6_), channel_id=1, source_target_pairs={{0,1},{1,0},{2,3},{3,2},{4,5},{5,4},{6,7},{7,6},{8,9},{9,8},{10,11... | collective-permute-start | bytes 294920 | tf_op jit(solution)/shard_map/ppermute | solution.py:242
  10.2 0.9 %collective-permute-done.9.refs_4_ = bf16[192,256]{1,0:T(8,128)(2,1)S(1)} collective-permute-done((bf16[192,256]{1,0:T(8,128)(2,1)S(1)}, bf16[192,256]{1,0:T(8,128)(2,1)S(1)}, u32[]{:S(2)}, u32[]{:S(2)}) %collective-permute-start.9) | collective-permute-done | bytes 98336 | tf_op jit(solution)/shard_map/ppermute | solution.py:238
  11.1 3.0 %collective-permute-done.refs_2_ = bf16[192,256]{1,0:T(8,128)(2,1)S(1)} collective-permute-done((bf16[192,256]{1,0:T(8,128)(2,1)S(1)}, bf16[192,256]{1,0:T(8,128)(2,1)S(1)}, u32[]{:S(2)}, u32[]{:S(2)}) %collective-permute-start) | collective-permute-done | bytes 98336 | tf_op jit(solution)/shard_map/ppermute | solution.py:238
  14.6 1.3 %collective-permute-start.3 = (bf16[192,256]{1,0:T(8,128)(2,1)S(1)}, bf16[192,256]{1,0:T(8,128)(2,1)S(1)}, u32[]{:S(2)}, u32[]{:S(2)}) collective-permute-start(bf16[192,256]{1,0:T(8,128)(2,1)S(1)} %collective-permute-done.refs_2_), channel_id=1, source_target_pairs={{0,12},{4,8},{8,4},{12,0},{16,28},{20,24},{24,20},{28,16},{1,13},{... | collective-permute-start | bytes 294920 | tf_op jit(solution)/shard_map/ppermute | solution.py:238
  15.9 1.7 %collective-permute-start.1 = (bf16[192,256]{1,0:T(8,128)(2,1)S(1)}, bf16[192,256]{1,0:T(8,128)(2,1)S(1)}, u32[]{:S(2)}, u32[]{:S(2)}) collective-permute-start(bf16[192,256]{1,0:T(8,128)(2,1)S(1)} %collective-permute-done.refs_2_), channel_id=1, source_target_pairs={{0,8},{4,12},{8,0},{12,4},{16,24},{20,28},{24,16},{28,20},{1,9},{5... | collective-permute-start | bytes 294920 | tf_op jit(solution)/shard_map/ppermute | solution.py:238
  18.1 0.8 %collective-permute-done.5.refs_6_ = bf16[192,256]{1,0:T(8,128)(2,1)S(1)} collective-permute-done((bf16[192,256]{1,0:T(8,128)(2,1)S(1)}, bf16[192,256]{1,0:T(8,128)(2,1)S(1)}, u32[]{:S(2)}, u32[]{:S(2)}) %collective-permute-start.5) | collective-permute-done | bytes 98336 | tf_op jit(solution)/shard_map/ppermute | solution.py:238
  18.9 1.2 %collective-permute-done.3.refs_4_ = bf16[192,256]{1,0:T(8,128)(2,1)S(1)} collective-permute-done((bf16[192,256]{1,0:T(8,128)(2,1)S(1)}, bf16[192,256]{1,0:T(8,128)(2,1)S(1)}, u32[]{:S(2)}, u32[]{:S(2)}) %collective-permute-start.3) | collective-permute-done | bytes 98336 | tf_op jit(solution)/shard_map/ppermute | solution.py:238
  20.1 1.1 %collective-permute-done.1.refs_2_ = bf16[192,256]{1,0:T(8,128)(2,1)S(1)} collective-permute-done((bf16[192,256]{1,0:T(8,128)(2,1)S(1)}, bf16[192,256]{1,0:T(8,128)(2,1)S(1)}, u32[]{:S(2)}, u32[]{:S(2)}) %collective-permute-start.1) | collective-permute-done | bytes 98336 | tf_op jit(solution)/shard_map/ppermute | solution.py:238
  21.3 1.1 %query.1.refs_1_ = bf16[384,512]{1,0:T(8,128)(2,1)S(1)} custom-call(bf16[384,2048]{1,0:T(8,128)(2,1)S(1)} %copy-done.1, bf16[2048,512]{1,0:T(8,128)(2,1)S(1)} %copy-done.2, f32[2,48,128]{2,1,0:T(8,128)S(1)} %copy-done.4, f32[2,64,128]{2,1,0:T(8,128)S(1)} %copy-done.3), custom_call_target="tpu_custom_call" | custom-call | flops 805306368 | bytes 3670016 | tf_op jit(solution)/shard_map/query/pallas_call | solution.py:291
  23.1 3.1 %first_attention.1 = (bf16[128,512]{1,0:T(8,128)(2,1)S(1)}, bf16[3072,256]{1,0:T(8,128)(2,1)S(1)}) custom-call(s32[6,32]{1,0:T(8,128)S(1)} %copy-done.5, bf16[384,512]{1,0:T(8,128)(2,1)S(1)} %query.1.refs_1_, bf16[192,256]{1,0:T(8,128)(2,1)S(1)} %collective-permute-done.1.refs_2_, ...), custom_call_target="tpu_custom_call", output_to_operand_aliasing={{1}: (8, {})} | custom-call | flops 553648128 | bytes 131072 | tf_op jit(solution)/shard_map/first_attention/pallas_call | solution.py:337
  26.2 3.0 %attention.3.refs_0_ = bf16[128,512]{1,0:T(8,128)(2,1)S(1)} custom-call(s32[6,32]{1,0:T(8,128)S(1)} %copy-done.5, bf16[384,512]{1,0:T(8,128)(2,1)S(1)} %query.1.refs_1_, bf16[3072,256]{1,0:T(8,128)(2,1)S(1)} %get-tuple-element.7.key_value), custom_call_target="tpu_custom_call" | custom-call | flops 553648128 | bytes 131072 | tf_op jit(solution)/shard_map/attention/pallas_call | solution.py:360
  29.2 1.6 %collective-permute-start.19 = (bf16[128,512]{1,0:T(8,128)(2,1)S(1)}, bf16[128,512]{1,0:T(8,128)(2,1)S(1)}, u32[]{:S(2)}, u32[]{:S(2)}) collective-permute-start(bf16[128,512]{1,0:T(8,128)(2,1)S(1)} %attention.3.refs_0_), channel_id=1, source_target_pairs={{0,2},{1,3},{2,0},{3,1},{4,6},{5,7},{6,4},{7,5},{8,10},{9,11},{10,... | collective-permute-start | bytes 393224 | tf_op jit(solution)/shard_map/ppermute | solution.py:363
  30.8 0.5 %collective-permute-start.22 = (bf16[128,512]{1,0:T(8,128)(2,1)S(1)}, bf16[128,512]{1,0:T(8,128)(2,1)S(1)}, u32[]{:S(2)}, u32[]{:S(2)}) collective-permute-start(bf16[128,512]{1,0:T(8,128)(2,1)S(1)} %get-tuple-element.8.refs_0_), channel_id=1, source_target_pairs={{0,2},{1,3},{2,0},{3,1},{4,6},{5,7},{6,4},{7,5},{8,10},{9,11},{10,... | collective-permute-start | bytes 393224 | tf_op jit(solution)/shard_map/ppermute | solution.py:363
  31.3 3.0 %attention.2.refs_0_ = bf16[128,512]{1,0:T(8,128)(2,1)S(1)} custom-call(s32[6,32]{1,0:T(8,128)S(1)} %copy-done.5, bf16[384,512]{1,0:T(8,128)(2,1)S(1)} %query.1.refs_1_, bf16[3072,256]{1,0:T(8,128)(2,1)S(1)} %get-tuple-element.7.key_value), custom_call_target="tpu_custom_call" | custom-call | flops 553648128 | bytes 131072 | tf_op jit(solution)/shard_map/attention/pallas_call | solution.py:360
  34.3 1.6 %collective-permute-start.16 = (bf16[128,512]{1,0:T(8,128)(2,1)S(1)}, bf16[128,512]{1,0:T(8,128)(2,1)S(1)}, u32[]{:S(2)}, u32[]{:S(2)}) collective-permute-start(bf16[128,512]{1,0:T(8,128)(2,1)S(1)} %attention.2.refs_0_), channel_id=1, source_target_pairs={{0,2},{1,3},{2,0},{3,1},{4,6},{5,7},{6,4},{7,5},{8,10},{9,11},{10,... | collective-permute-start | bytes 393224 | tf_op jit(solution)/shard_map/ppermute | solution.py:363
  35.9 2.6 %collective-permute-done.22.refs_2_ = bf16[128,512]{1,0:T(8,128)(2,1)S(1)} collective-permute-done((bf16[128,512]{1,0:T(8,128)(2,1)S(1)}, bf16[128,512]{1,0:T(8,128)(2,1)S(1)}, u32[]{:S(2)}, u32[]{:S(2)}) %collective-permute-start.22) | collective-permute-done | bytes 131104 | tf_op jit(solution)/shard_map/ppermute | solution.py:363
  39.0 1.8 %collective-permute-done.16.refs_2_ = bf16[128,512]{1,0:T(8,128)(2,1)S(1)} collective-permute-done((bf16[128,512]{1,0:T(8,128)(2,1)S(1)}, bf16[128,512]{1,0:T(8,128)(2,1)S(1)}, u32[]{:S(2)}, u32[]{:S(2)}) %collective-permute-start.16) | collective-permute-done | bytes 131104 | tf_op jit(solution)/shard_map/ppermute | solution.py:363
  41.3 1.1 %project.3.refs_5_ = bf16[384,512]{1,0:T(8,128)(2,1)} custom-call(bf16[128,512]{1,0:T(8,128)(2,1)S(1)} %get-tuple-element.8.refs_0_, bf16[128,512]{1,0:T(8,128)(2,1)S(1)} %collective-permute-done.21.refs_1_, bf16[128,512]{1,0:T(8,128)(2,1)S(1)} %collective-permute-done.22.refs_2_, bf16[128,512]{1,0:T(8,128)(2,1)S(1)} %collective-permute-done.23.refs_3_, ...), custom_call_target="tpu_custom_call" | custom-call | flops 268435456 | tf_op jit(solution)/shard_map/project/pallas_call | solution.py:386
  42.4 1.1 %project.4.refs_5_ = bf16[384,512]{1,0:T(8,128)(2,1)} custom-call(bf16[128,512]{1,0:T(8,128)(2,1)S(1)} %attention.3.refs_0_, bf16[128,512]{1,0:T(8,128)(2,1)S(1)} %collective-permute-done.18.refs_1_, bf16[128,512]{1,0:T(8,128)(2,1)S(1)} %collective-permute-done.19.refs_2_, ...), custom_call_target="tpu_custom_call", output_to_operand_aliasing={{}: (5, {})} | custom-call | flops 268435456 | tf_op jit(solution)/shard_map/project/pallas_call | solution.py:386
  43.6 1.1 %project.5 = bf16[384,512]{1,0:T(8,128)(2,1)} custom-call(bf16[128,512]{1,0:T(8,128)(2,1)S(1)} %attention.2.refs_0_, bf16[128,512]{1,0:T(8,128)(2,1)S(1)} %collective-permute-done.15.refs_1_, bf16[128,512]{1,0:T(8,128)(2,1)S(1)} %collective-permute-done.16.refs_2_, ...), custom_call_target="tpu_custom_call", output_to_operand_aliasing={{}: (5, {})} | custom-call | flops 268435456 | tf_op jit(solution)/shard_map/project/pallas_call | solution.py:386
  (45 shorter events, 2.7 us)
Async XLA Ops:
  2.4 7.2 %collective-permute-start.11 = (bf16[192,256]{1,0:T(8,128)(2,1)S(1)}, bf16[192,256]{1,0:T(8,128)(2,1)S(1)}, u32[]{:S(2)}, u32[]{:S(2)}) collective-permute-start(bf16[192,256]{1,0:T(8,128)(2,1)S(1)} %key_value.1.refs_0_), channel_id=1, source_target_pairs={{0,4},{4,0},{8,12},{12,8},{16,20},{20,16},{24,28},{28,24},{1,5},{5... | collective-permute-start | bytes 294920 | tf_op jit(solution)/shard_map/ppermute | solution.py:238
  5.5 5.6 %collective-permute-start.9 = (bf16[192,256]{1,0:T(8,128)(2,1)S(1)}, bf16[192,256]{1,0:T(8,128)(2,1)S(1)}, u32[]{:S(2)}, u32[]{:S(2)}) collective-permute-start(bf16[192,256]{1,0:T(8,128)(2,1)S(1)} %key_value.1.refs_0_), channel_id=1, source_target_pairs={{0,8},{4,12},{8,0},{12,4},{16,24},{20,28},{24,16},{28,20},{1,9},{5... | collective-permute-start | bytes 294920 | tf_op jit(solution)/shard_map/ppermute | solution.py:238
  7.1 7.0 %collective-permute-start = (bf16[192,256]{1,0:T(8,128)(2,1)S(1)}, bf16[192,256]{1,0:T(8,128)(2,1)S(1)}, u32[]{:S(2)}, u32[]{:S(2)}) collective-permute-start(bf16[192,256]{1,0:T(8,128)(2,1)S(1)} %key_value.1.refs_0_), channel_id=1, source_target_pairs={{0,16},{4,20},{8,24},{12,28},{16,0},{20,4},{24,8},{28,12},{1,17},{... | collective-permute-start | bytes 294920 | tf_op jit(solution)/shard_map/ppermute | solution.py:238
  9.6 5.0 %collective-permute-start.7 = (bf16[192,256]{1,0:T(8,128)(2,1)S(1)}, bf16[192,256]{1,0:T(8,128)(2,1)S(1)}, u32[]{:S(2)}, u32[]{:S(2)}) collective-permute-start(bf16[192,256]{1,0:T(8,128)(2,1)S(1)} %key_value.1.refs_0_), channel_id=1, source_target_pairs={{0,1},{1,0},{2,3},{3,2},{4,5},{5,4},{6,7},{7,6},{8,9},{9,8},{10,11... | collective-permute-start | bytes 294920 | tf_op jit(solution)/shard_map/ppermute | solution.py:242
  9.7 6.2 %collective-permute-start.12 = (bf16[192,256]{1,0:T(8,128)(2,1)S(1)}, bf16[192,256]{1,0:T(8,128)(2,1)S(1)}, u32[]{:S(2)}, u32[]{:S(2)}) collective-permute-start(bf16[192,256]{1,0:T(8,128)(2,1)S(1)} %collective-permute-done.11.refs_6_), channel_id=1, source_target_pairs={{0,1},{1,0},{2,3},{3,2},{4,5},{5,4},{6,7},{7,6},{8,9},{9,8},{10,11... | collective-permute-start | bytes 294920 | tf_op jit(solution)/shard_map/ppermute | solution.py:242
  11.1 6.5 %collective-permute-start.13 = (bf16[192,256]{1,0:T(8,128)(2,1)S(1)}, bf16[192,256]{1,0:T(8,128)(2,1)S(1)}, u32[]{:S(2)}, u32[]{:S(2)}) collective-permute-start(bf16[192,256]{1,0:T(8,128)(2,1)S(1)} %collective-permute-done.9.refs_4_), channel_id=1, source_target_pairs={{0,4},{4,0},{8,12},{12,8},{16,20},{20,16},{24,28},{28,24},{1,5},{5... | collective-permute-start | bytes 294920 | tf_op jit(solution)/shard_map/ppermute | solution.py:238
  11.1 6.5 %collective-permute-start.10 = (bf16[192,256]{1,0:T(8,128)(2,1)S(1)}, bf16[192,256]{1,0:T(8,128)(2,1)S(1)}, u32[]{:S(2)}, u32[]{:S(2)}) collective-permute-start(bf16[192,256]{1,0:T(8,128)(2,1)S(1)} %collective-permute-done.9.refs_4_), channel_id=1, source_target_pairs={{0,1},{1,0},{2,3},{3,2},{4,5},{5,4},{6,7},{7,6},{8,9},{9,8},{10,11... | collective-permute-start | bytes 294920 | tf_op jit(solution)/shard_map/ppermute | solution.py:242
  14.1 4.9 %collective-permute-start.5 = (bf16[192,256]{1,0:T(8,128)(2,1)S(1)}, bf16[192,256]{1,0:T(8,128)(2,1)S(1)}, u32[]{:S(2)}, u32[]{:S(2)}) collective-permute-start(bf16[192,256]{1,0:T(8,128)(2,1)S(1)} %collective-permute-done.refs_2_), channel_id=1, source_target_pairs={{0,4},{4,0},{8,12},{12,8},{16,20},{20,16},{24,28},{28,24},{1,5},{5... | collective-permute-start | bytes 294920 | tf_op jit(solution)/shard_map/ppermute | solution.py:238
  14.6 5.5 %collective-permute-start.3 = (bf16[192,256]{1,0:T(8,128)(2,1)S(1)}, bf16[192,256]{1,0:T(8,128)(2,1)S(1)}, u32[]{:S(2)}, u32[]{:S(2)}) collective-permute-start(bf16[192,256]{1,0:T(8,128)(2,1)S(1)} %collective-permute-done.refs_2_), channel_id=1, source_target_pairs={{0,12},{4,8},{8,4},{12,0},{16,28},{20,24},{24,20},{28,16},{1,13},{... | collective-permute-start | bytes 294920 | tf_op jit(solution)/shard_map/ppermute | solution.py:238
  15.9 5.3 %collective-permute-start.1 = (bf16[192,256]{1,0:T(8,128)(2,1)S(1)}, bf16[192,256]{1,0:T(8,128)(2,1)S(1)}, u32[]{:S(2)}, u32[]{:S(2)}) collective-permute-start(bf16[192,256]{1,0:T(8,128)(2,1)S(1)} %collective-permute-done.refs_2_), channel_id=1, source_target_pairs={{0,8},{4,12},{8,0},{12,4},{16,24},{20,28},{24,16},{28,20},{1,9},{5... | collective-permute-start | bytes 294920 | tf_op jit(solution)/shard_map/ppermute | solution.py:238
  17.6 4.8 %collective-permute-start.8 = (bf16[192,256]{1,0:T(8,128)(2,1)S(1)}, bf16[192,256]{1,0:T(8,128)(2,1)S(1)}, u32[]{:S(2)}, u32[]{:S(2)}) collective-permute-start(bf16[192,256]{1,0:T(8,128)(2,1)S(1)} %collective-permute-done.refs_2_), channel_id=1, source_target_pairs={{0,1},{1,0},{2,3},{3,2},{4,5},{5,4},{6,7},{7,6},{8,9},{9,8},{10,11... | collective-permute-start | bytes 294920 | tf_op jit(solution)/shard_map/ppermute | solution.py:242
  17.6 4.8 %collective-permute-start.14 = (bf16[192,256]{1,0:T(8,128)(2,1)S(1)}, bf16[192,256]{1,0:T(8,128)(2,1)S(1)}, u32[]{:S(2)}, u32[]{:S(2)}) collective-permute-start(bf16[192,256]{1,0:T(8,128)(2,1)S(1)} %collective-permute-done.13.refs_8_), channel_id=1, source_target_pairs={{0,1},{1,0},{2,3},{3,2},{4,5},{5,4},{6,7},{7,6},{8,9},{9,8},{10,11... | collective-permute-start | bytes 294920 | tf_op jit(solution)/shard_map/ppermute | solution.py:242
  18.9 3.9 %collective-permute-start.6 = (bf16[192,256]{1,0:T(8,128)(2,1)S(1)}, bf16[192,256]{1,0:T(8,128)(2,1)S(1)}, u32[]{:S(2)}, u32[]{:S(2)}) collective-permute-start(bf16[192,256]{1,0:T(8,128)(2,1)S(1)} %collective-permute-done.5.refs_6_), channel_id=1, source_target_pairs={{0,1},{1,0},{2,3},{3,2},{4,5},{5,4},{6,7},{7,6},{8,9},{9,8},{10,11... | collective-permute-start | bytes 294920 | tf_op jit(solution)/shard_map/ppermute | solution.py:242
  20.1 2.8 %collective-permute-start.4 = (bf16[192,256]{1,0:T(8,128)(2,1)S(1)}, bf16[192,256]{1,0:T(8,128)(2,1)S(1)}, u32[]{:S(2)}, u32[]{:S(2)}) collective-permute-start(bf16[192,256]{1,0:T(8,128)(2,1)S(1)} %collective-permute-done.3.refs_4_), channel_id=1, source_target_pairs={{0,1},{1,0},{2,3},{3,2},{4,5},{5,4},{6,7},{7,6},{8,9},{9,8},{10,11... | collective-permute-start | bytes 294920 | tf_op jit(solution)/shard_map/ppermute | solution.py:242
  21.2 1.7 %collective-permute-start.2 = (bf16[192,256]{1,0:T(8,128)(2,1)S(1)}, bf16[192,256]{1,0:T(8,128)(2,1)S(1)}, u32[]{:S(2)}, u32[]{:S(2)}) collective-permute-start(bf16[192,256]{1,0:T(8,128)(2,1)S(1)} %collective-permute-done.1.refs_2_), channel_id=1, source_target_pairs={{0,1},{1,0},{2,3},{3,2},{4,5},{5,4},{6,7},{7,6},{8,9},{9,8},{10,11... | collective-permute-start | bytes 294920 | tf_op jit(solution)/shard_map/ppermute | solution.py:242
  29.2 9.8 %collective-permute-start.19 = (bf16[128,512]{1,0:T(8,128)(2,1)S(1)}, bf16[128,512]{1,0:T(8,128)(2,1)S(1)}, u32[]{:S(2)}, u32[]{:S(2)}) collective-permute-start(bf16[128,512]{1,0:T(8,128)(2,1)S(1)} %attention.3.refs_0_), channel_id=1, source_target_pairs={{0,2},{1,3},{2,0},{3,1},{4,6},{5,7},{6,4},{7,5},{8,10},{9,11},{10,... | collective-permute-start | bytes 393224 | tf_op jit(solution)/shard_map/ppermute | solution.py:363
  30.8 7.7 %collective-permute-start.22 = (bf16[128,512]{1,0:T(8,128)(2,1)S(1)}, bf16[128,512]{1,0:T(8,128)(2,1)S(1)}, u32[]{:S(2)}, u32[]{:S(2)}) collective-permute-start(bf16[128,512]{1,0:T(8,128)(2,1)S(1)} %get-tuple-element.8.refs_0_), channel_id=1, source_target_pairs={{0,2},{1,3},{2,0},{3,1},{4,6},{5,7},{6,4},{7,5},{8,10},{9,11},{10,... | collective-permute-start | bytes 393224 | tf_op jit(solution)/shard_map/ppermute | solution.py:363
  34.3 6.5 %collective-permute-start.16 = (bf16[128,512]{1,0:T(8,128)(2,1)S(1)}, bf16[128,512]{1,0:T(8,128)(2,1)S(1)}, u32[]{:S(2)}, u32[]{:S(2)}) collective-permute-start(bf16[128,512]{1,0:T(8,128)(2,1)S(1)} %attention.2.refs_0_), channel_id=1, source_target_pairs={{0,2},{1,3},{2,0},{3,1},{4,6},{5,7},{6,4},{7,5},{8,10},{9,11},{10,... | collective-permute-start | bytes 393224 | tf_op jit(solution)/shard_map/ppermute | solution.py:363
  35.9 4.9 %collective-permute-start.21 = (bf16[128,512]{1,0:T(8,128)(2,1)S(1)}, bf16[128,512]{1,0:T(8,128)(2,1)S(1)}, u32[]{:S(2)}, u32[]{:S(2)}) collective-permute-start(bf16[128,512]{1,0:T(8,128)(2,1)S(1)} %get-tuple-element.8.refs_0_), channel_id=1, source_target_pairs={{0,1},{1,0},{2,3},{3,2},{4,5},{5,4},{6,7},{7,6},{8,9},{9,8},{10,11... | collective-permute-start | bytes 393224 | tf_op jit(solution)/shard_map/ppermute | solution.py:362
  38.5 2.8 %collective-permute-start.23 = (bf16[128,512]{1,0:T(8,128)(2,1)S(1)}, bf16[128,512]{1,0:T(8,128)(2,1)S(1)}, u32[]{:S(2)}, u32[]{:S(2)}) collective-permute-start(bf16[128,512]{1,0:T(8,128)(2,1)S(1)} %collective-permute-done.22.refs_2_), channel_id=1, source_target_pairs={{0,1},{1,0},{2,3},{3,2},{4,5},{5,4},{6,7},{7,6},{8,9},{9,8},{10,11... | collective-permute-start | bytes 393224 | tf_op jit(solution)/shard_map/ppermute | solution.py:364
  38.5 4.0 %collective-permute-start.18 = (bf16[128,512]{1,0:T(8,128)(2,1)S(1)}, bf16[128,512]{1,0:T(8,128)(2,1)S(1)}, u32[]{:S(2)}, u32[]{:S(2)}) collective-permute-start(bf16[128,512]{1,0:T(8,128)(2,1)S(1)} %attention.3.refs_0_), channel_id=1, source_target_pairs={{0,1},{1,0},{2,3},{3,2},{4,5},{5,4},{6,7},{7,6},{8,9},{9,8},{10,11... | collective-permute-start | bytes 393224 | tf_op jit(solution)/shard_map/ppermute | solution.py:362
  39.0 3.5 %collective-permute-start.20 = (bf16[128,512]{1,0:T(8,128)(2,1)S(1)}, bf16[128,512]{1,0:T(8,128)(2,1)S(1)}, u32[]{:S(2)}, u32[]{:S(2)}) collective-permute-start(bf16[128,512]{1,0:T(8,128)(2,1)S(1)} %collective-permute-done.19.refs_2_), channel_id=1, source_target_pairs={{0,1},{1,0},{2,3},{3,2},{4,5},{5,4},{6,7},{7,6},{8,9},{9,8},{10,11... | collective-permute-start | bytes 393224 | tf_op jit(solution)/shard_map/ppermute | solution.py:364
  40.8 2.8 %collective-permute-start.15 = (bf16[128,512]{1,0:T(8,128)(2,1)S(1)}, bf16[128,512]{1,0:T(8,128)(2,1)S(1)}, u32[]{:S(2)}, u32[]{:S(2)}) collective-permute-start(bf16[128,512]{1,0:T(8,128)(2,1)S(1)} %attention.2.refs_0_), channel_id=1, source_target_pairs={{0,1},{1,0},{2,3},{3,2},{4,5},{5,4},{6,7},{7,6},{8,9},{9,8},{10,11... | collective-permute-start | bytes 393224 | tf_op jit(solution)/shard_map/ppermute | solution.py:362
  40.8 2.8 %collective-permute-start.17 = (bf16[128,512]{1,0:T(8,128)(2,1)S(1)}, bf16[128,512]{1,0:T(8,128)(2,1)S(1)}, u32[]{:S(2)}, u32[]{:S(2)}) collective-permute-start(bf16[128,512]{1,0:T(8,128)(2,1)S(1)} %collective-permute-done.16.refs_2_), channel_id=1, source_target_pairs={{0,1},{1,0},{2,3},{3,2},{4,5},{5,4},{6,7},{7,6},{8,9},{9,8},{10,11... | collective-permute-start | bytes 393224 | tf_op jit(solution)/shard_map/ppermute | solution.py:364
  (6 other events, 97.8 us)

commit v4 on v3

--- a/solution.py
+++ b/solution.py
@@ -124,91 +124,95 @@
             out[span, column] = turn(product[span, column], angle).astype(jnp.bfloat16)
 
 
-def attend(block, first, chosen, query, key_value, out, scores):
+def attend(first, count, chosen, query, key_value, out, scores):
     heads = query.shape[1] // DH
     rows = heads * BLK
     tiles = NSEL // TILE
     lanes = TILE * BLK
     slot_of_lane = lax.broadcasted_iota(jnp.int32, (1, lanes), 1) // BLK
-    transposed = (((1,), (1,)), ((), ()))
-
-    def rows_of(place):
-        return pl.ds(pl.multiple_of(place * BLK, BLK), BLK)
-
-    def picked(tile, part):
-        return jnp.concatenate(
-            [key_value[rows_of(jnp.maximum(chosen[block, tile * TILE + slot], 0)), part] for slot in range(TILE)],
-            axis=0,
-        )
-
-    span = pl.ds(block * BLK, BLK)
-    mine = jnp.concatenate([query[span, head * DH : (head + 1) * DH] for head in range(heads)], axis=0)
-    own = rows_of(lax.axis_index("kv") * (query.shape[0] // BLK) + block)
-    highest = jnp.full((rows, lanes), MASKED, jnp.float32)
-    for tile in range(tiles):
-        score = lax.dot_general(mine, picked(tile, slice(0, DH)), transposed, preferred_element_type=jnp.float32)
-        bias = jnp.zeros((1, lanes), jnp.float32)
-        for slot in range(TILE):
-            missing = jnp.where(chosen[block, tile * TILE + slot] < 0, MASKED, 0.0)
-            bias = jnp.where(slot_of_lane == slot, missing, bias)
-        score = score + bias
-        scores[tile] = score
-        highest = jnp.maximum(highest, score)
-    diagonal = lax.dot_general(mine, key_value[own, :DH], transposed, preferred_element_type=jnp.float32)
     causal = (lax.broadcasted_iota(jnp.int32, (rows, BLK), 0) % BLK) >= lax.broadcasted_iota(
         jnp.int32, (rows, BLK), 1
     )
-    diagonal = jnp.where(causal, diagonal, MASKED)
-    top = jnp.maximum(jnp.max(highest, axis=1, keepdims=True), jnp.max(diagonal, axis=1, keepdims=True))
     ones = jnp.ones((lanes, DH), jnp.bfloat16)
-    probs = jnp.exp2((diagonal - top) * EXP2_SCALE).astype(jnp.bfloat16)
-    values = jnp.concatenate([key_value[own, DH:], ones[:BLK]], axis=1)
-    summed = jnp.dot(probs, values, preferred_element_type=jnp.float32)
-    for tile in range(tiles):
-        probs = jnp.exp2((scores[tile] - top) * EXP2_SCALE).astype(jnp.bfloat16)
-        values = jnp.concatenate([picked(tile, slice(DH, 2 * DH)), ones], axis=1)
-        summed += jnp.dot(probs, values, preferred_element_type=jnp.float32)
-    attention = (summed[:, :DH] / summed[:, DH:]).astype(jnp.bfloat16)
-    target = slice((block - first) * BLK, (block - first + 1) * BLK)
-    for head in range(heads):
-        out[target, head * DH : (head + 1) * DH] = attention[head * BLK : (head + 1) * BLK]
-
-
-def collect(shards, tags, key_value, sems, blocks, sharing):
-    kv_index = lax.axis_index("kv")
-    member = lax.axis_index("tp") % sharing
-    held = blocks // sharing
-    span = held * BLK
-
-    def moves(act):
-        for number, (shard, (bits, sibling)) in enumerate(zip(shards, tags)):
-            source = kv_index ^ bits
-            place = pl.multiple_of((source * blocks + (member ^ sibling) * held) * BLK, BLK)
-            copy = pltpu.make_async_copy(shard, key_value.at[pl.ds(place, span)], sems.at[number])
-
-            @pl.when(source <= kv_index)
-            def _():
-                act(copy)
-
-    moves(lambda copy: copy.start())
-    moves(lambda copy: copy.wait())
-
-
-def collect_kernel(*refs, tags, blocks, sharing):
-    collect(refs[: len(tags)], tags, refs[-2], refs[-1], blocks, sharing)
+
+    def rows_of(place):
+        return pl.ds(pl.multiple_of(place * BLK, BLK), BLK)
+
+    def own(block):
+        return rows_of(lax.axis_index("kv") * (query.shape[0] // BLK) + block)
+
+    table = chosen[...]
+    picks = {
+        block: [lax.squeeze(lax.slice(table, (block, slot), (block + 1, slot + 1)), (0, 1)) for slot in range(NSEL)]
+        for block in range(first, first + count)
+    }
+
+    def picked(block, tile, part):
+        places = [jnp.maximum(pick, 0) for pick in picks[block][tile * TILE : (tile + 1) * TILE]]
+        return jnp.concatenate([key_value[rows_of(place), part] for place in places], axis=0)
+
+    def products(left, right):
+        return lax.dot_general(left, right, (((1,), (1,)), ((), ())), preferred_element_type=jnp.float32)
+
+    def weigh(score, top, values, width):
+        probs = jnp.exp2((score - top) * EXP2_SCALE).astype(jnp.bfloat16)
+        return jnp.dot(probs, jnp.concatenate([values, ones[:width]], axis=1), preferred_element_type=jnp.float32)
+
+    def queries(block):
+        span = slice(block * BLK, (block + 1) * BLK)
+        return jnp.concatenate([query[span, head * DH : (head + 1) * DH] for head in range(heads)], axis=0)
+
+    diagonals = [
+        jnp.where(causal, products(queries(block), key_value[own(block), :DH]), MASKED)
+        for block in range(first, first + count)
+    ]
+    mine = highest = top = summed = None
+    for step in range(count + 1):
+        block = first + step
+        side = step % 2
+        if step < count:
+            mine = queries(block)
+            highest = None
+        for tile in range(tiles):
+            if step < count:
+                bias = jnp.zeros((1, lanes), jnp.float32)
+                for slot in range(TILE):
+                    missing = jnp.where(picks[block][tile * TILE + slot] < 0, MASKED, 0.0)
+                    bias = jnp.where(slot_of_lane == slot, missing, bias)
+                score = products(mine, picked(block, tile, slice(0, DH))) + bias
+                scores[side, tile] = score
+                largest = jnp.maximum(score[:, : lanes // 2], score[:, lanes // 2 :])
+                highest = largest if highest is None else jnp.maximum(highest, largest)
+            if step > 0:
+                product = weigh(scores[1 - side, tile], top, picked(block - 1, tile, slice(DH, 2 * DH)), lanes)
+                summed = product if summed is None else summed + product
+        if step > 0:
+            summed += weigh(diagonals[step - 1], top, key_value[own(block - 1), DH:], BLK)
+            attention = (summed[:, :DH] / summed[:, DH:]).astype(jnp.bfloat16)
+            target = slice((step - 1) * BLK, step * BLK)
+            for head in range(heads):
+                out[target, head * DH : (head + 1) * DH] = attention[head * BLK : (head + 1) * BLK]
+        if step < count:
+            top = jnp.maximum(
+                jnp.max(highest, axis=1, keepdims=True), jnp.max(diagonals[step], axis=1, keepdims=True)
+            )
+            summed = None
 
 
 def first_attention_kernel(*refs, first, count, tags, sharing):
     chosen, query = refs[:2]
-    out, key_value, scores, sems = refs[-4:]
-    collect(refs[2 : 2 + len(tags)], tags, key_value, sems, query.shape[0] // BLK, sharing)
-    for block in range(first, first + count):
-        attend(block, first, chosen, query, key_value, out, scores)
+    out, key_value, scores = refs[-3:]
+    blocks = query.shape[0] // BLK
+    held = blocks // sharing
+    member = lax.axis_index("tp") % sharing
+    for shard, (bits, sibling) in zip(refs[2 : 2 + len(tags)], tags):
+        place = ((lax.axis_index("kv") ^ bits) * blocks + (member ^ sibling) * held) * BLK
+        key_value[pl.ds(pl.multiple_of(place, BLK), held * BLK)] = shard[...]
+    attend(first, count, chosen, query, key_value, out, scores)
 
 
 def attention_kernel(chosen, query, key_value, out, scores, *, first, count):
-    for block in range(first, first + count):
-        attend(block, first, chosen, query, key_value, out, scores)
+    attend(first, count, chosen, query, key_value, out, scores)
 
 
 def project_kernel(*refs, pieces, first, relative):
@@ -278,7 +282,7 @@
             pltpu.VMEM((width, DH), jnp.bfloat16),
             pltpu.VMEM(coarse.shape, jnp.float32),
             pltpu.VMEM(fine.shape, jnp.float32),
-            pltpu.SemaphoreType.DMA((4, 3)),
+            pltpu.SemaphoreType.DMA((2, 3)),
             pltpu.SemaphoreType.DMA((2,)),
         ],
         cost_estimate=pl.CostEstimate(
@@ -303,18 +307,6 @@
 
     if small:
         shards = spread_small(own_part, kv_count, tp_count)
-        late = [tag for tag in shards if tag[0] > 4]
-        early = [tag for tag in shards if tag not in late]
-        key_value = pl.pallas_call(
-            functools.partial(collect_kernel, tags=early, blocks=local_blocks, sharing=sharing),
-            out_shape=pltpu.VMEM((kv_count * rows, 2 * DH), jnp.bfloat16),
-            in_specs=[VMEM] * len(early),
-            out_specs=VMEM,
-            scratch_shapes=[pltpu.SemaphoreType.DMA((len(early),))],
-            compiler_params=room(2),
-            name="collect",
-        )(*[keep(shards[tag]) for tag in early])
-        key_value = keep(key_value)
     else:
         groups = [[g * sharing + i for i in range(sharing)] for g in range(KVH)]
         whole = lax.all_gather(own_part, "tp", axis=0, tiled=True, axis_index_groups=groups)
@@ -322,9 +314,10 @@
 
     splits = 3
     per = local_blocks // splits
-    scores = pltpu.VMEM((NSEL // TILE, own_heads * BLK, TILE * BLK), jnp.float32)
+    scores = pltpu.VMEM((2, NSEL // TILE, own_heads * BLK, TILE * BLK), jnp.float32)
     result = None
     w_out = keep(w_out)
+    chosen = keep(chosen)
     for split in range(splits):
         first = split * per
         shape = pltpu.VMEM((per * BLK, own_width), jnp.bfloat16)
@@ -335,22 +328,22 @@
         )
         if small and split == 0:
             attention, key_value = pl.pallas_call(
-                functools.partial(first_attention_kernel, first=first, count=per, tags=late, sharing=sharing),
+                functools.partial(first_attention_kernel, first=first, count=per, tags=tuple(shards), sharing=sharing),
                 out_shape=[shape, pltpu.VMEM((kv_count * rows, 2 * DH), jnp.bfloat16)],
-                in_specs=[SMEM, VMEM] + [VMEM] * (len(late) + 1),
+                in_specs=[VMEM, VMEM] + [VMEM] * len(shards),
                 out_specs=[VMEM, VMEM],
-                input_output_aliases={len(late) + 2: 1},
-                scratch_shapes=[scores, pltpu.SemaphoreType.DMA((len(late),))],
+                scratch_shapes=[scores],
                 cost_estimate=cost,
                 compiler_params=room(12),
                 name="first_attention",
-            )(chosen, query, *[keep(shards[tag]) for tag in late], key_value)
+            )(chosen, query, *[keep(shard) for shard in shards.values()])
+            key_value = keep(key_value)
             key_value = keep(key_value)
         else:
             call = pl.pallas_call(
                 functools.partial(attention_kernel, first=first, count=per),
                 out_shape=shape,
-                in_specs=[SMEM, VMEM, VMEM],
+                in_specs=[VMEM, VMEM, VMEM],
                 out_specs=VMEM,
                 scratch_shapes=[scores],
                 cost_estimate=cost,

time: 44.9 us -> 41.8 us (0.931)
  Pallas kernels: 16.4 us -> 12.4 us
  waiting for transfers between devices: 11.5 us -> 12.6 us
    pallas_call x2, Pallas kernels: 5.99 us -> 3.79 us  [body(): attention = call(chosen, query, key_value)]
    pallas_call x1, Pallas kernels: 3.09 us -> 1.95 us  [body(): pl.pallas_call(functools.partial(first_attention_kernel, first=first, cou...]
    ppermute x3, waiting for transfers between devices: 4.41 us -> 5.46 us  [body(): lax.ppermute(attention, 'tp', [(i, i ^ 2) for i in range(tp_count)])]
  transfers between devices with their start and end apart: 24 -> 24, of which waited for: 7 -> 8; matrix products, arithmetic and copies ran while one was open for 0% -> 0% of each run, Pallas kernels for 15% -> 13%
where the time goes in v4:
time: 41.8 us; the launch traced here: 41.6 us
  starting transfers between devices  16.4 us (39%)
  waiting for transfers between devices  12.6 us (30%)
  Pallas kernels  12.4 us (30%)
    ppermute x7, starting transfers between devices, spread_small(): shards[bits] = lax.ppermute(shards[bits ^ hop], 'kv', pairs)  10.7 us
    ppermute x7, waiting for transfers between devices, spread_small(): shards[bits] = lax.ppermute(shards[bits ^ hop], 'kv', pairs)  7.05 us
    ppermute x3, waiting for transfers between devices, body(): lax.ppermute(attention, 'tp', [(i, i ^ 2) for i in range(tp_count)])  5.46 us
    pallas_call x2, Pallas kernels, body(): attention = call(chosen, query, key_value)  3.79 us
    ppermute x3, starting transfers between devices, body(): lax.ppermute(attention, 'tp', [(i, i ^ 2) for i in range(tp_count)])  3.65 us
    pallas_call x3, Pallas kernels, body(): result = call(*parts, w_out, *earlier)  3.35 us
    pallas_call x1, Pallas kernels, body(): pl.pallas_call(key_value_kernel, out_shape=pltpu.VMEM((part_rows, 2 * DH)...  2.16 us
    pallas_call x1, Pallas kernels, body(): pl.pallas_call(functools.partial(first_attention_kernel, first=first, cou...  1.95 us
  transfers between devices with their start and end apart: 24, of which 8 were waited for; matrix products, arithmetic and copies ran while one was open for 0% of the time, Pallas kernels for 13%

profile of v4, /device:TPU:0, one launch (start us, length us, event | category | flops | bytes accessed | tf_op | source)
XLA Modules:
  0.0 41.6 jit_solution(15642587694297560234)
XLA Ops:
  0.0 2.2 %key_value.1.refs_2_ = bf16[192,256]{1,0:T(8,128)(2,1)S(1)} custom-call(bf16[384,2048]{1,0:T(8,128)(2,1)} %tokens.3, bf16[2048,256]{1,0:T(8,128)(2,1)} %w_key.1, bf16[2048,256]{1,0:T(8,128)(2,1)} %w_value.1, f32[2,48,128]{2,1,0:T(8,128)} %constant.4.clone.coarse.coarse_hbm, f32[2,64,128]{2,1,0:T(8,128)} %constant.5.clone.fine.fine_hbm), custom_call_target="tpu_custom_call" | custom-call | flops 201326592 | bytes 1835008 | tf_op jit(solution)/shard_map/key_value/pallas_call | solution.py:274
  2.2 3.1 %collective-permute-start.5 = (bf16[192,256]{1,0:T(8,128)(2,1)S(1)}, bf16[192,256]{1,0:T(8,128)(2,1)S(1)}, u32[]{:S(2)}, u32[]{:S(2)}) collective-permute-start(bf16[192,256]{1,0:T(8,128)(2,1)S(1)} %key_value.1.refs_2_), channel_id=1, source_target_pairs={{0,4},{4,0},{8,12},{12,8},{16,20},{20,16},{24,28},{28,24},{1,5},{5... | collective-permute-start | bytes 294920 | tf_op jit(solution)/shard_map/ppermute | solution.py:242
  5.3 1.6 %collective-permute-start.3 = (bf16[192,256]{1,0:T(8,128)(2,1)S(1)}, bf16[192,256]{1,0:T(8,128)(2,1)S(1)}, u32[]{:S(2)}, u32[]{:S(2)}) collective-permute-start(bf16[192,256]{1,0:T(8,128)(2,1)S(1)} %key_value.1.refs_2_), channel_id=1, source_target_pairs={{0,8},{4,12},{8,0},{12,4},{16,24},{20,28},{24,16},{28,20},{1,9},{5... | collective-permute-start | bytes 294920 | tf_op jit(solution)/shard_map/ppermute | solution.py:242
  6.8 2.6 %collective-permute-start.1 = (bf16[192,256]{1,0:T(8,128)(2,1)S(1)}, bf16[192,256]{1,0:T(8,128)(2,1)S(1)}, u32[]{:S(2)}, u32[]{:S(2)}) collective-permute-start(bf16[192,256]{1,0:T(8,128)(2,1)S(1)} %key_value.1.refs_2_), channel_id=1, source_target_pairs={{0,16},{4,20},{8,24},{12,28},{16,0},{20,4},{24,8},{28,12},{1,17},{... | collective-permute-start | bytes 294920 | tf_op jit(solution)/shard_map/ppermute | solution.py:242
  9.9 0.9 %collective-permute-done.3.refs_6_ = bf16[192,256]{1,0:T(8,128)(2,1)S(1)} collective-permute-done((bf16[192,256]{1,0:T(8,128)(2,1)S(1)}, bf16[192,256]{1,0:T(8,128)(2,1)S(1)}, u32[]{:S(2)}, u32[]{:S(2)}) %collective-permute-start.3) | collective-permute-done | bytes 98336 | tf_op jit(solution)/shard_map/ppermute | solution.py:242
  10.9 3.0 %collective-permute-done.1.refs_4_ = bf16[192,256]{1,0:T(8,128)(2,1)S(1)} collective-permute-done((bf16[192,256]{1,0:T(8,128)(2,1)S(1)}, bf16[192,256]{1,0:T(8,128)(2,1)S(1)}, u32[]{:S(2)}, u32[]{:S(2)}) %collective-permute-start.1) | collective-permute-done | bytes 98336 | tf_op jit(solution)/shard_map/ppermute | solution.py:242
  14.4 1.3 %collective-permute-start.11 = (bf16[192,256]{1,0:T(8,128)(2,1)S(1)}, bf16[192,256]{1,0:T(8,128)(2,1)S(1)}, u32[]{:S(2)}, u32[]{:S(2)}) collective-permute-start(bf16[192,256]{1,0:T(8,128)(2,1)S(1)} %collective-permute-done.1.refs_4_), channel_id=1, source_target_pairs={{0,12},{4,8},{8,4},{12,0},{16,28},{20,24},{24,20},{28,16},{1,13},{... | collective-permute-start | bytes 294920 | tf_op jit(solution)/shard_map/ppermute | solution.py:242
  15.7 1.7 %collective-permute-start.9 = (bf16[192,256]{1,0:T(8,128)(2,1)S(1)}, bf16[192,256]{1,0:T(8,128)(2,1)S(1)}, u32[]{:S(2)}, u32[]{:S(2)}) collective-permute-start(bf16[192,256]{1,0:T(8,128)(2,1)S(1)} %collective-permute-done.1.refs_4_), channel_id=1, source_target_pairs={{0,8},{4,12},{8,0},{12,4},{16,24},{20,28},{24,16},{28,20},{1,9},{5... | collective-permute-start | bytes 294920 | tf_op jit(solution)/shard_map/ppermute | solution.py:242
  17.9 0.8 %collective-permute-done.13.refs_16_ = bf16[192,256]{1,0:T(8,128)(2,1)S(1)} collective-permute-done((bf16[192,256]{1,0:T(8,128)(2,1)S(1)}, bf16[192,256]{1,0:T(8,128)(2,1)S(1)}, u32[]{:S(2)}, u32[]{:S(2)}) %collective-permute-start.13) | collective-permute-done | bytes 98336 | tf_op jit(solution)/shard_map/ppermute | solution.py:242
  18.7 1.2 %collective-permute-done.11.refs_14_ = bf16[192,256]{1,0:T(8,128)(2,1)S(1)} collective-permute-done((bf16[192,256]{1,0:T(8,128)(2,1)S(1)}, bf16[192,256]{1,0:T(8,128)(2,1)S(1)}, u32[]{:S(2)}, u32[]{:S(2)}) %collective-permute-start.11) | collective-permute-done | bytes 98336 | tf_op jit(solution)/shard_map/ppermute | solution.py:242
  19.9 1.1 %collective-permute-done.9.refs_12_ = bf16[192,256]{1,0:T(8,128)(2,1)S(1)} collective-permute-done((bf16[192,256]{1,0:T(8,128)(2,1)S(1)}, bf16[192,256]{1,0:T(8,128)(2,1)S(1)}, u32[]{:S(2)}, u32[]{:S(2)}) %collective-permute-start.9) | collective-permute-done | bytes 98336 | tf_op jit(solution)/shard_map/ppermute | solution.py:242
  21.0 1.1 %query.1.refs_1_ = bf16[384,512]{1,0:T(8,128)(2,1)S(1)} custom-call(bf16[384,2048]{1,0:T(8,128)(2,1)S(1)} %copy-done.1, bf16[2048,512]{1,0:T(8,128)(2,1)S(1)} %copy-done.2, f32[2,48,128]{2,1,0:T(8,128)S(1)} %copy-done.4, f32[2,64,128]{2,1,0:T(8,128)S(1)} %copy-done.3), custom_call_target="tpu_custom_call" | custom-call | flops 805306368 | bytes 3670016 | tf_op jit(solution)/shard_map/query/pallas_call | solution.py:295
  22.3 2.0 %first_attention.1 = (bf16[128,512]{1,0:T(8,128)(2,1)S(1)}, bf16[3072,256]{1,0:T(8,128)(2,1)S(1)}) custom-call(s32[6,32]{1,0:T(8,128)S(1)} %copy-done.5, bf16[384,512]{1,0:T(8,128)(2,1)S(1)} %query.1.refs_1_, bf16[192,256]{1,0:T(8,128)(2,1)S(1)} %key_value.1.refs_2_, bf16[192,256]{1,0:T(8,128)(2,1)S(1)} %collective-permute-done.refs_3_, ...), custom_call_target="tpu_custom_call" | custom-call | flops 553648128 | bytes 131072 | tf_op jit(solution)/shard_map/first_attention/pallas_call | solution.py:330
  24.3 1.9 %attention.3.refs_0_ = bf16[128,512]{1,0:T(8,128)(2,1)S(1)} custom-call(s32[6,32]{1,0:T(8,128)S(1)} %copy-done.5, bf16[384,512]{1,0:T(8,128)(2,1)S(1)} %query.1.refs_1_, bf16[3072,256]{1,0:T(8,128)(2,1)S(1)} %get-tuple-element.7.key_value), custom_call_target="tpu_custom_call" | custom-call | flops 553648128 | bytes 131072 | tf_op jit(solution)/shard_map/attention/pallas_call | solution.py:353
  26.2 1.6 %collective-permute-start.19 = (bf16[128,512]{1,0:T(8,128)(2,1)S(1)}, bf16[128,512]{1,0:T(8,128)(2,1)S(1)}, u32[]{:S(2)}, u32[]{:S(2)}) collective-permute-start(bf16[128,512]{1,0:T(8,128)(2,1)S(1)} %attention.3.refs_0_), channel_id=1, source_target_pairs={{0,2},{1,3},{2,0},{3,1},{4,6},{5,7},{6,4},{7,5},{8,10},{9,11},{10,... | collective-permute-start | bytes 393224 | tf_op jit(solution)/shard_map/ppermute | solution.py:356
  27.7 0.5 %collective-permute-start.22 = (bf16[128,512]{1,0:T(8,128)(2,1)S(1)}, bf16[128,512]{1,0:T(8,128)(2,1)S(1)}, u32[]{:S(2)}, u32[]{:S(2)}) collective-permute-start(bf16[128,512]{1,0:T(8,128)(2,1)S(1)} %get-tuple-element.8.refs_0_), channel_id=1, source_target_pairs={{0,2},{1,3},{2,0},{3,1},{4,6},{5,7},{6,4},{7,5},{8,10},{9,11},{10,... | collective-permute-start | bytes 393224 | tf_op jit(solution)/shard_map/ppermute | solution.py:356
  28.3 1.9 %attention.2.refs_0_ = bf16[128,512]{1,0:T(8,128)(2,1)S(1)} custom-call(s32[6,32]{1,0:T(8,128)S(1)} %copy-done.5, bf16[384,512]{1,0:T(8,128)(2,1)S(1)} %query.1.refs_1_, bf16[3072,256]{1,0:T(8,128)(2,1)S(1)} %get-tuple-element.7.key_value), custom_call_target="tpu_custom_call" | custom-call | flops 553648128 | bytes 131072 | tf_op jit(solution)/shard_map/attention/pallas_call | solution.py:353
  30.2 1.6 %collective-permute-start.16 = (bf16[128,512]{1,0:T(8,128)(2,1)S(1)}, bf16[128,512]{1,0:T(8,128)(2,1)S(1)}, u32[]{:S(2)}, u32[]{:S(2)}) collective-permute-start(bf16[128,512]{1,0:T(8,128)(2,1)S(1)} %attention.2.refs_0_), channel_id=1, source_target_pairs={{0,2},{1,3},{2,0},{3,1},{4,6},{5,7},{6,4},{7,5},{8,10},{9,11},{10,... | collective-permute-start | bytes 393224 | tf_op jit(solution)/shard_map/ppermute | solution.py:356
  31.7 3.7 %collective-permute-done.22.refs_2_ = bf16[128,512]{1,0:T(8,128)(2,1)S(1)} collective-permute-done((bf16[128,512]{1,0:T(8,128)(2,1)S(1)}, bf16[128,512]{1,0:T(8,128)(2,1)S(1)}, u32[]{:S(2)}, u32[]{:S(2)}) %collective-permute-start.22) | collective-permute-done | bytes 131104 | tf_op jit(solution)/shard_map/ppermute | solution.py:356
  35.9 1.8 %collective-permute-done.16.refs_2_ = bf16[128,512]{1,0:T(8,128)(2,1)S(1)} collective-permute-done((bf16[128,512]{1,0:T(8,128)(2,1)S(1)}, bf16[128,512]{1,0:T(8,128)(2,1)S(1)}, u32[]{:S(2)}, u32[]{:S(2)}) %collective-permute-start.16) | collective-permute-done | bytes 131104 | tf_op jit(solution)/shard_map/ppermute | solution.py:356
  37.7 0.5 %collective-permute-start.17 = (bf16[128,512]{1,0:T(8,128)(2,1)S(1)}, bf16[128,512]{1,0:T(8,128)(2,1)S(1)}, u32[]{:S(2)}, u32[]{:S(2)}) collective-permute-start(bf16[128,512]{1,0:T(8,128)(2,1)S(1)} %collective-permute-done.16.refs_2_), channel_id=1, source_target_pairs={{0,1},{1,0},{2,3},{3,2},{4,5},{5,4},{6,7},{7,6},{8,9},{9,8},{10,11... | collective-permute-start | bytes 393224 | tf_op jit(solution)/shard_map/ppermute | solution.py:357
  38.2 1.1 %project.3.refs_5_ = bf16[384,512]{1,0:T(8,128)(2,1)} custom-call(bf16[128,512]{1,0:T(8,128)(2,1)S(1)} %get-tuple-element.8.refs_0_, bf16[128,512]{1,0:T(8,128)(2,1)S(1)} %collective-permute-done.21.refs_1_, bf16[128,512]{1,0:T(8,128)(2,1)S(1)} %collective-permute-done.22.refs_2_, bf16[128,512]{1,0:T(8,128)(2,1)S(1)} %collective-permute-done.23.refs_3_, ...), custom_call_target="tpu_custom_call" | custom-call | flops 268435456 | tf_op jit(solution)/shard_map/project/pallas_call | solution.py:379
  39.4 1.1 %project.4.refs_5_ = bf16[384,512]{1,0:T(8,128)(2,1)} custom-call(bf16[128,512]{1,0:T(8,128)(2,1)S(1)} %attention.3.refs_0_, bf16[128,512]{1,0:T(8,128)(2,1)S(1)} %collective-permute-done.18.refs_1_, bf16[128,512]{1,0:T(8,128)(2,1)S(1)} %collective-permute-done.19.refs_2_, ...), custom_call_target="tpu_custom_call", output_to_operand_aliasing={{}: (5, {})} | custom-call | flops 268435456 | tf_op jit(solution)/shard_map/project/pallas_call | solution.py:379
  40.5 1.1 %project.5 = bf16[384,512]{1,0:T(8,128)(2,1)} custom-call(bf16[128,512]{1,0:T(8,128)(2,1)S(1)} %attention.2.refs_0_, bf16[128,512]{1,0:T(8,128)(2,1)S(1)} %collective-permute-done.15.refs_1_, bf16[128,512]{1,0:T(8,128)(2,1)S(1)} %collective-permute-done.16.refs_2_, ...), custom_call_target="tpu_custom_call", output_to_operand_aliasing={{}: (5, {})} | custom-call | flops 268435456 | tf_op jit(solution)/shard_map/project/pallas_call | solution.py:379
  (44 shorter events, 2.2 us)
Async XLA Ops:
  2.2 7.2 %collective-permute-start.5 = (bf16[192,256]{1,0:T(8,128)(2,1)S(1)}, bf16[192,256]{1,0:T(8,128)(2,1)S(1)}, u32[]{:S(2)}, u32[]{:S(2)}) collective-permute-start(bf16[192,256]{1,0:T(8,128)(2,1)S(1)} %key_value.1.refs_2_), channel_id=1, source_target_pairs={{0,4},{4,0},{8,12},{12,8},{16,20},{20,16},{24,28},{28,24},{1,5},{5... | collective-permute-start | bytes 294920 | tf_op jit(solution)/shard_map/ppermute | solution.py:242
  5.3 5.6 %collective-permute-start.3 = (bf16[192,256]{1,0:T(8,128)(2,1)S(1)}, bf16[192,256]{1,0:T(8,128)(2,1)S(1)}, u32[]{:S(2)}, u32[]{:S(2)}) collective-permute-start(bf16[192,256]{1,0:T(8,128)(2,1)S(1)} %key_value.1.refs_2_), channel_id=1, source_target_pairs={{0,8},{4,12},{8,0},{12,4},{16,24},{20,28},{24,16},{28,20},{1,9},{5... | collective-permute-start | bytes 294920 | tf_op jit(solution)/shard_map/ppermute | solution.py:242
  6.8 7.0 %collective-permute-start.1 = (bf16[192,256]{1,0:T(8,128)(2,1)S(1)}, bf16[192,256]{1,0:T(8,128)(2,1)S(1)}, u32[]{:S(2)}, u32[]{:S(2)}) collective-permute-start(bf16[192,256]{1,0:T(8,128)(2,1)S(1)} %key_value.1.refs_2_), channel_id=1, source_target_pairs={{0,16},{4,20},{8,24},{12,28},{16,0},{20,4},{24,8},{28,12},{1,17},{... | collective-permute-start | bytes 294920 | tf_op jit(solution)/shard_map/ppermute | solution.py:242
  9.4 5.0 %collective-permute-start = (bf16[192,256]{1,0:T(8,128)(2,1)S(1)}, bf16[192,256]{1,0:T(8,128)(2,1)S(1)}, u32[]{:S(2)}, u32[]{:S(2)}) collective-permute-start(bf16[192,256]{1,0:T(8,128)(2,1)S(1)} %key_value.1.refs_2_), channel_id=1, source_target_pairs={{0,1},{1,0},{2,3},{3,2},{4,5},{5,4},{6,7},{7,6},{8,9},{9,8},{10,11... | collective-permute-start | bytes 294920 | tf_op jit(solution)/shard_map/ppermute | solution.py:246
  9.4 6.3 %collective-permute-start.6 = (bf16[192,256]{1,0:T(8,128)(2,1)S(1)}, bf16[192,256]{1,0:T(8,128)(2,1)S(1)}, u32[]{:S(2)}, u32[]{:S(2)}) collective-permute-start(bf16[192,256]{1,0:T(8,128)(2,1)S(1)} %collective-permute-done.5.refs_8_), channel_id=1, source_target_pairs={{0,1},{1,0},{2,3},{3,2},{4,5},{5,4},{6,7},{7,6},{8,9},{9,8},{10,11... | collective-permute-start | bytes 294920 | tf_op jit(solution)/shard_map/ppermute | solution.py:246
  10.9 6.5 %collective-permute-start.7 = (bf16[192,256]{1,0:T(8,128)(2,1)S(1)}, bf16[192,256]{1,0:T(8,128)(2,1)S(1)}, u32[]{:S(2)}, u32[]{:S(2)}) collective-permute-start(bf16[192,256]{1,0:T(8,128)(2,1)S(1)} %collective-permute-done.3.refs_6_), channel_id=1, source_target_pairs={{0,4},{4,0},{8,12},{12,8},{16,20},{20,16},{24,28},{28,24},{1,5},{5... | collective-permute-start | bytes 294920 | tf_op jit(solution)/shard_map/ppermute | solution.py:242
  10.9 6.5 %collective-permute-start.4 = (bf16[192,256]{1,0:T(8,128)(2,1)S(1)}, bf16[192,256]{1,0:T(8,128)(2,1)S(1)}, u32[]{:S(2)}, u32[]{:S(2)}) collective-permute-start(bf16[192,256]{1,0:T(8,128)(2,1)S(1)} %collective-permute-done.3.refs_6_), channel_id=1, source_target_pairs={{0,1},{1,0},{2,3},{3,2},{4,5},{5,4},{6,7},{7,6},{8,9},{9,8},{10,11... | collective-permute-start | bytes 294920 | tf_op jit(solution)/shard_map/ppermute | solution.py:246
  13.9 4.9 %collective-permute-start.13 = (bf16[192,256]{1,0:T(8,128)(2,1)S(1)}, bf16[192,256]{1,0:T(8,128)(2,1)S(1)}, u32[]{:S(2)}, u32[]{:S(2)}) collective-permute-start(bf16[192,256]{1,0:T(8,128)(2,1)S(1)} %collective-permute-done.1.refs_4_), channel_id=1, source_target_pairs={{0,4},{4,0},{8,12},{12,8},{16,20},{20,16},{24,28},{28,24},{1,5},{5... | collective-permute-start | bytes 294920 | tf_op jit(solution)/shard_map/ppermute | solution.py:242
  14.4 5.5 %collective-permute-start.11 = (bf16[192,256]{1,0:T(8,128)(2,1)S(1)}, bf16[192,256]{1,0:T(8,128)(2,1)S(1)}, u32[]{:S(2)}, u32[]{:S(2)}) collective-permute-start(bf16[192,256]{1,0:T(8,128)(2,1)S(1)} %collective-permute-done.1.refs_4_), channel_id=1, source_target_pairs={{0,12},{4,8},{8,4},{12,0},{16,28},{20,24},{24,20},{28,16},{1,13},{... | collective-permute-start | bytes 294920 | tf_op jit(solution)/shard_map/ppermute | solution.py:242
  15.7 5.3 %collective-permute-start.9 = (bf16[192,256]{1,0:T(8,128)(2,1)S(1)}, bf16[192,256]{1,0:T(8,128)(2,1)S(1)}, u32[]{:S(2)}, u32[]{:S(2)}) collective-permute-start(bf16[192,256]{1,0:T(8,128)(2,1)S(1)} %collective-permute-done.1.refs_4_), channel_id=1, source_target_pairs={{0,8},{4,12},{8,0},{12,4},{16,24},{20,28},{24,16},{28,20},{1,9},{5... | collective-permute-start | bytes 294920 | tf_op jit(solution)/shard_map/ppermute | solution.py:242
  17.4 4.8 %collective-permute-start.2 = (bf16[192,256]{1,0:T(8,128)(2,1)S(1)}, bf16[192,256]{1,0:T(8,128)(2,1)S(1)}, u32[]{:S(2)}, u32[]{:S(2)}) collective-permute-start(bf16[192,256]{1,0:T(8,128)(2,1)S(1)} %collective-permute-done.1.refs_4_), channel_id=1, source_target_pairs={{0,1},{1,0},{2,3},{3,2},{4,5},{5,4},{6,7},{7,6},{8,9},{9,8},{10,11... | collective-permute-start | bytes 294920 | tf_op jit(solution)/shard_map/ppermute | solution.py:246
  17.4 4.8 %collective-permute-start.8 = (bf16[192,256]{1,0:T(8,128)(2,1)S(1)}, bf16[192,256]{1,0:T(8,128)(2,1)S(1)}, u32[]{:S(2)}, u32[]{:S(2)}) collective-permute-start(bf16[192,256]{1,0:T(8,128)(2,1)S(1)} %collective-permute-done.7.refs_10_), channel_id=1, source_target_pairs={{0,1},{1,0},{2,3},{3,2},{4,5},{5,4},{6,7},{7,6},{8,9},{9,8},{10,11... | collective-permute-start | bytes 294920 | tf_op jit(solution)/shard_map/ppermute | solution.py:246
  18.7 3.5 %collective-permute-start.14 = (bf16[192,256]{1,0:T(8,128)(2,1)S(1)}, bf16[192,256]{1,0:T(8,128)(2,1)S(1)}, u32[]{:S(2)}, u32[]{:S(2)}) collective-permute-start(bf16[192,256]{1,0:T(8,128)(2,1)S(1)} %collective-permute-done.13.refs_16_), channel_id=1, source_target_pairs={{0,1},{1,0},{2,3},{3,2},{4,5},{5,4},{6,7},{7,6},{8,9},{9,8},{10,11... | collective-permute-start | bytes 294920 | tf_op jit(solution)/shard_map/ppermute | solution.py:246
  19.9 2.3 %collective-permute-start.12 = (bf16[192,256]{1,0:T(8,128)(2,1)S(1)}, bf16[192,256]{1,0:T(8,128)(2,1)S(1)}, u32[]{:S(2)}, u32[]{:S(2)}) collective-permute-start(bf16[192,256]{1,0:T(8,128)(2,1)S(1)} %collective-permute-done.11.refs_14_), channel_id=1, source_target_pairs={{0,1},{1,0},{2,3},{3,2},{4,5},{5,4},{6,7},{7,6},{8,9},{9,8},{10,11... | collective-permute-start | bytes 294920 | tf_op jit(solution)/shard_map/ppermute | solution.py:246
  21.0 1.3 %collective-permute-start.10 = (bf16[192,256]{1,0:T(8,128)(2,1)S(1)}, bf16[192,256]{1,0:T(8,128)(2,1)S(1)}, u32[]{:S(2)}, u32[]{:S(2)}) collective-permute-start(bf16[192,256]{1,0:T(8,128)(2,1)S(1)} %collective-permute-done.9.refs_12_), channel_id=1, source_target_pairs={{0,1},{1,0},{2,3},{3,2},{4,5},{5,4},{6,7},{7,6},{8,9},{9,8},{10,11... | collective-permute-start | bytes 294920 | tf_op jit(solution)/shard_map/ppermute | solution.py:246
  26.2 9.8 %collective-permute-start.19 = (bf16[128,512]{1,0:T(8,128)(2,1)S(1)}, bf16[128,512]{1,0:T(8,128)(2,1)S(1)}, u32[]{:S(2)}, u32[]{:S(2)}) collective-permute-start(bf16[128,512]{1,0:T(8,128)(2,1)S(1)} %attention.3.refs_0_), channel_id=1, source_target_pairs={{0,2},{1,3},{2,0},{3,1},{4,6},{5,7},{6,4},{7,5},{8,10},{9,11},{10,... | collective-permute-start | bytes 393224 | tf_op jit(solution)/shard_map/ppermute | solution.py:356
  27.7 7.7 %collective-permute-start.22 = (bf16[128,512]{1,0:T(8,128)(2,1)S(1)}, bf16[128,512]{1,0:T(8,128)(2,1)S(1)}, u32[]{:S(2)}, u32[]{:S(2)}) collective-permute-start(bf16[128,512]{1,0:T(8,128)(2,1)S(1)} %get-tuple-element.8.refs_0_), channel_id=1, source_target_pairs={{0,2},{1,3},{2,0},{3,1},{4,6},{5,7},{6,4},{7,5},{8,10},{9,11},{10,... | collective-permute-start | bytes 393224 | tf_op jit(solution)/shard_map/ppermute | solution.py:356
  30.2 7.5 %collective-permute-start.16 = (bf16[128,512]{1,0:T(8,128)(2,1)S(1)}, bf16[128,512]{1,0:T(8,128)(2,1)S(1)}, u32[]{:S(2)}, u32[]{:S(2)}) collective-permute-start(bf16[128,512]{1,0:T(8,128)(2,1)S(1)} %attention.2.refs_0_), channel_id=1, source_target_pairs={{0,2},{1,3},{2,0},{3,1},{4,6},{5,7},{6,4},{7,5},{8,10},{9,11},{10,... | collective-permute-start | bytes 393224 | tf_op jit(solution)/shard_map/ppermute | solution.py:356
  31.7 6.0 %collective-permute-start.21 = (bf16[128,512]{1,0:T(8,128)(2,1)S(1)}, bf16[128,512]{1,0:T(8,128)(2,1)S(1)}, u32[]{:S(2)}, u32[]{:S(2)}) collective-permute-start(bf16[128,512]{1,0:T(8,128)(2,1)S(1)} %get-tuple-element.8.refs_0_), channel_id=1, source_target_pairs={{0,1},{1,0},{2,3},{3,2},{4,5},{5,4},{6,7},{7,6},{8,9},{9,8},{10,11... | collective-permute-start | bytes 393224 | tf_op jit(solution)/shard_map/ppermute | solution.py:355
  35.4 2.8 %collective-permute-start.23 = (bf16[128,512]{1,0:T(8,128)(2,1)S(1)}, bf16[128,512]{1,0:T(8,128)(2,1)S(1)}, u32[]{:S(2)}, u32[]{:S(2)}) collective-permute-start(bf16[128,512]{1,0:T(8,128)(2,1)S(1)} %collective-permute-done.22.refs_2_), channel_id=1, source_target_pairs={{0,1},{1,0},{2,3},{3,2},{4,5},{5,4},{6,7},{7,6},{8,9},{9,8},{10,11... | collective-permute-start | bytes 393224 | tf_op jit(solution)/shard_map/ppermute | solution.py:357
  35.4 3.9 %collective-permute-start.18 = (bf16[128,512]{1,0:T(8,128)(2,1)S(1)}, bf16[128,512]{1,0:T(8,128)(2,1)S(1)}, u32[]{:S(2)}, u32[]{:S(2)}) collective-permute-start(bf16[128,512]{1,0:T(8,128)(2,1)S(1)} %attention.3.refs_0_), channel_id=1, source_target_pairs={{0,1},{1,0},{2,3},{3,2},{4,5},{5,4},{6,7},{7,6},{8,9},{9,8},{10,11... | collective-permute-start | bytes 393224 | tf_op jit(solution)/shard_map/ppermute | solution.py:355
  35.9 3.4 %collective-permute-start.20 = (bf16[128,512]{1,0:T(8,128)(2,1)S(1)}, bf16[128,512]{1,0:T(8,128)(2,1)S(1)}, u32[]{:S(2)}, u32[]{:S(2)}) collective-permute-start(bf16[128,512]{1,0:T(8,128)(2,1)S(1)} %collective-permute-done.19.refs_2_), channel_id=1, source_target_pairs={{0,1},{1,0},{2,3},{3,2},{4,5},{5,4},{6,7},{7,6},{8,9},{9,8},{10,11... | collective-permute-start | bytes 393224 | tf_op jit(solution)/shard_map/ppermute | solution.py:357
  37.7 2.8 %collective-permute-start.15 = (bf16[128,512]{1,0:T(8,128)(2,1)S(1)}, bf16[128,512]{1,0:T(8,128)(2,1)S(1)}, u32[]{:S(2)}, u32[]{:S(2)}) collective-permute-start(bf16[128,512]{1,0:T(8,128)(2,1)S(1)} %attention.2.refs_0_), channel_id=1, source_target_pairs={{0,1},{1,0},{2,3},{3,2},{4,5},{5,4},{6,7},{7,6},{8,9},{9,8},{10,11... | collective-permute-start | bytes 393224 | tf_op jit(solution)/shard_map/ppermute | solution.py:355
  37.7 2.8 %collective-permute-start.17 = (bf16[128,512]{1,0:T(8,128)(2,1)S(1)}, bf16[128,512]{1,0:T(8,128)(2,1)S(1)}, u32[]{:S(2)}, u32[]{:S(2)}) collective-permute-start(bf16[128,512]{1,0:T(8,128)(2,1)S(1)} %collective-permute-done.16.refs_2_), channel_id=1, source_target_pairs={{0,1},{1,0},{2,3},{3,2},{4,5},{5,4},{6,7},{7,6},{8,9},{9,8},{10,11... | collective-permute-start | bytes 393224 | tf_op jit(solution)/shard_map/ppermute | solution.py:357
  (6 other events, 118.2 us)

commit v5 on v4

--- a/solution.py
+++ b/solution.py
@@ -56,11 +56,11 @@
     return values * cosine + pltpu.roll(values, HALF, 1) * sine
 
 
-def key_value_kernel(tokens, w_key, w_value, coarse_hbm, fine_hbm, out, slab, keys, values, coarse, fine, sems, table_sems):
+def key_value_kernel(tokens, w_key, w_value, coarse_hbm, fine_hbm, out, slab, keys, values, coarse, fine, sems, table_sems, *, sharing):
     rows = slab.shape[0]
     width = tokens.shape[1]
     member = lax.axis_index("tp") % (tokens.shape[0] // rows)
-    head = lax.axis_index("tp") // (tokens.shape[0] // rows)
+    head = lax.axis_index("tp") // sharing
     row = pl.multiple_of(member * rows, 8)
     column = pl.multiple_of(head * DH, DH)
     pieces = sems.shape[0]
@@ -199,15 +199,14 @@
             summed = None
 
 
-def first_attention_kernel(*refs, first, count, tags, sharing):
+def first_attention_kernel(*refs, first, count, tags):
     chosen, query = refs[:2]
     out, key_value, scores = refs[-3:]
-    blocks = query.shape[0] // BLK
-    held = blocks // sharing
-    member = lax.axis_index("tp") % sharing
-    for shard, (bits, sibling) in zip(refs[2 : 2 + len(tags)], tags):
-        place = ((lax.axis_index("kv") ^ bits) * blocks + (member ^ sibling) * held) * BLK
-        key_value[pl.ds(pl.multiple_of(place, BLK), held * BLK)] = shard[...]
+    core = lax.axis_index("tp") % 2
+    for shard, (even, odd) in zip(refs[2 : 2 + len(tags)], tags):
+        rows = shard.shape[0]
+        source = lax.axis_index("kv") ^ jnp.where(core == 0, even, odd)
+        key_value[pl.ds(pl.multiple_of(source * rows, BLK), rows)] = shard[...]
     attend(first, count, chosen, query, key_value, out, scores)
 
 
@@ -215,10 +214,7 @@
     attend(first, count, chosen, query, key_value, out, scores)
 
 
-def project_kernel(*refs, pieces, first, relative):
-    parts = refs[:pieces]
-    w_out = refs[pieces]
-    out, staged, sem = refs[-3:]
+def projected(parts, w_out, relative):
     depth = parts[0].shape[1]
     total = None
     for index, part in enumerate(parts):
@@ -226,25 +222,73 @@
         rows = pl.ds(pl.multiple_of(place * depth, depth), depth)
         product = jnp.dot(part[...], w_out[rows], preferred_element_type=jnp.float32)
         total = product if total is None else total + product
-    staged[...] = total.astype(jnp.bfloat16)
-    copy = pltpu.make_async_copy(staged, out.at[pl.ds(first, staged.shape[0])], sem)
-    copy.start()
-    copy.wait()
-
-
-EXCHANGES = ((4, 4), (2, 2), (1, 1), (3, 1), (6, 2), (7, 3), (5, 1))
+    return total.astype(jnp.bfloat16)
+
+
+def project_kernel(*refs, relative):
+    refs[-1][...] = projected(refs[:-2], refs[-2], relative)
+
+
+def last_project_kernel(*refs, pieces, relative):
+    w_out = refs[pieces]
+    earlier = refs[pieces + 1 : -3]
+    out, staged, sems = refs[-3:]
+    rows = staged.shape[0]
+    copies = [
+        pltpu.make_async_copy(source, out.at[pl.ds(number * rows, rows)], sems.at[number])
+        for number, source in enumerate((*earlier, staged))
+    ]
+    for copy in copies[:-1]:
+        copy.start()
+    staged[...] = projected(refs[:pieces], w_out, relative)
+    copies[-1].start()
+    for copy in copies:
+        copy.wait()
+
+
+SHARDS = {"own": (0, 0), "a": (2, 4), "sa": (4, 2), "b": (1, 1), "e": (3, 6), "se": (6, 3), "h": (7, 5), "sh": (5, 7)}
+
+
+def choose_kernel(first, second, out):
+    core = lax.axis_index("tp") % 2
+
+    @pl.when(core == 0)
+    def _():
+        out[...] = first[...]
+
+    @pl.when(core != 0)
+    def _():
+        out[...] = second[...]
 
 
 def spread_small(own, kv_count, tp_count):
-    shards = {0: own}
-    for bits, hop in EXCHANGES:
-        pairs = [(i, i ^ hop) for i in range(kv_count)]
-        shards[bits] = lax.ppermute(shards[bits ^ hop], "kv", pairs)
-    everything = {}
-    for bits, shard in shards.items():
-        everything[bits, 0] = shard
-        everything[bits, 1] = lax.ppermute(shard, "tp", [(i, i ^ 1) for i in range(tp_count)])
-    return everything
+    def exchange(array, hops):
+        pairs = []
+        for place in range(kv_count * tp_count):
+            kv_at, tp_at = divmod(place, tp_count)
+            pairs.append((place, (kv_at ^ hops[tp_at % 2]) * tp_count + tp_at))
+        return lax.ppermute(array, ("kv", "tp"), pairs)
+
+    def swap(array):
+        return lax.ppermute(array, "tp", [(i, i ^ 1) for i in range(tp_count)])
+
+    shards = {"own": own}
+    shards["a"] = exchange(own, (2, 4))
+    shards["b"] = exchange(own, (1, 1))
+    shards["sa"] = swap(shards["a"])
+    shards["e"] = exchange(shards["a"], (1, 2))
+    fourth = pl.pallas_call(
+        choose_kernel,
+        out_shape=pltpu.VMEM(own.shape, own.dtype),
+        in_specs=[VMEM, VMEM],
+        out_specs=VMEM,
+        compiler_params=room(2),
+        name="choose",
+    )(keep(shards["sa"]), keep(shards["a"]))
+    shards["h"] = exchange(fourth, (3, 1))
+    shards["se"] = swap(shards["e"])
+    shards["sh"] = swap(shards["h"])
+    return shards
 
 
 def keep(array):
@@ -267,12 +311,12 @@
     own_heads = w_query.shape[1] // DH
     own_width = own_heads * DH
     sharing = tp_count // KVH
-    part_rows = rows // sharing
     small = kv_count == 8 and tp_count == 4
+    part_rows = rows if small else rows // sharing
     coarse, fine = (jnp.asarray(table) for table in tables(kv_count * local_blocks))
 
     own_part = pl.pallas_call(
-        key_value_kernel,
+        functools.partial(key_value_kernel, sharing=sharing),
         out_shape=pltpu.VMEM((part_rows, 2 * DH), jnp.bfloat16),
         in_specs=[HBM] * 5,
         out_specs=VMEM,
@@ -307,6 +351,7 @@
 
     if small:
         shards = spread_small(own_part, kv_count, tp_count)
+        tags = [SHARDS[name] for name in shards]
     else:
         groups = [[g * sharing + i for i in range(sharing)] for g in range(KVH)]
         whole = lax.all_gather(own_part, "tp", axis=0, tiled=True, axis_index_groups=groups)
@@ -315,7 +360,7 @@
     splits = 3
     per = local_blocks // splits
     scores = pltpu.VMEM((2, NSEL // TILE, own_heads * BLK, TILE * BLK), jnp.float32)
-    result = None
+    earlier = []
     w_out = keep(w_out)
     chosen = keep(chosen)
     for split in range(splits):
@@ -328,7 +373,7 @@
         )
         if small and split == 0:
             attention, key_value = pl.pallas_call(
-                functools.partial(first_attention_kernel, first=first, count=per, tags=tuple(shards), sharing=sharing),
+                functools.partial(first_attention_kernel, first=first, count=per, tags=tags),
                 out_shape=[shape, pltpu.VMEM((kv_count * rows, 2 * DH), jnp.bfloat16)],
                 in_specs=[VMEM, VMEM] + [VMEM] * len(shards),
                 out_specs=[VMEM, VMEM],
@@ -337,7 +382,6 @@
                 compiler_params=room(12),
                 name="first_attention",
             )(chosen, query, *[keep(shard) for shard in shards.values()])
-            key_value = keep(key_value)
             key_value = keep(key_value)
         else:
             call = pl.pallas_call(
@@ -359,24 +403,34 @@
         else:
             parts = [lax.all_gather(attention, "tp", axis=1, tiled=True)]
         parts = [keep(part) for part in parts]
-        earlier = [] if result is None else [result]
-        call = pl.pallas_call(
-            functools.partial(project_kernel, pieces=len(parts), first=first * BLK, relative=small),
-            out_shape=jax.ShapeDtypeStruct((rows, w_out.shape[1]), jnp.bfloat16),
-            in_specs=[VMEM] * (len(parts) + 1) + [ANY] * len(earlier),
-            out_specs=ANY,
-            input_output_aliases={len(parts) + 1: 0} if earlier else {},
-            scratch_shapes=[
-                pltpu.VMEM((per * BLK, w_out.shape[1]), jnp.bfloat16),
-                pltpu.SemaphoreType.DMA,
-            ],
-            cost_estimate=pl.CostEstimate(
-                flops=2 * per * BLK * H * DH * w_out.shape[1], bytes_accessed=0, transcendentals=0
-            ),
-            compiler_params=room(8),
-            name="project",
+        cost = pl.CostEstimate(
+            flops=2 * per * BLK * H * DH * w_out.shape[1], bytes_accessed=0, transcendentals=0
         )
-        result = call(*parts, w_out, *earlier)
+        if split < splits - 1:
+            call = pl.pallas_call(
+                functools.partial(project_kernel, relative=small),
+                out_shape=pltpu.VMEM((per * BLK, w_out.shape[1]), jnp.bfloat16),
+                in_specs=[VMEM] * (len(parts) + 1),
+                out_specs=VMEM,
+                cost_estimate=cost,
+                compiler_params=room(8),
+                name="project",
+            )
+            earlier.append(keep(call(*parts, w_out)))
+        else:
+            result = pl.pallas_call(
+                functools.partial(last_project_kernel, pieces=len(parts), relative=small),
+                out_shape=jax.ShapeDtypeStruct((rows, w_out.shape[1]), jnp.bfloat16),
+                in_specs=[VMEM] * (len(parts) + 1 + len(earlier)),
+                out_specs=HBM,
+                scratch_shapes=[
+                    pltpu.VMEM((per * BLK, w_out.shape[1]), jnp.bfloat16),
+                    pltpu.SemaphoreType.DMA((splits,)),
+                ],
+                cost_estimate=cost,
+                compiler_params=room(8),
+                name="last_project",
+            )(*parts, w_out, *earlier)
     return result
 
 

time: 41.8 us -> 43.1 us (1.031)
  waiting for transfers between devices: 12.6 us -> 15 us
  Pallas kernels: 12.4 us -> 11.5 us
    ppermute x15 -> x7, waiting for transfers between devices: 7.14 us -> 9.58 us  [the longest x4 9.57 us: exchange(): return lax.ppermute(array, ('kv', 'tp'), pairs)]
    pallas_call x4 -> x5, Pallas kernels: 5.51 us -> 4.65 us  [the longest x1 2.61 us: body(): pl.pallas_call(functools.partial(key_value_kernel, sharing=sharing), out_...]
    ppermute x15 -> x7, starting transfers between devices: 11.8 us -> 11 us  [the longest x4 8.06 us: exchange(): return lax.ppermute(array, ('kv', 'tp'), pairs)]
    ppermute x3, starting transfers between devices: 0.51 us -> 0.99 us  [body(): far = lax.ppermute(across, 'tp', [(i, i ^ 1) for i in range(tp_count)])]
  transfers between devices with their start and end apart: 24 -> 16, of which waited for: 8 -> 7; matrix products, arithmetic and copies ran while one was open for 0% -> 0% of each run, Pallas kernels for 13% -> 9%
where the time goes in v5:
time: 43.1 us; the launch traced here: 42.9 us
  starting transfers between devices  16.2 us (38%)
  waiting for transfers between devices  15 us (35%)
  Pallas kernels  11.5 us (27%)
    ppermute x4, waiting for transfers between devices, exchange(): return lax.ppermute(array, ('kv', 'tp'), pairs)  9.57 us
    ppermute x4, starting transfers between devices, exchange(): return lax.ppermute(array, ('kv', 'tp'), pairs)  8.06 us
    ppermute x3, waiting for transfers between devices, body(): lax.ppermute(attention, 'tp', [(i, i ^ 2) for i in range(tp_count)])  5.34 us
    pallas_call x2, Pallas kernels, body(): attention = call(chosen, query, key_value)  3.79 us
    ppermute x3, starting transfers between devices, body(): lax.ppermute(attention, 'tp', [(i, i ^ 2) for i in range(tp_count)])  3.73 us
    ppermute x3, starting transfers between devices, swap(): return lax.ppermute(array, 'tp', [(i, i ^ 1) for i in range(tp_count)])  2.93 us
    pallas_call x1, Pallas kernels, body(): pl.pallas_call(functools.partial(key_value_kernel, sharing=sharing), out_...  2.61 us
    pallas_call x1, Pallas kernels, body(): pl.pallas_call(functools.partial(first_attention_kernel, first=first, cou...  1.95 us
  transfers between devices with their start and end apart: 16, of which 7 were waited for; matrix products, arithmetic and copies ran while one was open for 0% of the time, Pallas kernels for 9%

profile of v5, /device:TPU:0, one launch (start us, length us, event | category | flops | bytes accessed | tf_op | source)
XLA Modules:
  0.0 42.9 jit_solution(16807016576086029175)
XLA Ops:
  0.0 2.6 %key_value.1.refs_2_ = bf16[384,256]{1,0:T(8,128)(2,1)S(1)} custom-call(bf16[384,2048]{1,0:T(8,128)(2,1)} %tokens.3, bf16[2048,256]{1,0:T(8,128)(2,1)} %w_key.1, bf16[2048,256]{1,0:T(8,128)(2,1)} %w_value.1, f32[2,48,128]{2,1,0:T(8,128)} %constant.4.clone.coarse.coarse_hbm, f32[2,64,128]{2,1,0:T(8,128)} %constant.5.clone.fine.fine_hbm), custom_call_target="tpu_custom_call" | custom-call | flops 402653184 | bytes 2621440 | tf_op jit(solution)/shard_map/key_value/pallas_call | solution.py:318
  2.6 3.1 %collective-permute-start = (bf16[384,256]{1,0:T(8,128)(2,1)S(1)}, bf16[384,256]{1,0:T(8,128)(2,1)S(1)}, u32[]{:S(2)}, u32[]{:S(2)}) collective-permute-start(bf16[384,256]{1,0:T(8,128)(2,1)S(1)} %key_value.1.refs_2_), channel_id=1, source_target_pairs={{0,8},{1,17},{2,10},{3,19},{4,12},{5,21},{6,14},{7,23},{8,0},{9,25... | collective-permute-start | bytes 589832 | tf_op jit(solution)/shard_map/ppermute | solution.py:270
  5.8 5.4 %collective-permute-done.second.refs_3_ = bf16[384,256]{1,0:T(8,128)(2,1)S(1)} collective-permute-done((bf16[384,256]{1,0:T(8,128)(2,1)S(1)}, bf16[384,256]{1,0:T(8,128)(2,1)S(1)}, u32[]{:S(2)}, u32[]{:S(2)}) %collective-permute-start) | collective-permute-done | bytes 196640 | tf_op jit(solution)/shard_map/ppermute | solution.py:270
  11.2 0.4 collective-permute-start.2
  11.5 1.6 %collective-permute-start.3 = (bf16[384,256]{1,0:T(8,128)(2,1)S(1)}, bf16[384,256]{1,0:T(8,128)(2,1)S(1)}, u32[]{:S(2)}, u32[]{:S(2)}) collective-permute-start(bf16[384,256]{1,0:T(8,128)(2,1)S(1)} %collective-permute-done.second.refs_3_), channel_id=1, source_target_pairs={{0,4},{1,9},{2,6},{3,11},{4,0},{5,13},{6,2},{7,15},{8,12},{9,1},{1... | collective-permute-start | bytes 589832 | tf_op jit(solution)/shard_map/ppermute | solution.py:270
  13.1 2.8 %collective-permute-start.4 = (bf16[384,256]{1,0:T(8,128)(2,1)S(1)}, bf16[384,256]{1,0:T(8,128)(2,1)S(1)}, u32[]{:S(2)}, u32[]{:S(2)}) collective-permute-start(bf16[384,256]{1,0:T(8,128)(2,1)S(1)} %choose.1), channel_id=1, source_target_pairs={{0,12},{1,5},{2,14},{3,7},{4,8},{5,1},{6,10},{7,3},{8,4},{9,13},{1... | collective-permute-start | bytes 589832 | tf_op jit(solution)/shard_map/ppermute | solution.py:270
  15.9 0.6 %collective-permute-start.1 = (bf16[384,256]{1,0:T(8,128)(2,1)S(1)}, bf16[384,256]{1,0:T(8,128)(2,1)S(1)}, u32[]{:S(2)}, u32[]{:S(2)}) collective-permute-start(bf16[384,256]{1,0:T(8,128)(2,1)S(1)} %key_value.1.refs_2_), channel_id=1, source_target_pairs={{0,4},{1,5},{2,6},{3,7},{4,0},{5,1},{6,2},{7,3},{8,12},{9,13},{10,... | collective-permute-start | bytes 589832 | tf_op jit(solution)/shard_map/ppermute | solution.py:270
  16.5 3.7 %collective-permute-done.3.refs_6_ = bf16[384,256]{1,0:T(8,128)(2,1)S(1)} collective-permute-done((bf16[384,256]{1,0:T(8,128)(2,1)S(1)}, bf16[384,256]{1,0:T(8,128)(2,1)S(1)}, u32[]{:S(2)}, u32[]{:S(2)}) %collective-permute-start.3) | collective-permute-done | bytes 196640 | tf_op jit(solution)/shard_map/ppermute | solution.py:270
  20.2 2.6 %collective-permute-start.6 = (bf16[384,256]{1,0:T(8,128)(2,1)S(1)}, bf16[384,256]{1,0:T(8,128)(2,1)S(1)}, u32[]{:S(2)}, u32[]{:S(2)}) collective-permute-start(bf16[384,256]{1,0:T(8,128)(2,1)S(1)} %collective-permute-done.4.refs_7_), channel_id=1, source_target_pairs={{0,1},{1,0},{2,3},{3,2},{4,5},{5,4},{6,7},{7,6},{8,9},{9,8},{10,11... | collective-permute-start | bytes 589832 | tf_op jit(solution)/shard_map/ppermute | solution.py:273
  22.8 1.1 %query.1.refs_1_ = bf16[384,512]{1,0:T(8,128)(2,1)S(1)} custom-call(bf16[384,2048]{1,0:T(8,128)(2,1)S(1)} %copy-done.1, bf16[2048,512]{1,0:T(8,128)(2,1)S(1)} %copy-done.2, f32[2,48,128]{2,1,0:T(8,128)S(1)} %copy-done.4, f32[2,64,128]{2,1,0:T(8,128)S(1)} %copy-done.3), custom_call_target="tpu_custom_call" | custom-call | flops 805306368 | bytes 3670016 | tf_op jit(solution)/shard_map/query/pallas_call | solution.py:339
  23.9 0.5 %collective-permute-done.1.refs_4_ = bf16[384,256]{1,0:T(8,128)(2,1)S(1)} collective-permute-done((bf16[384,256]{1,0:T(8,128)(2,1)S(1)}, bf16[384,256]{1,0:T(8,128)(2,1)S(1)}, u32[]{:S(2)}, u32[]{:S(2)}) %collective-permute-start.1) | collective-permute-done | bytes 196640 | tf_op jit(solution)/shard_map/ppermute | solution.py:270
  24.4 2.0 %first_attention.1 = (bf16[128,512]{1,0:T(8,128)(2,1)S(1)}, bf16[3072,256]{1,0:T(8,128)(2,1)S(1)}) custom-call(s32[6,32]{1,0:T(8,128)S(1)} %copy-done.5, bf16[384,512]{1,0:T(8,128)(2,1)S(1)} %query.1.refs_1_, bf16[384,256]{1,0:T(8,128)(2,1)S(1)} %key_value.1.refs_2_, bf16[384,256]{1,0:T(8,128)(2,1)S(1)} %collective-permute-done.second.refs_3_, ...), custom_call_target="tpu_custom_call" | custom-call | flops 553648128 | bytes 131072 | tf_op jit(solution)/shard_map/first_attention/pallas_call | solution.py:375
  26.4 1.9 %attention.3.refs_0_ = bf16[128,512]{1,0:T(8,128)(2,1)S(1)} custom-call(s32[6,32]{1,0:T(8,128)S(1)} %copy-done.5, bf16[384,512]{1,0:T(8,128)(2,1)S(1)} %query.1.refs_1_, bf16[3072,256]{1,0:T(8,128)(2,1)S(1)} %get-tuple-element.7.key_value), custom_call_target="tpu_custom_call" | custom-call | flops 553648128 | bytes 131072 | tf_op jit(solution)/shard_map/attention/pallas_call | solution.py:397
  28.3 1.6 %collective-permute-start.14 = (bf16[128,512]{1,0:T(8,128)(2,1)S(1)}, bf16[128,512]{1,0:T(8,128)(2,1)S(1)}, u32[]{:S(2)}, u32[]{:S(2)}) collective-permute-start(bf16[128,512]{1,0:T(8,128)(2,1)S(1)} %attention.3.refs_0_), channel_id=1, source_target_pairs={{0,2},{1,3},{2,0},{3,1},{4,6},{5,7},{6,4},{7,5},{8,10},{9,11},{10,... | collective-permute-start | bytes 393224 | tf_op jit(solution)/shard_map/ppermute | solution.py:400
  29.9 0.5 %collective-permute-start.11 = (bf16[128,512]{1,0:T(8,128)(2,1)S(1)}, bf16[128,512]{1,0:T(8,128)(2,1)S(1)}, u32[]{:S(2)}, u32[]{:S(2)}) collective-permute-start(bf16[128,512]{1,0:T(8,128)(2,1)S(1)} %get-tuple-element.8.refs_0_), channel_id=1, source_target_pairs={{0,2},{1,3},{2,0},{3,1},{4,6},{5,7},{6,4},{7,5},{8,10},{9,11},{10,... | collective-permute-start | bytes 393224 | tf_op jit(solution)/shard_map/ppermute | solution.py:400
  30.4 1.9 %attention.2.refs_0_ = bf16[128,512]{1,0:T(8,128)(2,1)S(1)} custom-call(s32[6,32]{1,0:T(8,128)S(1)} %copy-done.5, bf16[384,512]{1,0:T(8,128)(2,1)S(1)} %query.1.refs_1_, bf16[3072,256]{1,0:T(8,128)(2,1)S(1)} %get-tuple-element.7.key_value), custom_call_target="tpu_custom_call" | custom-call | flops 553648128 | bytes 131072 | tf_op jit(solution)/shard_map/attention/pallas_call | solution.py:397
  32.3 1.6 %collective-permute-start.8 = (bf16[128,512]{1,0:T(8,128)(2,1)S(1)}, bf16[128,512]{1,0:T(8,128)(2,1)S(1)}, u32[]{:S(2)}, u32[]{:S(2)}) collective-permute-start(bf16[128,512]{1,0:T(8,128)(2,1)S(1)} %attention.2.refs_0_), channel_id=1, source_target_pairs={{0,2},{1,3},{2,0},{3,1},{4,6},{5,7},{6,4},{7,5},{8,10},{9,11},{10,... | collective-permute-start | bytes 393224 | tf_op jit(solution)/shard_map/ppermute | solution.py:400
  34.1 0.5 %collective-permute-done.14.refs_2_ = bf16[128,512]{1,0:T(8,128)(2,1)S(1)} collective-permute-done((bf16[128,512]{1,0:T(8,128)(2,1)S(1)}, bf16[128,512]{1,0:T(8,128)(2,1)S(1)}, u32[]{:S(2)}, u32[]{:S(2)}) %collective-permute-start.14) | collective-permute-done | bytes 131104 | tf_op jit(solution)/shard_map/ppermute | solution.py:400
  35.1 2.3 %collective-permute-done.11.refs_2_ = bf16[128,512]{1,0:T(8,128)(2,1)S(1)} collective-permute-done((bf16[128,512]{1,0:T(8,128)(2,1)S(1)}, bf16[128,512]{1,0:T(8,128)(2,1)S(1)}, u32[]{:S(2)}, u32[]{:S(2)}) %collective-permute-start.11) | collective-permute-done | bytes 131104 | tf_op jit(solution)/shard_map/ppermute | solution.py:400
  37.7 2.5 %collective-permute-done.8.refs_2_ = bf16[128,512]{1,0:T(8,128)(2,1)S(1)} collective-permute-done((bf16[128,512]{1,0:T(8,128)(2,1)S(1)}, bf16[128,512]{1,0:T(8,128)(2,1)S(1)}, u32[]{:S(2)}, u32[]{:S(2)}) %collective-permute-start.8) | collective-permute-done | bytes 131104 | tf_op jit(solution)/shard_map/ppermute | solution.py:400
  40.4 0.4 collective-permute-start.9
  40.8 0.4 %project.3.refs_6_ = bf16[128,512]{1,0:T(8,128)(2,1)S(1)} custom-call(bf16[128,512]{1,0:T(8,128)(2,1)S(1)} %attention.3.refs_0_, bf16[128,512]{1,0:T(8,128)(2,1)S(1)} %collective-permute-done.13.refs_1_, bf16[128,512]{1,0:T(8,128)(2,1)S(1)} %collective-permute-done.14.refs_2_, bf16[128,512]{1,0:T(8,128)(2,1)S(1)} %collective-permute-done.15.refs_3_, ...), custom_call_target="tpu_custom_call" | custom-call | flops 268435456 | tf_op jit(solution)/shard_map/project/pallas_call | solution.py:419
  41.2 0.4 %project.2.refs_5_ = bf16[128,512]{1,0:T(8,128)(2,1)S(1)} custom-call(bf16[128,512]{1,0:T(8,128)(2,1)S(1)} %get-tuple-element.8.refs_0_, bf16[128,512]{1,0:T(8,128)(2,1)S(1)} %collective-permute-done.10.refs_1_, bf16[128,512]{1,0:T(8,128)(2,1)S(1)} %collective-permute-done.11.refs_2_, bf16[128,512]{1,0:T(8,128)(2,1)S(1)} %collective-permute-done.12.refs_3_, ...), custom_call_target="tpu_custom_call" | custom-call | flops 268435456 | tf_op jit(solution)/shard_map/project/pallas_call | solution.py:419
  41.8 1.1 %last_project.1 = bf16[384,512]{1,0:T(8,128)(2,1)} custom-call(bf16[128,512]{1,0:T(8,128)(2,1)S(1)} %attention.2.refs_0_, bf16[128,512]{1,0:T(8,128)(2,1)S(1)} %collective-permute-done.7.refs_1_, bf16[128,512]{1,0:T(8,128)(2,1)S(1)} %collective-permute-done.8.refs_2_, bf16[128,512]{1,0:T(8,128)(2,1)S(1)} %collective-permute-done.9.refs_3_, ...), custom_call_target="tpu_custom_call" | custom-call | flops 268435456 | tf_op jit(solution)/shard_map/last_project/pallas_call | solution.py:421
  (29 shorter events, 1.2 us)
Async XLA Ops:
  0.0 22.8 %copy-start.3 = (f32[2,64,128]{2,1,0:T(8,128)S(1)}, f32[2,64,128]{2,1,0:T(8,128)}, u32[]{:S(2)}) copy-start(f32[2,64,128]{2,1,0:T(8,128)} %constant.5.clone.fine.fine_hbm) | copy-start | bytes 196612
  0.0 22.8 %copy-start.4 = (f32[2,48,128]{2,1,0:T(8,128)S(1)}, f32[2,48,128]{2,1,0:T(8,128)}, u32[]{:S(2)}) copy-start(f32[2,48,128]{2,1,0:T(8,128)} %constant.4.clone.coarse.coarse_hbm) | copy-start | bytes 147460
  0.0 22.8 %copy-start.1 = (bf16[384,2048]{1,0:T(8,128)(2,1)S(1)}, bf16[384,2048]{1,0:T(8,128)(2,1)}, u32[]{:S(2)}) copy-start(bf16[384,2048]{1,0:T(8,128)(2,1)} %tokens.3) | copy-start | bytes 4718596
  0.0 22.8 %copy-start.2 = (bf16[2048,512]{1,0:T(8,128)(2,1)S(1)}, bf16[2048,512]{1,0:T(8,128)(2,1)}, u32[]{:S(2)}) copy-start(bf16[2048,512]{1,0:T(8,128)(2,1)} %w_query.1) | copy-start | bytes 6291460
  2.6 8.6 %collective-permute-start = (bf16[384,256]{1,0:T(8,128)(2,1)S(1)}, bf16[384,256]{1,0:T(8,128)(2,1)S(1)}, u32[]{:S(2)}, u32[]{:S(2)}) collective-permute-start(bf16[384,256]{1,0:T(8,128)(2,1)S(1)} %key_value.1.refs_2_), channel_id=1, source_target_pairs={{0,8},{1,17},{2,10},{3,19},{4,12},{5,21},{6,14},{7,23},{8,0},{9,25... | collective-permute-start | bytes 589832 | tf_op jit(solution)/shard_map/ppermute | solution.py:270
  11.2 1.9 %collective-permute-start.2 = (bf16[384,256]{1,0:T(8,128)(2,1)S(1)}, bf16[384,256]{1,0:T(8,128)(2,1)S(1)}, u32[]{:S(2)}, u32[]{:S(2)}) collective-permute-start(bf16[384,256]{1,0:T(8,128)(2,1)S(1)} %collective-permute-done.second.refs_3_), channel_id=1, source_target_pairs={{0,1},{1,0},{2,3},{3,2},{4,5},{5,4},{6,7},{7,6},{8,9},{9,8},{10,11... | collective-permute-start | bytes 589832 | tf_op jit(solution)/shard_map/ppermute | solution.py:273
  11.5 8.6 %collective-permute-start.3 = (bf16[384,256]{1,0:T(8,128)(2,1)S(1)}, bf16[384,256]{1,0:T(8,128)(2,1)S(1)}, u32[]{:S(2)}, u32[]{:S(2)}) collective-permute-start(bf16[384,256]{1,0:T(8,128)(2,1)S(1)} %collective-permute-done.second.refs_3_), channel_id=1, source_target_pairs={{0,4},{1,9},{2,6},{3,11},{4,0},{5,13},{6,2},{7,15},{8,12},{9,1},{1... | collective-permute-start | bytes 589832 | tf_op jit(solution)/shard_map/ppermute | solution.py:270
  13.1 11.3 %copy-start.5 = (s32[6,32]{1,0:T(8,128)S(1)}, s32[6,32]{1,0:T(8,128)}, u32[]{:S(2)}) copy-start(s32[6,32]{1,0:T(8,128)} %chosen.3) | copy-start | bytes 2308
  13.1 7.1 %collective-permute-start.4 = (bf16[384,256]{1,0:T(8,128)(2,1)S(1)}, bf16[384,256]{1,0:T(8,128)(2,1)S(1)}, u32[]{:S(2)}, u32[]{:S(2)}) collective-permute-start(bf16[384,256]{1,0:T(8,128)(2,1)S(1)} %choose.1), channel_id=1, source_target_pairs={{0,12},{1,5},{2,14},{3,7},{4,8},{5,1},{6,10},{7,3},{8,4},{9,13},{1... | collective-permute-start | bytes 589832 | tf_op jit(solution)/shard_map/ppermute | solution.py:270
  15.9 8.5 %collective-permute-start.1 = (bf16[384,256]{1,0:T(8,128)(2,1)S(1)}, bf16[384,256]{1,0:T(8,128)(2,1)S(1)}, u32[]{:S(2)}, u32[]{:S(2)}) collective-permute-start(bf16[384,256]{1,0:T(8,128)(2,1)S(1)} %key_value.1.refs_2_), channel_id=1, source_target_pairs={{0,4},{1,5},{2,6},{3,7},{4,0},{5,1},{6,2},{7,3},{8,12},{9,13},{10,... | collective-permute-start | bytes 589832 | tf_op jit(solution)/shard_map/ppermute | solution.py:270
  20.2 4.2 %collective-permute-start.5 = (bf16[384,256]{1,0:T(8,128)(2,1)S(1)}, bf16[384,256]{1,0:T(8,128)(2,1)S(1)}, u32[]{:S(2)}, u32[]{:S(2)}) collective-permute-start(bf16[384,256]{1,0:T(8,128)(2,1)S(1)} %collective-permute-done.3.refs_6_), channel_id=1, source_target_pairs={{0,1},{1,0},{2,3},{3,2},{4,5},{5,4},{6,7},{7,6},{8,9},{9,8},{10,11... | collective-permute-start | bytes 589832 | tf_op jit(solution)/shard_map/ppermute | solution.py:273
  20.2 4.2 %collective-permute-start.6 = (bf16[384,256]{1,0:T(8,128)(2,1)S(1)}, bf16[384,256]{1,0:T(8,128)(2,1)S(1)}, u32[]{:S(2)}, u32[]{:S(2)}) collective-permute-start(bf16[384,256]{1,0:T(8,128)(2,1)S(1)} %collective-permute-done.4.refs_7_), channel_id=1, source_target_pairs={{0,1},{1,0},{2,3},{3,2},{4,5},{5,4},{6,7},{7,6},{8,9},{9,8},{10,11... | collective-permute-start | bytes 589832 | tf_op jit(solution)/shard_map/ppermute | solution.py:273
  26.4 14.4 %copy-start = (bf16[2048,512]{1,0:T(8,128)(2,1)S(1)}, bf16[2048,512]{1,0:T(8,128)(2,1)}, u32[]{:S(2)}) copy-start(bf16[2048,512]{1,0:T(8,128)(2,1)} %refs_4_.5) | copy-start | bytes 6291460
  28.3 6.3 %collective-permute-start.14 = (bf16[128,512]{1,0:T(8,128)(2,1)S(1)}, bf16[128,512]{1,0:T(8,128)(2,1)S(1)}, u32[]{:S(2)}, u32[]{:S(2)}) collective-permute-start(bf16[128,512]{1,0:T(8,128)(2,1)S(1)} %attention.3.refs_0_), channel_id=1, source_target_pairs={{0,2},{1,3},{2,0},{3,1},{4,6},{5,7},{6,4},{7,5},{8,10},{9,11},{10,... | collective-permute-start | bytes 393224 | tf_op jit(solution)/shard_map/ppermute | solution.py:400
  29.9 7.5 %collective-permute-start.11 = (bf16[128,512]{1,0:T(8,128)(2,1)S(1)}, bf16[128,512]{1,0:T(8,128)(2,1)S(1)}, u32[]{:S(2)}, u32[]{:S(2)}) collective-permute-start(bf16[128,512]{1,0:T(8,128)(2,1)S(1)} %get-tuple-element.8.refs_0_), channel_id=1, source_target_pairs={{0,2},{1,3},{2,0},{3,1},{4,6},{5,7},{6,4},{7,5},{8,10},{9,11},{10,... | collective-permute-start | bytes 393224 | tf_op jit(solution)/shard_map/ppermute | solution.py:400
  32.3 8.0 %collective-permute-start.8 = (bf16[128,512]{1,0:T(8,128)(2,1)S(1)}, bf16[128,512]{1,0:T(8,128)(2,1)S(1)}, u32[]{:S(2)}, u32[]{:S(2)}) collective-permute-start(bf16[128,512]{1,0:T(8,128)(2,1)S(1)} %attention.2.refs_0_), channel_id=1, source_target_pairs={{0,2},{1,3},{2,0},{3,1},{4,6},{5,7},{6,4},{7,5},{8,10},{9,11},{10,... | collective-permute-start | bytes 393224 | tf_op jit(solution)/shard_map/ppermute | solution.py:400
  33.9 6.5 %collective-permute-start.13 = (bf16[128,512]{1,0:T(8,128)(2,1)S(1)}, bf16[128,512]{1,0:T(8,128)(2,1)S(1)}, u32[]{:S(2)}, u32[]{:S(2)}) collective-permute-start(bf16[128,512]{1,0:T(8,128)(2,1)S(1)} %attention.3.refs_0_), channel_id=1, source_target_pairs={{0,1},{1,0},{2,3},{3,2},{4,5},{5,4},{6,7},{7,6},{8,9},{9,8},{10,11... | collective-permute-start | bytes 393224 | tf_op jit(solution)/shard_map/ppermute | solution.py:399
  34.6 6.1 %collective-permute-start.15 = (bf16[128,512]{1,0:T(8,128)(2,1)S(1)}, bf16[128,512]{1,0:T(8,128)(2,1)S(1)}, u32[]{:S(2)}, u32[]{:S(2)}) collective-permute-start(bf16[128,512]{1,0:T(8,128)(2,1)S(1)} %collective-permute-done.14.refs_2_), channel_id=1, source_target_pairs={{0,1},{1,0},{2,3},{3,2},{4,5},{5,4},{6,7},{7,6},{8,9},{9,8},{10,11... | collective-permute-start | bytes 393224 | tf_op jit(solution)/shard_map/ppermute | solution.py:401
  34.9 6.3 %collective-permute-start.10 = (bf16[128,512]{1,0:T(8,128)(2,1)S(1)}, bf16[128,512]{1,0:T(8,128)(2,1)S(1)}, u32[]{:S(2)}, u32[]{:S(2)}) collective-permute-start(bf16[128,512]{1,0:T(8,128)(2,1)S(1)} %get-tuple-element.8.refs_0_), channel_id=1, source_target_pairs={{0,1},{1,0},{2,3},{3,2},{4,5},{5,4},{6,7},{7,6},{8,9},{9,8},{10,11... | collective-permute-start | bytes 393224 | tf_op jit(solution)/shard_map/ppermute | solution.py:399
  37.4 3.8 %collective-permute-start.12 = (bf16[128,512]{1,0:T(8,128)(2,1)S(1)}, bf16[128,512]{1,0:T(8,128)(2,1)S(1)}, u32[]{:S(2)}, u32[]{:S(2)}) collective-permute-start(bf16[128,512]{1,0:T(8,128)(2,1)S(1)} %collective-permute-done.11.refs_2_), channel_id=1, source_target_pairs={{0,1},{1,0},{2,3},{3,2},{4,5},{5,4},{6,7},{7,6},{8,9},{9,8},{10,11... | collective-permute-start | bytes 393224 | tf_op jit(solution)/shard_map/ppermute | solution.py:401
  40.3 1.5 %collective-permute-start.7 = (bf16[128,512]{1,0:T(8,128)(2,1)S(1)}, bf16[128,512]{1,0:T(8,128)(2,1)S(1)}, u32[]{:S(2)}, u32[]{:S(2)}) collective-permute-start(bf16[128,512]{1,0:T(8,128)(2,1)S(1)} %attention.2.refs_0_), channel_id=1, source_target_pairs={{0,1},{1,0},{2,3},{3,2},{4,5},{5,4},{6,7},{7,6},{8,9},{9,8},{10,11... | collective-permute-start | bytes 393224 | tf_op jit(solution)/shard_map/ppermute | solution.py:399
  40.4 1.4 %collective-permute-start.9 = (bf16[128,512]{1,0:T(8,128)(2,1)S(1)}, bf16[128,512]{1,0:T(8,128)(2,1)S(1)}, u32[]{:S(2)}, u32[]{:S(2)}) collective-permute-start(bf16[128,512]{1,0:T(8,128)(2,1)S(1)} %collective-permute-done.8.refs_2_), channel_id=1, source_target_pairs={{0,1},{1,0},{2,3},{3,2},{4,5},{5,4},{6,7},{7,6},{8,9},{9,8},{10,11... | collective-permute-start | bytes 393224 | tf_op jit(solution)/shard_map/ppermute | solution.py:401

commit v6 on v5

--- a/solution.py
+++ b/solution.py
@@ -19,7 +19,7 @@
 SCALE = DH ** (-0.5)
 EXP2_SCALE = SCALE * 1.4426950408889634
 MASKED = -1e30
-TILE = 4
+TILE = 8
 
 ANY = pl.BlockSpec(memory_space=pl.ANY)
 VMEM = pl.BlockSpec(memory_space=pltpu.VMEM)
@@ -214,24 +214,24 @@
     attend(first, count, chosen, query, key_value, out, scores)
 
 
-def projected(parts, w_out, relative):
+def projected(parts, w_out, relative, first=0):
     depth = parts[0].shape[1]
     total = None
     for index, part in enumerate(parts):
-        place = (lax.axis_index("tp") ^ index) if relative else index
+        place = (lax.axis_index("tp") ^ (index + first)) if relative else index + first
         rows = pl.ds(pl.multiple_of(place * depth, depth), depth)
         product = jnp.dot(part[...], w_out[rows], preferred_element_type=jnp.float32)
         total = product if total is None else total + product
-    return total.astype(jnp.bfloat16)
+    return total
 
 
 def project_kernel(*refs, relative):
-    refs[-1][...] = projected(refs[:-2], refs[-2], relative)
-
-
-def last_project_kernel(*refs, pieces, relative):
-    w_out = refs[pieces]
-    earlier = refs[pieces + 1 : -3]
+    refs[-1][...] = projected(refs[:-2], refs[-2], relative).astype(refs[-1].dtype)
+
+
+def last_project_kernel(*refs, relative, before):
+    partial, part, w_out = refs[:3]
+    earlier = refs[3:-3]
     out, staged, sems = refs[-3:]
     rows = staged.shape[0]
     copies = [
@@ -240,7 +240,7 @@
     ]
     for copy in copies[:-1]:
         copy.start()
-    staged[...] = projected(refs[:pieces], w_out, relative)
+    staged[...] = (partial[...] + projected([part], w_out, relative, before)).astype(jnp.bfloat16)
     copies[-1].start()
     for copy in copies:
         copy.wait()
@@ -401,7 +401,7 @@
             far = lax.ppermute(across, "tp", [(i, i ^ 1) for i in range(tp_count)])
             parts = [attention, sibling, across, far]
         else:
-            parts = [lax.all_gather(attention, "tp", axis=1, tiled=True)]
+            parts = jnp.split(lax.all_gather(attention, "tp", axis=1, tiled=True), 2, axis=1)
         parts = [keep(part) for part in parts]
         cost = pl.CostEstimate(
             flops=2 * per * BLK * H * DH * w_out.shape[1], bytes_accessed=0, transcendentals=0
@@ -418,10 +418,20 @@
             )
             earlier.append(keep(call(*parts, w_out)))
         else:
+            call = pl.pallas_call(
+                functools.partial(project_kernel, relative=small),
+                out_shape=pltpu.VMEM((per * BLK, w_out.shape[1]), jnp.float32),
+                in_specs=[VMEM] * len(parts),
+                out_specs=VMEM,
+                cost_estimate=cost,
+                compiler_params=room(8),
+                name="project",
+            )
+            product = call(*parts[:-1], w_out)
             result = pl.pallas_call(
-                functools.partial(last_project_kernel, pieces=len(parts), relative=small),
+                functools.partial(last_project_kernel, relative=small, before=len(parts) - 1),
                 out_shape=jax.ShapeDtypeStruct((rows, w_out.shape[1]), jnp.bfloat16),
-                in_specs=[VMEM] * (len(parts) + 1 + len(earlier)),
+                in_specs=[VMEM] * (3 + len(earlier)),
                 out_specs=HBM,
                 scratch_shapes=[
                     pltpu.VMEM((per * BLK, w_out.shape[1]), jnp.bfloat16),
@@ -430,7 +440,7 @@
                 cost_estimate=cost,
                 compiler_params=room(8),
                 name="last_project",
-            )(*parts, w_out, *earlier)
+            )(keep(product), parts[-1], w_out, *earlier)
     return result
 
 

time: 43.1 us -> 43.6 us (1.012)
  waiting for transfers between devices: 15 us -> 15.9 us
    ppermute x3, waiting for transfers between devices: 5.34 us -> 6.29 us  [body(): lax.ppermute(attention, 'tp', [(i, i ^ 2) for i in range(tp_count)])]
    pallas_call x1 -> x2, Pallas kernels: 1.13 us -> 1.3 us  [the longest x1 0.93 us: body(): pl.pallas_call(functools.partial(last_project_kernel, relative=small, bef...]
  transfers between devices with their start and end apart: 16 -> 16, of which waited for: 7 -> 6; matrix products, arithmetic and copies ran while one was open for 0% -> 0% of each run, Pallas kernels for 9% -> 10%
where the time goes in v6:
time: 43.6 us; the launch traced here: 43.5 us
  starting transfers between devices  15.9 us (36%)
  waiting for transfers between devices  15.9 us (36%)
  Pallas kernels  11.5 us (26%)
    ppermute x4, waiting for transfers between devices, exchange(): return lax.ppermute(array, ('kv', 'tp'), pairs)  9.57 us
    ppermute x4, starting transfers between devices, exchange(): return lax.ppermute(array, ('kv', 'tp'), pairs)  8.06 us
    ppermute x3, waiting for transfers between devices, body(): lax.ppermute(attention, 'tp', [(i, i ^ 2) for i in range(tp_count)])  6.29 us
    ppermute x3, starting transfers between devices, body(): lax.ppermute(attention, 'tp', [(i, i ^ 2) for i in range(tp_count)])  3.73 us
    pallas_call x2, Pallas kernels, body(): attention = call(chosen, query, key_value)  3.67 us
    ppermute x3, starting transfers between devices, swap(): return lax.ppermute(array, 'tp', [(i, i ^ 1) for i in range(tp_count)])  2.93 us
    pallas_call x1, Pallas kernels, body(): pl.pallas_call(functools.partial(key_value_kernel, sharing=sharing), out_...  2.61 us
    pallas_call x1, Pallas kernels, body(): pl.pallas_call(functools.partial(first_attention_kernel, first=first, cou...  1.91 us
  transfers between devices with their start and end apart: 16, of which 6 were waited for; matrix products, arithmetic and copies ran while one was open for 0% of the time, Pallas kernels for 10%

profile of v6, /device:TPU:0, one launch (start us, length us, event | category | flops | bytes accessed | tf_op | source)
XLA Modules:
  0.0 43.5 jit_solution(14041084023674919891)
XLA Ops:
  0.0 2.6 %key_value.1.refs_2_ = bf16[384,256]{1,0:T(8,128)(2,1)S(1)} custom-call(bf16[384,2048]{1,0:T(8,128)(2,1)} %tokens.3, bf16[2048,256]{1,0:T(8,128)(2,1)} %w_key.1, bf16[2048,256]{1,0:T(8,128)(2,1)} %w_value.1, f32[2,48,128]{2,1,0:T(8,128)} %constant.4.clone.coarse.coarse_hbm, f32[2,64,128]{2,1,0:T(8,128)} %constant.5.clone.fine.fine_hbm), custom_call_target="tpu_custom_call" | custom-call | flops 402653184 | bytes 2621440 | tf_op jit(solution)/shard_map/key_value/pallas_call | solution.py:318
  2.6 3.1 %collective-permute-start = (bf16[384,256]{1,0:T(8,128)(2,1)S(1)}, bf16[384,256]{1,0:T(8,128)(2,1)S(1)}, u32[]{:S(2)}, u32[]{:S(2)}) collective-permute-start(bf16[384,256]{1,0:T(8,128)(2,1)S(1)} %key_value.1.refs_2_), channel_id=1, source_target_pairs={{0,8},{1,17},{2,10},{3,19},{4,12},{5,21},{6,14},{7,23},{8,0},{9,25... | collective-permute-start | bytes 589832 | tf_op jit(solution)/shard_map/ppermute | solution.py:270
  5.8 5.4 %collective-permute-done.second.refs_3_ = bf16[384,256]{1,0:T(8,128)(2,1)S(1)} collective-permute-done((bf16[384,256]{1,0:T(8,128)(2,1)S(1)}, bf16[384,256]{1,0:T(8,128)(2,1)S(1)}, u32[]{:S(2)}, u32[]{:S(2)}) %collective-permute-start) | collective-permute-done | bytes 196640 | tf_op jit(solution)/shard_map/ppermute | solution.py:270
  11.2 0.4 collective-permute-start.2
  11.5 1.6 %collective-permute-start.3 = (bf16[384,256]{1,0:T(8,128)(2,1)S(1)}, bf16[384,256]{1,0:T(8,128)(2,1)S(1)}, u32[]{:S(2)}, u32[]{:S(2)}) collective-permute-start(bf16[384,256]{1,0:T(8,128)(2,1)S(1)} %collective-permute-done.second.refs_3_), channel_id=1, source_target_pairs={{0,4},{1,9},{2,6},{3,11},{4,0},{5,13},{6,2},{7,15},{8,12},{9,1},{1... | collective-permute-start | bytes 589832 | tf_op jit(solution)/shard_map/ppermute | solution.py:270
  13.1 2.8 %collective-permute-start.4 = (bf16[384,256]{1,0:T(8,128)(2,1)S(1)}, bf16[384,256]{1,0:T(8,128)(2,1)S(1)}, u32[]{:S(2)}, u32[]{:S(2)}) collective-permute-start(bf16[384,256]{1,0:T(8,128)(2,1)S(1)} %choose.1), channel_id=1, source_target_pairs={{0,12},{1,5},{2,14},{3,7},{4,8},{5,1},{6,10},{7,3},{8,4},{9,13},{1... | collective-permute-start | bytes 589832 | tf_op jit(solution)/shard_map/ppermute | solution.py:270
  15.9 0.6 %collective-permute-start.1 = (bf16[384,256]{1,0:T(8,128)(2,1)S(1)}, bf16[384,256]{1,0:T(8,128)(2,1)S(1)}, u32[]{:S(2)}, u32[]{:S(2)}) collective-permute-start(bf16[384,256]{1,0:T(8,128)(2,1)S(1)} %key_value.1.refs_2_), channel_id=1, source_target_pairs={{0,4},{1,5},{2,6},{3,7},{4,0},{5,1},{6,2},{7,3},{8,12},{9,13},{10,... | collective-permute-start | bytes 589832 | tf_op jit(solution)/shard_map/ppermute | solution.py:270
  16.5 3.7 %collective-permute-done.3.refs_6_ = bf16[384,256]{1,0:T(8,128)(2,1)S(1)} collective-permute-done((bf16[384,256]{1,0:T(8,128)(2,1)S(1)}, bf16[384,256]{1,0:T(8,128)(2,1)S(1)}, u32[]{:S(2)}, u32[]{:S(2)}) %collective-permute-start.3) | collective-permute-done | bytes 196640 | tf_op jit(solution)/shard_map/ppermute | solution.py:270
  20.2 2.6 %collective-permute-start.6 = (bf16[384,256]{1,0:T(8,128)(2,1)S(1)}, bf16[384,256]{1,0:T(8,128)(2,1)S(1)}, u32[]{:S(2)}, u32[]{:S(2)}) collective-permute-start(bf16[384,256]{1,0:T(8,128)(2,1)S(1)} %collective-permute-done.4.refs_7_), channel_id=1, source_target_pairs={{0,1},{1,0},{2,3},{3,2},{4,5},{5,4},{6,7},{7,6},{8,9},{9,8},{10,11... | collective-permute-start | bytes 589832 | tf_op jit(solution)/shard_map/ppermute | solution.py:273
  22.8 1.1 %query.1.refs_1_ = bf16[384,512]{1,0:T(8,128)(2,1)S(1)} custom-call(bf16[384,2048]{1,0:T(8,128)(2,1)S(1)} %copy-done.1, bf16[2048,512]{1,0:T(8,128)(2,1)S(1)} %copy-done.2, f32[2,48,128]{2,1,0:T(8,128)S(1)} %copy-done.4, f32[2,64,128]{2,1,0:T(8,128)S(1)} %copy-done.3), custom_call_target="tpu_custom_call" | custom-call | flops 805306368 | bytes 3670016 | tf_op jit(solution)/shard_map/query/pallas_call | solution.py:339
  23.9 0.5 %collective-permute-done.1.refs_4_ = bf16[384,256]{1,0:T(8,128)(2,1)S(1)} collective-permute-done((bf16[384,256]{1,0:T(8,128)(2,1)S(1)}, bf16[384,256]{1,0:T(8,128)(2,1)S(1)}, u32[]{:S(2)}, u32[]{:S(2)}) %collective-permute-start.1) | collective-permute-done | bytes 196640 | tf_op jit(solution)/shard_map/ppermute | solution.py:270
  24.4 1.9 %first_attention.1 = (bf16[128,512]{1,0:T(8,128)(2,1)S(1)}, bf16[3072,256]{1,0:T(8,128)(2,1)S(1)}) custom-call(s32[6,32]{1,0:T(8,128)S(1)} %copy-done.5, bf16[384,512]{1,0:T(8,128)(2,1)S(1)} %query.1.refs_1_, bf16[384,256]{1,0:T(8,128)(2,1)S(1)} %key_value.1.refs_2_, bf16[384,256]{1,0:T(8,128)(2,1)S(1)} %collective-permute-done.second.refs_3_, ...), custom_call_target="tpu_custom_call" | custom-call | flops 553648128 | bytes 131072 | tf_op jit(solution)/shard_map/first_attention/pallas_call | solution.py:375
  26.3 1.8 %attention.3.refs_0_ = bf16[128,512]{1,0:T(8,128)(2,1)S(1)} custom-call(s32[6,32]{1,0:T(8,128)S(1)} %copy-done.5, bf16[384,512]{1,0:T(8,128)(2,1)S(1)} %query.1.refs_1_, bf16[3072,256]{1,0:T(8,128)(2,1)S(1)} %get-tuple-element.7.key_value), custom_call_target="tpu_custom_call" | custom-call | flops 553648128 | bytes 131072 | tf_op jit(solution)/shard_map/attention/pallas_call | solution.py:397
  28.2 1.6 %collective-permute-start.14 = (bf16[128,512]{1,0:T(8,128)(2,1)S(1)}, bf16[128,512]{1,0:T(8,128)(2,1)S(1)}, u32[]{:S(2)}, u32[]{:S(2)}) collective-permute-start(bf16[128,512]{1,0:T(8,128)(2,1)S(1)} %attention.3.refs_0_), channel_id=1, source_target_pairs={{0,2},{1,3},{2,0},{3,1},{4,6},{5,7},{6,4},{7,5},{8,10},{9,11},{10,... | collective-permute-start | bytes 393224 | tf_op jit(solution)/shard_map/ppermute | solution.py:400
  29.8 1.8 %attention.2.refs_0_ = bf16[128,512]{1,0:T(8,128)(2,1)S(1)} custom-call(s32[6,32]{1,0:T(8,128)S(1)} %copy-done.5, bf16[384,512]{1,0:T(8,128)(2,1)S(1)} %query.1.refs_1_, bf16[3072,256]{1,0:T(8,128)(2,1)S(1)} %get-tuple-element.7.key_value), custom_call_target="tpu_custom_call" | custom-call | flops 553648128 | bytes 131072 | tf_op jit(solution)/shard_map/attention/pallas_call | solution.py:397
  31.7 0.5 %collective-permute-start.8 = (bf16[128,512]{1,0:T(8,128)(2,1)S(1)}, bf16[128,512]{1,0:T(8,128)(2,1)S(1)}, u32[]{:S(2)}, u32[]{:S(2)}) collective-permute-start(bf16[128,512]{1,0:T(8,128)(2,1)S(1)} %attention.2.refs_0_), channel_id=1, source_target_pairs={{0,2},{1,3},{2,0},{3,1},{4,6},{5,7},{6,4},{7,5},{8,10},{9,11},{10,... | collective-permute-start | bytes 393224 | tf_op jit(solution)/shard_map/ppermute | solution.py:400
  32.2 1.6 %collective-permute-start.11 = (bf16[128,512]{1,0:T(8,128)(2,1)S(1)}, bf16[128,512]{1,0:T(8,128)(2,1)S(1)}, u32[]{:S(2)}, u32[]{:S(2)}) collective-permute-start(bf16[128,512]{1,0:T(8,128)(2,1)S(1)} %get-tuple-element.8.refs_0_), channel_id=1, source_target_pairs={{0,2},{1,3},{2,0},{3,1},{4,6},{5,7},{6,4},{7,5},{8,10},{9,11},{10,... | collective-permute-start | bytes 393224 | tf_op jit(solution)/shard_map/ppermute | solution.py:400
  34.6 3.4 %collective-permute-done.8.refs_2_ = bf16[128,512]{1,0:T(8,128)(2,1)S(1)} collective-permute-done((bf16[128,512]{1,0:T(8,128)(2,1)S(1)}, bf16[128,512]{1,0:T(8,128)(2,1)S(1)}, u32[]{:S(2)}, u32[]{:S(2)}) %collective-permute-start.8) | collective-permute-done | bytes 131104 | tf_op jit(solution)/shard_map/ppermute | solution.py:400
  38.1 2.6 %collective-permute-done.11.refs_2_ = bf16[128,512]{1,0:T(8,128)(2,1)S(1)} collective-permute-done((bf16[128,512]{1,0:T(8,128)(2,1)S(1)}, bf16[128,512]{1,0:T(8,128)(2,1)S(1)}, u32[]{:S(2)}, u32[]{:S(2)}) %collective-permute-start.11) | collective-permute-done | bytes 131104 | tf_op jit(solution)/shard_map/ppermute | solution.py:400
  40.7 0.5 %collective-permute-start.9 = (bf16[128,512]{1,0:T(8,128)(2,1)S(1)}, bf16[128,512]{1,0:T(8,128)(2,1)S(1)}, u32[]{:S(2)}, u32[]{:S(2)}) collective-permute-start(bf16[128,512]{1,0:T(8,128)(2,1)S(1)} %collective-permute-done.8.refs_2_), channel_id=1, source_target_pairs={{0,1},{1,0},{2,3},{3,2},{4,5},{5,4},{6,7},{7,6},{8,9},{9,8},{10,11... | collective-permute-start | bytes 393224 | tf_op jit(solution)/shard_map/ppermute | solution.py:401
  41.2 0.4 project.3.refs_0_
  41.6 0.5 %project.5.refs_4_ = bf16[128,512]{1,0:T(8,128)(2,1)S(1)} custom-call(bf16[128,512]{1,0:T(8,128)(2,1)S(1)} %attention.3.refs_0_, bf16[128,512]{1,0:T(8,128)(2,1)S(1)} %collective-permute-done.13.refs_1_, bf16[128,512]{1,0:T(8,128)(2,1)S(1)} %collective-permute-done.14.refs_2_, bf16[128,512]{1,0:T(8,128)(2,1)S(1)} %collective-permute-done.15.refs_3_, ...), custom_call_target="tpu_custom_call" | custom-call | flops 268435456 | tf_op jit(solution)/shard_map/project/pallas_call | solution.py:419
  42.1 0.4 %project.4.refs_3_ = bf16[128,512]{1,0:T(8,128)(2,1)S(1)} custom-call(bf16[128,512]{1,0:T(8,128)(2,1)S(1)} %get-tuple-element.8.refs_0_, bf16[128,512]{1,0:T(8,128)(2,1)S(1)} %collective-permute-done.10.refs_1_, bf16[128,512]{1,0:T(8,128)(2,1)S(1)} %collective-permute-done.11.refs_2_, bf16[128,512]{1,0:T(8,128)(2,1)S(1)} %collective-permute-done.12.refs_3_, ...), custom_call_target="tpu_custom_call" | custom-call | flops 268435456 | tf_op jit(solution)/shard_map/project/pallas_call | solution.py:419
  42.5 0.9 %last_project.1 = bf16[384,512]{1,0:T(8,128)(2,1)} custom-call(f32[128,512]{1,0:T(8,128)S(1)} %project.3.refs_0_, bf16[128,512]{1,0:T(8,128)(2,1)S(1)} %collective-permute-done.9.refs_1_, bf16[2048,512]{1,0:T(8,128)(2,1)S(1)} %copy-done, bf16[128,512]{1,0:T(8,128)(2,1)S(1)} %project.4.refs_3_, bf16[128,512]{1,0:T(8,128)(2,1)S(1)} %project.5.refs_4_), custom_call_target="tpu_custom_call" | custom-call | flops 268435456 | tf_op jit(solution)/shard_map/last_project/pallas_call | solution.py:431
  (30 shorter events, 1.0 us)
Async XLA Ops:
  0.0 22.8 %copy-start.3 = (f32[2,64,128]{2,1,0:T(8,128)S(1)}, f32[2,64,128]{2,1,0:T(8,128)}, u32[]{:S(2)}) copy-start(f32[2,64,128]{2,1,0:T(8,128)} %constant.5.clone.fine.fine_hbm) | copy-start | bytes 196612
  0.0 22.8 %copy-start.4 = (f32[2,48,128]{2,1,0:T(8,128)S(1)}, f32[2,48,128]{2,1,0:T(8,128)}, u32[]{:S(2)}) copy-start(f32[2,48,128]{2,1,0:T(8,128)} %constant.4.clone.coarse.coarse_hbm) | copy-start | bytes 147460
  0.0 22.8 %copy-start.1 = (bf16[384,2048]{1,0:T(8,128)(2,1)S(1)}, bf16[384,2048]{1,0:T(8,128)(2,1)}, u32[]{:S(2)}) copy-start(bf16[384,2048]{1,0:T(8,128)(2,1)} %tokens.3) | copy-start | bytes 4718596
  0.0 22.8 %copy-start.2 = (bf16[2048,512]{1,0:T(8,128)(2,1)S(1)}, bf16[2048,512]{1,0:T(8,128)(2,1)}, u32[]{:S(2)}) copy-start(bf16[2048,512]{1,0:T(8,128)(2,1)} %w_query.1) | copy-start | bytes 6291460
  2.6 8.6 %collective-permute-start = (bf16[384,256]{1,0:T(8,128)(2,1)S(1)}, bf16[384,256]{1,0:T(8,128)(2,1)S(1)}, u32[]{:S(2)}, u32[]{:S(2)}) collective-permute-start(bf16[384,256]{1,0:T(8,128)(2,1)S(1)} %key_value.1.refs_2_), channel_id=1, source_target_pairs={{0,8},{1,17},{2,10},{3,19},{4,12},{5,21},{6,14},{7,23},{8,0},{9,25... | collective-permute-start | bytes 589832 | tf_op jit(solution)/shard_map/ppermute | solution.py:270
  11.2 1.9 %collective-permute-start.2 = (bf16[384,256]{1,0:T(8,128)(2,1)S(1)}, bf16[384,256]{1,0:T(8,128)(2,1)S(1)}, u32[]{:S(2)}, u32[]{:S(2)}) collective-permute-start(bf16[384,256]{1,0:T(8,128)(2,1)S(1)} %collective-permute-done.second.refs_3_), channel_id=1, source_target_pairs={{0,1},{1,0},{2,3},{3,2},{4,5},{5,4},{6,7},{7,6},{8,9},{9,8},{10,11... | collective-permute-start | bytes 589832 | tf_op jit(solution)/shard_map/ppermute | solution.py:273
  11.5 8.6 %collective-permute-start.3 = (bf16[384,256]{1,0:T(8,128)(2,1)S(1)}, bf16[384,256]{1,0:T(8,128)(2,1)S(1)}, u32[]{:S(2)}, u32[]{:S(2)}) collective-permute-start(bf16[384,256]{1,0:T(8,128)(2,1)S(1)} %collective-permute-done.second.refs_3_), channel_id=1, source_target_pairs={{0,4},{1,9},{2,6},{3,11},{4,0},{5,13},{6,2},{7,15},{8,12},{9,1},{1... | collective-permute-start | bytes 589832 | tf_op jit(solution)/shard_map/ppermute | solution.py:270
  13.1 11.3 %copy-start.5 = (s32[6,32]{1,0:T(8,128)S(1)}, s32[6,32]{1,0:T(8,128)}, u32[]{:S(2)}) copy-start(s32[6,32]{1,0:T(8,128)} %chosen.3) | copy-start | bytes 2308
  13.1 7.1 %collective-permute-start.4 = (bf16[384,256]{1,0:T(8,128)(2,1)S(1)}, bf16[384,256]{1,0:T(8,128)(2,1)S(1)}, u32[]{:S(2)}, u32[]{:S(2)}) collective-permute-start(bf16[384,256]{1,0:T(8,128)(2,1)S(1)} %choose.1), channel_id=1, source_target_pairs={{0,12},{1,5},{2,14},{3,7},{4,8},{5,1},{6,10},{7,3},{8,4},{9,13},{1... | collective-permute-start | bytes 589832 | tf_op jit(solution)/shard_map/ppermute | solution.py:270
  15.9 8.5 %collective-permute-start.1 = (bf16[384,256]{1,0:T(8,128)(2,1)S(1)}, bf16[384,256]{1,0:T(8,128)(2,1)S(1)}, u32[]{:S(2)}, u32[]{:S(2)}) collective-permute-start(bf16[384,256]{1,0:T(8,128)(2,1)S(1)} %key_value.1.refs_2_), channel_id=1, source_target_pairs={{0,4},{1,5},{2,6},{3,7},{4,0},{5,1},{6,2},{7,3},{8,12},{9,13},{10,... | collective-permute-start | bytes 589832 | tf_op jit(solution)/shard_map/ppermute | solution.py:270
  20.2 4.2 %collective-permute-start.5 = (bf16[384,256]{1,0:T(8,128)(2,1)S(1)}, bf16[384,256]{1,0:T(8,128)(2,1)S(1)}, u32[]{:S(2)}, u32[]{:S(2)}) collective-permute-start(bf16[384,256]{1,0:T(8,128)(2,1)S(1)} %collective-permute-done.3.refs_6_), channel_id=1, source_target_pairs={{0,1},{1,0},{2,3},{3,2},{4,5},{5,4},{6,7},{7,6},{8,9},{9,8},{10,11... | collective-permute-start | bytes 589832 | tf_op jit(solution)/shard_map/ppermute | solution.py:273
  20.2 4.2 %collective-permute-start.6 = (bf16[384,256]{1,0:T(8,128)(2,1)S(1)}, bf16[384,256]{1,0:T(8,128)(2,1)S(1)}, u32[]{:S(2)}, u32[]{:S(2)}) collective-permute-start(bf16[384,256]{1,0:T(8,128)(2,1)S(1)} %collective-permute-done.4.refs_7_), channel_id=1, source_target_pairs={{0,1},{1,0},{2,3},{3,2},{4,5},{5,4},{6,7},{7,6},{8,9},{9,8},{10,11... | collective-permute-start | bytes 589832 | tf_op jit(solution)/shard_map/ppermute | solution.py:273
  26.3 14.9 %copy-start = (bf16[2048,512]{1,0:T(8,128)(2,1)S(1)}, bf16[2048,512]{1,0:T(8,128)(2,1)}, u32[]{:S(2)}) copy-start(bf16[2048,512]{1,0:T(8,128)(2,1)} %refs_2_.1) | copy-start | bytes 6291460
  28.2 6.3 %collective-permute-start.14 = (bf16[128,512]{1,0:T(8,128)(2,1)S(1)}, bf16[128,512]{1,0:T(8,128)(2,1)S(1)}, u32[]{:S(2)}, u32[]{:S(2)}) collective-permute-start(bf16[128,512]{1,0:T(8,128)(2,1)S(1)} %attention.3.refs_0_), channel_id=1, source_target_pairs={{0,2},{1,3},{2,0},{3,1},{4,6},{5,7},{6,4},{7,5},{8,10},{9,11},{10,... | collective-permute-start | bytes 393224 | tf_op jit(solution)/shard_map/ppermute | solution.py:400
  31.7 6.4 %collective-permute-start.8 = (bf16[128,512]{1,0:T(8,128)(2,1)S(1)}, bf16[128,512]{1,0:T(8,128)(2,1)S(1)}, u32[]{:S(2)}, u32[]{:S(2)}) collective-permute-start(bf16[128,512]{1,0:T(8,128)(2,1)S(1)} %attention.2.refs_0_), channel_id=1, source_target_pairs={{0,2},{1,3},{2,0},{3,1},{4,6},{5,7},{6,4},{7,5},{8,10},{9,11},{10,... | collective-permute-start | bytes 393224 | tf_op jit(solution)/shard_map/ppermute | solution.py:400
  32.2 8.5 %collective-permute-start.11 = (bf16[128,512]{1,0:T(8,128)(2,1)S(1)}, bf16[128,512]{1,0:T(8,128)(2,1)S(1)}, u32[]{:S(2)}, u32[]{:S(2)}) collective-permute-start(bf16[128,512]{1,0:T(8,128)(2,1)S(1)} %get-tuple-element.8.refs_0_), channel_id=1, source_target_pairs={{0,2},{1,3},{2,0},{3,1},{4,6},{5,7},{6,4},{7,5},{8,10},{9,11},{10,... | collective-permute-start | bytes 393224 | tf_op jit(solution)/shard_map/ppermute | solution.py:400
  33.7 6.9 %collective-permute-start.7 = (bf16[128,512]{1,0:T(8,128)(2,1)S(1)}, bf16[128,512]{1,0:T(8,128)(2,1)S(1)}, u32[]{:S(2)}, u32[]{:S(2)}) collective-permute-start(bf16[128,512]{1,0:T(8,128)(2,1)S(1)} %attention.2.refs_0_), channel_id=1, source_target_pairs={{0,1},{1,0},{2,3},{3,2},{4,5},{5,4},{6,7},{7,6},{8,9},{9,8},{10,11... | collective-permute-start | bytes 393224 | tf_op jit(solution)/shard_map/ppermute | solution.py:399
  33.9 7.6 %collective-permute-start.13 = (bf16[128,512]{1,0:T(8,128)(2,1)S(1)}, bf16[128,512]{1,0:T(8,128)(2,1)S(1)}, u32[]{:S(2)}, u32[]{:S(2)}) collective-permute-start(bf16[128,512]{1,0:T(8,128)(2,1)S(1)} %attention.3.refs_0_), channel_id=1, source_target_pairs={{0,1},{1,0},{2,3},{3,2},{4,5},{5,4},{6,7},{7,6},{8,9},{9,8},{10,11... | collective-permute-start | bytes 393224 | tf_op jit(solution)/shard_map/ppermute | solution.py:399
  34.5 7.0 %collective-permute-start.15 = (bf16[128,512]{1,0:T(8,128)(2,1)S(1)}, bf16[128,512]{1,0:T(8,128)(2,1)S(1)}, u32[]{:S(2)}, u32[]{:S(2)}) collective-permute-start(bf16[128,512]{1,0:T(8,128)(2,1)S(1)} %collective-permute-done.14.refs_2_), channel_id=1, source_target_pairs={{0,1},{1,0},{2,3},{3,2},{4,5},{5,4},{6,7},{7,6},{8,9},{9,8},{10,11... | collective-permute-start | bytes 393224 | tf_op jit(solution)/shard_map/ppermute | solution.py:401
  38.1 4.0 %collective-permute-start.10 = (bf16[128,512]{1,0:T(8,128)(2,1)S(1)}, bf16[128,512]{1,0:T(8,128)(2,1)S(1)}, u32[]{:S(2)}, u32[]{:S(2)}) collective-permute-start(bf16[128,512]{1,0:T(8,128)(2,1)S(1)} %get-tuple-element.8.refs_0_), channel_id=1, source_target_pairs={{0,1},{1,0},{2,3},{3,2},{4,5},{5,4},{6,7},{7,6},{8,9},{9,8},{10,11... | collective-permute-start | bytes 393224 | tf_op jit(solution)/shard_map/ppermute | solution.py:399
  40.7 1.4 %collective-permute-start.12 = (bf16[128,512]{1,0:T(8,128)(2,1)S(1)}, bf16[128,512]{1,0:T(8,128)(2,1)S(1)}, u32[]{:S(2)}, u32[]{:S(2)}) collective-permute-start(bf16[128,512]{1,0:T(8,128)(2,1)S(1)} %collective-permute-done.11.refs_2_), channel_id=1, source_target_pairs={{0,1},{1,0},{2,3},{3,2},{4,5},{5,4},{6,7},{7,6},{8,9},{9,8},{10,11... | collective-permute-start | bytes 393224 | tf_op jit(solution)/shard_map/ppermute | solution.py:401
  40.7 1.8 %collective-permute-start.9 = (bf16[128,512]{1,0:T(8,128)(2,1)S(1)}, bf16[128,512]{1,0:T(8,128)(2,1)S(1)}, u32[]{:S(2)}, u32[]{:S(2)}) collective-permute-start(bf16[128,512]{1,0:T(8,128)(2,1)S(1)} %collective-permute-done.8.refs_2_), channel_id=1, source_target_pairs={{0,1},{1,0},{2,3},{3,2},{4,5},{5,4},{6,7},{7,6},{8,9},{9,8},{10,11... | collective-permute-start | bytes 393224 | tf_op jit(solution)/shard_map/ppermute | solution.py:401
